TPU v7x, 256 devices: a whole 4x4x8 slice. The times are simulated.
256 devices in a mesh: sp: 64 (over z, y, core), tp: 4 (over x).
Axes of the slice: x: 4, y: 4, z: 8, core: 2. Of those that a mesh axis runs over, the one named last changes fastest.
Arguments:
- queries: bfloat16 [8192, 2048], P('sp', 'tp'), may hold values from -6 to 6
- forget_logits: bfloat16 [2, 8192, 2048], P(None, 'sp', 'tp'), may hold values from -7.5 to 7.5
- value_matrix: bfloat16 [8192, 2048], P('sp', 'tp'), may hold values from -6 to 6
- output_gate_logits: bfloat16 [8192, 2048], P('sp', 'tp'), may hold values from -6 to 6
- forget_slack: float32 [2048], P('tp'), may hold values from 6.1035156e-05 to 0.07
- spike_log_forget: float32 [8192, 16], P('sp', 'tp'), may hold values from -2.8 to 0, as said below
- head_norm_gain: bfloat16 [128], replicated, may hold values from 0.099609375 to 1.8984375
- output_weight: bfloat16 [2048, 2048], P('tp'), may hold values from -0.125 to 0.125
- residual: bfloat16 [8192, 2048], P('sp'), may hold values from -6 to 6
- mixer_norm_gain: bfloat16 [2048], replicated, may hold values from 0.099609375 to 1.8984375
- mixer_gate_weight: bfloat16 [2048, 5632], P('sp', 'tp'), may hold values from -0.125 to 0.125
- mixer_up_weight: bfloat16 [2048, 5632], P('sp', 'tp'), may hold values from -0.125 to 0.125
- mixer_down_weight: bfloat16 [5632, 2048], P('tp', 'sp'), may hold values from -0.078125 to 0.078125
Outputs:
- layer_out: bfloat16 [8192, 2048], P(('sp', 'tp'))
Inputs may be any that keep to these rules, and one draw needn't show every extreme that they name: `spike_log_forget`: zero at all but a few tokens.
All inputs are finite; a program needn't handle non-finite values.
Results may differ from a plain program's by a relative error of at most 0.015.
Values may be sent and summed in bfloat16 or wider, within the bound.
No kernel may reach another device: no remote copies, remote signals or barrier semaphores. Data moves between devices by JAX's collectives and lax.ppermute only.
A program may use at most 128 MiB of HBM per device.

v0:
```python
import jax
import jax.numpy as jnp
from jax import lax
from jax.experimental import pallas as pl
from jax.experimental.pallas import tpu as pltpu
from jax.sharding import Mesh
from jax.sharding import PartitionSpec as P


SP = ("sp_0", "sp_1", "sp_2")
SP_TP = ("sp_0", "sp_1", "sp_2", "tp")
NORM_EPS = 1e-06
F32 = jnp.float32
BF16 = jnp.bfloat16
HEAD = 128


def nt_dot(a, b):
    return lax.dot_general(a, b, (((1,), (1,)), ((), ())), preferred_element_type=F32)


def tn_dot(a, b):
    return lax.dot_general(a, b, (((0,), (0,)), ((), ())), preferred_element_type=F32)


def in_three(a):
    high = a.astype(BF16)
    rest = a - high.astype(F32)
    middle = rest.astype(BF16)
    return high, middle, (rest - middle.astype(F32)).astype(BF16)


def local_body(q_ref, f_ref, v_ref, slack_ref, spike_ref, send_ref, near_ref, reach_ref):
    rows = q_ref.shape[0]
    heads = spike_ref.shape[0]
    chunk = send_ref.shape[1] - 8
    pieces = HEAD // chunk
    at_row = lax.broadcasted_iota(jnp.int32, (rows, rows), 0)
    at_col = lax.broadcasted_iota(jnp.int32, (rows, rows), 1)
    spikes = []
    for w in range(2):
        keep = at_row >= at_col if w == 0 else at_row <= at_col
        ones = keep.astype(BF16)
        high, middle, low = in_three(spike_ref[...])
        spikes.append(nt_dot(ones, low) + nt_dot(ones, middle) + nt_dot(ones, high))
    for h in range(heads):
        cols = slice(h * HEAD, (h + 1) * HEAD)
        q = q_ref[:, cols].astype(F32)
        q = q * jax.nn.sigmoid(q) * HEAD ** (-0.5)
        v = v_ref[:, cols]
        scores = jnp.zeros((rows, rows), F32)
        for w in range(2):
            keep = at_row >= at_col if w == 0 else at_row <= at_col
            key = slack_ref[:, cols] * jax.nn.sigmoid(-f_ref[w, :, cols].astype(F32))
            decay = jnp.log1p(-key)
            ones = keep.astype(BF16)
            high, middle, low = in_three(decay)
            running = (
                jnp.dot(ones, low, preferred_element_type=F32)
                + jnp.dot(ones, middle, preferred_element_type=F32)
                + jnp.dot(ones, high, preferred_element_type=F32)
                + spikes[w][:, h : h + 1]
            )
            final = running[rows - 1 : rows] if w == 0 else running[0:1]
            q_scaled = (q * jnp.exp(running)).astype(BF16)
            k_scaled = (key * jnp.exp(-running)).astype(BF16)
            scores = scores + jnp.where(keep, nt_dot(q_scaled, k_scaled), 0.0)
            k_end = (key * jnp.exp(final - running)).astype(BF16)
            state = tn_dot(v, k_end).astype(BF16)
            reach_ref[w, :, cols] = q_scaled
            at = (w * heads + h) * pieces
            send_ref[at : at + pieces, 0:chunk, :] = state.reshape(pieces, chunk, HEAD)
            total = jnp.concatenate([t.astype(F32) for t in in_three(jnp.exp(final))], axis=0)
            total = jnp.concatenate([total, jnp.zeros((5, HEAD), F32)], axis=0).astype(BF16)
            send_ref[at : at + pieces, chunk : chunk + 8, :] = jnp.broadcast_to(
                total[None], (pieces, 8, HEAD)
            )
        near_ref[:, cols] = jnp.dot(scores.astype(BF16), v, preferred_element_type=F32)


def scan_body(back_ref, got_ref, give_ref):
    blocks, wide, _ = got_ref.shape
    chunk = wide - 8
    back = back_ref[0]
    state = jnp.zeros((chunk, HEAD), F32)
    for b in range(blocks):
        at = jnp.where(back == 1, blocks - 1 - b, b)
        give_ref[at] = state.astype(BF16)
        piece = got_ref[at].astype(F32)
        total = piece[chunk : chunk + 1] + piece[chunk + 1 : chunk + 2] + piece[chunk + 2 : chunk + 3]
        state = total * state + piece[0:chunk]


def project_body(
    own_ref, near_ref, reach_ref, enter_ref, gate_ref, gain_ref, weight_ref, o0, o1, o2, o3, mixed_ref
):
    heads = near_ref.shape[1] // HEAD
    gain = gain_ref[...].astype(F32)
    for h in range(heads):
        cols = slice(h * HEAD, (h + 1) * HEAD)
        mix = near_ref[:, cols]
        mix = mix + nt_dot(reach_ref[0, :, cols], enter_ref[h])
        mix = mix + nt_dot(reach_ref[1, :, cols], enter_ref[heads + h])
        scale = lax.rsqrt(jnp.mean(mix * mix, axis=-1, keepdims=True) + NORM_EPS)
        g = gate_ref[:, cols].astype(F32)
        mixed_ref[:, cols] = (mix * scale * gain * (g * jax.nn.sigmoid(g))).astype(BF16)
    outs = (o0, o1, o2, o3)
    part = o0.shape[0]
    own = own_ref[0]
    for d in range(len(outs)):
        at = pl.multiple_of(lax.rem(own + d, len(outs)) * part, part)
        outs[d][...] = jnp.dot(
            mixed_ref[pl.ds(at, part), :], weight_ref[...], preferred_element_type=F32
        ).astype(BF16)


def halves_body(parity_ref, gate_ref, up_ref, down_ref, keep_ref, give_ref):
    hidden = gate_ref.shape[1]
    width = keep_ref.shape[1] // 3

    def write(out_ref, start):
        for k, ref in enumerate((gate_ref, up_ref, down_ref)):
            out_ref[:, k * width : (k + 1) * width] = ref[:, start : start + width]

    @pl.when(parity_ref[0] == 0)
    def _():
        write(keep_ref, 0)
        write(give_ref, hidden - width)

    @pl.when(parity_ref[0] != 0)
    def _():
        write(keep_ref, hidden - width)
        write(give_ref, 0)


def mixer_body(at_ref, tokens_ref, whole_ref, o0, o1, o2, o3, weights_ref, act_ref, sems, *, hidden):
    z_size, y_size, cores, _, wide = weights_ref.shape
    model = tokens_ref.shape[1]
    y = at_ref[0]
    chunks = 2
    z_step = z_size // chunks
    step = model // chunks
    width = wide // 3
    groups = []
    for n in range(chunks):
        z = slice(n * z_step, (n + 1) * z_step)
        group = []
        for c in range(cores):
            for k in range(y_size):
                group.append(
                    pltpu.make_async_copy(
                        whole_ref.at[z, c, k],
                        weights_ref.at[z, lax.rem(y + y_size - k, y_size), c],
                        sems.at[(n * cores + c) * y_size + k],
                    )
                )
        groups.append(group)
    for group in groups:
        for copy in group:
            copy.start()
    weights = weights_ref.reshape(model, wide)
    for n, group in enumerate(groups):
        for copy in group:
            copy.wait()
        at = slice(n * step, (n + 1) * step)
        term = jnp.dot(tokens_ref[:, at], weights[at, : 2 * width], preferred_element_type=F32)
        if n == 0:
            act_ref[...] = term
        else:
            act_ref[...] += term
    gate, up = act_ref[:, :width], act_ref[:, width:]
    inner = gate * jax.nn.sigmoid(gate) * up
    lane = lax.broadcasted_iota(jnp.int32, inner.shape, 1)
    low = jnp.where(lax.rem(y, 2) == 0, 0, width - hidden // 2)
    inner = jnp.where((lane >= low) & (lane < low + hidden // 2), inner, 0.0).astype(BF16)
    lowered = nt_dot(inner, weights[:, 2 * width :])
    part = o0.shape[0]
    for d, out_ref in enumerate((o0, o1, o2, o3)):
        out_ref[...] = lowered[d * part : (d + 1) * part].astype(out_ref.dtype)


VMEM = pl.BlockSpec(memory_space=pltpu.VMEM)
ANY = pl.BlockSpec(memory_space=pl.ANY)
SMEM = pl.BlockSpec(memory_space=pltpu.SMEM)


def shift(array, axis, by):
    size = lax.axis_size(axis)
    return lax.ppermute(array, axis, [(k, (k + by) % size) for k in range(size)])


def local(
    queries,
    forget_logits,
    value_matrix,
    output_gate_logits,
    forget_slack,
    spike_log_forget,
    head_norm_gain,
    output_weight,
    residual,
    mixer_norm_gain,
    mixer_gate_weight,
    mixer_up_weight,
    mixer_down_weight,
):
    rows, width = queries.shape
    heads = spike_log_forget.shape[1]
    model = output_weight.shape[1]
    hidden = mixer_gate_weight.shape[1]
    blocks = lax.axis_size(SP)
    n_tp = lax.axis_size("tp")
    sp_at = lax.axis_index(SP)
    tp_at = lax.axis_index("tp")
    chunk = 2 * heads * HEAD // blocks

    z_size, y_size, cores = (lax.axis_size(axis) for axis in SP)
    y_at = lax.axis_index("sp_1")
    slab = mixer_gate_weight.shape[0]
    half = (hidden // 2 + HEAD - 1) // HEAD * HEAD
    send, near, reach = pl.pallas_call(
        local_body,
        out_shape=(
            jax.ShapeDtypeStruct((blocks, chunk + 8, HEAD), BF16),
            jax.ShapeDtypeStruct((rows, width), F32),
            jax.ShapeDtypeStruct((2, rows, width), BF16),
        ),
        in_specs=[VMEM] * 5,
        out_specs=(VMEM,) * 3,
        name="local_sweep",
    )(queries, forget_logits, value_matrix, forget_slack[None], spike_log_forget.T)
    weights = (mixer_gate_weight, mixer_up_weight, mixer_down_weight.T)
    weights, send = lax.optimization_barrier((weights, send))
    got = lax.all_to_all(send, SP, 0, 0, tiled=True)
    keep, give = pl.pallas_call(
        halves_body,
        out_shape=(jax.ShapeDtypeStruct((slab, 3 * half), BF16),) * 2,
        in_specs=[SMEM] + [VMEM] * 3,
        out_specs=(VMEM,) * 2,
        name="weight_halves",
    )((y_at % 2)[None], *weights)
    line = [keep] + [shift(give if d % 2 else keep, "sp_1", d) for d in range(1, y_size)]
    whole = lax.all_gather(
        jnp.concatenate(line, axis=0), ("sp_0", "sp_2"), axis=0, tiled=True
    ).reshape(z_size, cores, y_size, slab, 3 * half)
    give = pl.pallas_call(
        scan_body,
        out_shape=jax.ShapeDtypeStruct((blocks, chunk, HEAD), BF16),
        in_specs=[SMEM, VMEM],
        out_specs=VMEM,
        name="block_scan",
    )((sp_at >= blocks // 2).astype(jnp.int32)[None], got)
    enter = lax.all_to_all(give, SP, 0, 0, tiled=True).reshape(2 * heads, HEAD, HEAD)

    part = rows // n_tp
    parts = pl.pallas_call(
        project_body,
        out_shape=(jax.ShapeDtypeStruct((part, model), BF16),) * n_tp,
        in_specs=[SMEM] + [VMEM] * 6,
        out_specs=(VMEM,) * n_tp,
        scratch_shapes=[pltpu.VMEM((rows, width), BF16)],
        name="norm_project",
    )(tp_at[None], near, reach, enter, output_gate_logits, head_norm_gain[None], output_weight)

    arrived = [parts[0]] + [shift(parts[d], "tp", d) for d in range(1, n_tp)]
    own_resid = lax.dynamic_slice_in_dim(residual, tp_at * part, part, 0)
    hidden_f = own_resid.astype(F32)
    for a in arrived:
        hidden_f = hidden_f + a.astype(F32)
    hidden_state = hidden_f.astype(BF16)
    held = hidden_state.astype(F32)
    normed = (
        held
        * lax.rsqrt(jnp.mean(held * held, axis=-1, keepdims=True) + NORM_EPS)
        * mixer_norm_gain.astype(F32)
    ).astype(BF16)
    swap = [(k, k ^ 1) for k in range(y_size)]
    both = jnp.concatenate([normed, lax.ppermute(normed, "sp_1", swap)], axis=0)
    tokens = jnp.concatenate([both] + [shift(both, "tp", d) for d in range(1, n_tp)], axis=0)
    lowered = pl.pallas_call(
        lambda *refs: mixer_body(*refs, hidden=hidden),
        out_shape=(jax.ShapeDtypeStruct((2 * part, model), F32),)
        + (jax.ShapeDtypeStruct((2 * part, model), BF16),) * (n_tp - 1),
        in_specs=[SMEM, VMEM, ANY],
        out_specs=(VMEM,) * n_tp,
        scratch_shapes=[
            pltpu.VMEM((z_size, y_size, cores, slab, 3 * half), BF16),
            pltpu.VMEM((2 * rows, 2 * half), F32),
            pltpu.SemaphoreType.DMA((2 * y_size * cores,)),
        ],
        compiler_params=pltpu.CompilerParams(vmem_limit_bytes=56 * 1024 * 1024),
        name="channel_mixer",
    )(y_at[None], tokens, whole)
    summed = lowered[0]
    for d in range(1, n_tp):
        summed = summed + shift(lowered[d], "tp", n_tp - d).astype(F32)
    theirs = lax.ppermute(summed[part:].astype(BF16), "sp_1", swap)
    return (hidden_state.astype(F32) + summed[:part] + theirs.astype(F32)).astype(BF16)


def solution(mesh):
    torus = Mesh(mesh.devices.reshape(8, 4, 2, mesh.shape["tp"]), ("sp_0", "sp_1", "sp_2", "tp"))
    return jax.shard_map(
        local,
        mesh=torus,
        in_specs=(
            P(SP, "tp"),
            P(None, SP, "tp"),
            P(SP, "tp"),
            P(SP, "tp"),
            P("tp"),
            P(SP, "tp"),
            P(),
            P("tp", None),
            P(SP, None),
            P(),
            P(SP, "tp"),
            P(SP, "tp"),
            P("tp", SP),
        ),
        out_specs=P(SP_TP, None),
        check_vma=False,
    )
```

profile of v0, /device:TPU:1, one launch (start us, length us, event | category | flops | bytes accessed | tf_op | source)
XLA Modules:
  0.0 154.7 jit_solution(10052029488343718038)
XLA Ops:
  6.5 0.0 all-gather.2.cloned.1.call-start
  6.5 3.4 %local_sweep.1 = (bf16[64,24,128]{2,1,0:T(8,128)(2,1)}, f32[128,512]{1,0:T(8,128)}, bf16[2,128,512]{2,1,0:T(8,128)(2,1)}) custom-call(bf16[128,512]{1,0:T(8,128)(2,1)} %q_ref.1, bf16[2,128,512]{2,1,0:T(8,128)(2,1)} %f_ref.1, bf16[128,512]{1,0:T(8,128)(2,1)} %v_ref.1, f32[1,512]{1,0:T(1,128)} %bitcast.13, f32[4,128]{1,0:T(4,128)} %bitcast.14), custom_call_target="tpu_custom_call" | custom-call | tf_op jit(solution)/shard_map/local_sweep/pallas_call | solution.py:221
  10.0 1.7 %weight_halves.1 = (bf16[32,2304]{1,0:T(8,128)(2,1)}, bf16[32,2304]{1,0:T(8,128)(2,1)}) custom-call(s32[1]{0:T(128)} %bitcast.8.parity_ref, bf16[32,1408]{1,0:T(8,128)(2,1)} %gate_ref.2, bf16[32,1408]{1,0:T(8,128)(2,1)} %up_ref, bf16[32,1408]{1,0:T(8,128)(2,1)} %bitcast.12), custom_call_target="tpu_custom_call" | custom-call | tf_op jit(solution)/shard_map/weight_halves/pallas_call | solution.py:235
  11.7 3.5 %collective-permute-start.9 = (bf16[32,2304]{1,0:T(8,128)(2,1)}, bf16[32,2304]{1,0:T(8,128)(2,1)S(1)}, u32[]{:S(2)}, u32[]{:S(2)}) collective-permute-start(bf16[32,2304]{1,0:T(8,128)(2,1)} %get-tuple-element.34), channel_id=1, source_target_pairs={{0,24},{8,0},{16,8},{24,16},{1,25},{9,1},{17,9},{25,17},{2,26},{10... | collective-permute-start | bytes 442376 | tf_op jit(solution)/shard_map/ppermute | solution.py:189
  15.2 0.4 collective-permute-start.8
  15.6 0.7 collective-permute-start.7
  16.3 3.5 %collective-permute-done.9 = bf16[32,2304]{1,0:T(8,128)(2,1)S(1)} collective-permute-done((bf16[32,2304]{1,0:T(8,128)(2,1)}, bf16[32,2304]{1,0:T(8,128)(2,1)S(1)}, u32[]{:S(2)}, u32[]{:S(2)}) %collective-permute-start.9) | collective-permute-done | bytes 147488 | tf_op jit(solution)/shard_map/ppermute | solution.py:189
  19.8 1.6 %collective-permute-done.8 = bf16[32,2304]{1,0:T(8,128)(2,1)S(1)} collective-permute-done((bf16[32,2304]{1,0:T(8,128)(2,1)}, bf16[32,2304]{1,0:T(8,128)(2,1)S(1)}, u32[]{:S(2)}, u32[]{:S(2)}) %collective-permute-start.8) | collective-permute-done | bytes 147488 | tf_op jit(solution)/shard_map/ppermute | solution.py:189
  21.4 4.5 %collective-permute-done.7 = bf16[32,2304]{1,0:T(8,128)(2,1)S(1)} collective-permute-done((bf16[32,2304]{1,0:T(8,128)(2,1)}, bf16[32,2304]{1,0:T(8,128)(2,1)S(1)}, u32[]{:S(2)}, u32[]{:S(2)}) %collective-permute-start.7) | collective-permute-done | bytes 147488 | tf_op jit(solution)/shard_map/ppermute | solution.py:189
  25.9 1.8 %pad_maximum_fusion = bf16[128,2304]{1,0:T(8,128)(2,1)} fusion(bf16[32,2304]{1,0:T(8,128)(2,1)S(1)} %collective-permute-done.9, bf16[32,2304]{1,0:T(8,128)(2,1)S(1)} %collective-permute-done.8, bf16[32,2304]{1,0:T(8,128)(2,1)S(1)} %collective-permute-done.7, bf16[32,2304]{1,0:T(8,128)(2,1)} %get-tuple-element.33), kind=kLoop, calls=%fused_computation | loop fusion | flops 2359296 | bytes 1179648 | tf_op jit(solution)/shard_map/concatenate | solution.py:244
  27.7 0.0 all-gather.2.cloned.1.call-update
  27.7 9.6 %all-to-all-start = ((bf16[64,24,128]{2,1,0:T(8,128)(2,1)}), bf16[64,24,128]{2,1,0:T(8,128)(2,1)S(1)}, u32[]{:S(2)}, u32[]{:S(2)}) async-start(bf16[64,24,128]{2,1,0:T(8,128)(2,1)} %get-tuple-element.25), calls=%async_computation | async-start | bytes 786432 | tf_op jit(solution)/shard_map/all_to_all | solution.py:234
  37.3 18.1 %all-to-all-done.got_ref = bf16[64,24,128]{2,1,0:T(8,128)(2,1)S(1)} async-done(((bf16[64,24,128]{2,1,0:T(8,128)(2,1)}), bf16[64,24,128]{2,1,0:T(8,128)(2,1)S(1)}, u32[]{:S(2)}, u32[]{:S(2)}) %all-to-all-start) | async-done | bytes 393248 | tf_op jit(solution)/shard_map/all_to_all | solution.py:234
  55.4 0.0 copy-start
  55.4 0.7 copy-done
  56.1 1.8 %block_scan.1 = bf16[64,16,128]{2,1,0:T(8,128)(2,1)} custom-call(s32[1]{0:T(128)} %bitcast.3.back_ref, bf16[64,24,128]{2,1,0:T(8,128)(2,1)} %copy-done), custom_call_target="tpu_custom_call" | custom-call | tf_op jit(solution)/shard_map/block_scan/pallas_call | solution.py:246
  58.0 5.7 %all-to-all-start.1 = ((bf16[64,16,128]{2,1,0:T(8,128)(2,1)}), bf16[64,16,128]{2,1,0:T(8,128)(2,1)S(1)}, u32[]{:S(2)}, u32[]{:S(2)}) async-start(bf16[64,16,128]{2,1,0:T(8,128)(2,1)} %block_scan.1), calls=%async_computation.1 | async-start | bytes 524288 | tf_op jit(solution)/shard_map/all_to_all | solution.py:253
  63.7 15.4 %all-to-all-done.1 = bf16[64,16,128]{2,1,0:T(8,128)(2,1)S(1)} async-done(((bf16[64,16,128]{2,1,0:T(8,128)(2,1)}), bf16[64,16,128]{2,1,0:T(8,128)(2,1)S(1)}, u32[]{:S(2)}, u32[]{:S(2)}) %all-to-all-start.1) | async-done | bytes 262176 | tf_op jit(solution)/shard_map/all_to_all | solution.py:253
  79.1 0.0 copy-start.2
  79.1 0.7 copy-done.2
  79.8 0.0 copy-start.3
  79.8 4.5 %norm_project.1 = (bf16[32,2048]{1,0:T(8,128)(2,1)}, bf16[32,2048]{1,0:T(8,128)(2,1)}, bf16[32,2048]{1,0:T(8,128)(2,1)}, bf16[32,2048]{1,0:T(8,128)(2,1)}) custom-call(s32[1]{0:T(128)} %bitcast.own_ref, f32[128,512]{1,0:T(8,128)} %get-tuple-element.22.near_ref, bf16[2,128,512]{2,1,0:T(8,128)(2,1)} %get-tuple-element.23.reach_ref, ...), custom_call_target="tpu_custom_call" | custom-call | tf_op jit(solution)/shard_map/norm_project/pallas_call | solution.py:256
  84.3 2.5 %collective-permute-start.2 = (bf16[32,2048]{1,0:T(8,128)(2,1)}, bf16[32,2048]{1,0:T(8,128)(2,1)S(1)}, u32[]{:S(2)}, u32[]{:S(2)}) collective-permute-start(bf16[32,2048]{1,0:T(8,128)(2,1)} %get-tuple-element.29), channel_id=1, source_target_pairs={{0,3},{1,0},{2,1},{3,2},{4,7},{5,4},{6,5},{7,6},{8,11},{9,8},{10,9... | collective-permute-start | bytes 393224 | tf_op jit(solution)/shard_map/ppermute | solution.py:189
  86.8 0.5 collective-permute-start.1
  87.3 0.6 collective-permute-start
  87.9 0.0 copy-done.3
  87.9 4.4 %collective-permute-done.2 = bf16[32,2048]{1,0:T(8,128)(2,1)S(1)} collective-permute-done((bf16[32,2048]{1,0:T(8,128)(2,1)}, bf16[32,2048]{1,0:T(8,128)(2,1)S(1)}, u32[]{:S(2)}, u32[]{:S(2)}) %collective-permute-start.2) | collective-permute-done | bytes 131104 | tf_op jit(solution)/shard_map/ppermute | solution.py:189
  92.3 0.7 collective-permute-done.1
  93.0 3.8 %collective-permute-done = bf16[32,2048]{1,0:T(8,128)(2,1)S(1)} collective-permute-done((bf16[32,2048]{1,0:T(8,128)(2,1)}, bf16[32,2048]{1,0:T(8,128)(2,1)S(1)}, u32[]{:S(2)}, u32[]{:S(2)}) %collective-permute-start) | collective-permute-done | bytes 131104 | tf_op jit(solution)/shard_map/ppermute | solution.py:189
  96.8 1.2 fusion
  98.0 0.1 constant_dynamic-update-slice_fusion.4
  98.1 1.2 collective-permute-start.3
  99.4 3.5 %collective-permute-done.3 = bf16[32,2048]{1,0:T(8,128)(2,1)S(1)} collective-permute-done((bf16[32,2048]{1,0:T(8,128)(2,1)S(1)}, bf16[32,2048]{1,0:T(8,128)(2,1)S(1)}, u32[]{:S(2)}, u32[]{:S(2)}) %collective-permute-start.3) | collective-permute-done | bytes 131104 | tf_op jit(solution)/shard_map/ppermute | solution.py:278
  102.9 0.1 collective-permute-start.4
  103.0 0.3 collective-permute-start.5
  103.3 2.3 %collective-permute-start.6 = (bf16[64,2048]{1,0:T(8,128)(2,1)S(1)}, bf16[64,2048]{1,0:T(8,128)(2,1)S(1)}, u32[]{:S(2)}, u32[]{:S(2)}) collective-permute-start(bf16[64,2048]{1,0:T(8,128)(2,1)S(1)} %pad_maximum_fusion.1), channel_id=1, source_target_pairs={{0,3},{1,0},{2,1},{3,2},{4,7},{5,4},{6,5},{7,6},{8,11},{9,8},{10,9... | collective-permute-start | bytes 786440 | tf_op jit(solution)/shard_map/ppermute | solution.py:189
  105.7 11.2 %collective-permute-done.4 = bf16[64,2048]{1,0:T(8,128)(2,1)S(1)} collective-permute-done((bf16[64,2048]{1,0:T(8,128)(2,1)S(1)}, bf16[64,2048]{1,0:T(8,128)(2,1)S(1)}, u32[]{:S(2)}, u32[]{:S(2)}) %collective-permute-start.4) | collective-permute-done | bytes 262176 | tf_op jit(solution)/shard_map/ppermute | solution.py:189
  116.9 0.0 collective-permute-done.5
  116.9 0.1 collective-permute-done.6
  117.0 0.0 copy-start.1
  117.0 0.0 all-gather.2.cloned.1.call-done
  117.1 1.0 copy-done.1
  118.0 7.9 %channel_mixer.1 = (f32[64,2048]{1,0:T(8,128)}, bf16[64,2048]{1,0:T(8,128)(2,1)}, bf16[64,2048]{1,0:T(8,128)(2,1)}, bf16[64,2048]{1,0:T(8,128)(2,1)}) custom-call(s32[1]{0:T(128)} %bitcast.7.refs_0_, bf16[256,2048]{1,0:T(8,128)(2,1)} %copy-done.1, bf16[8,2,4,32,2304]{4,3,2,1,0:T(8,128)(2,1)} %bitcast.10), custom_call_target="tpu_custom_call" | custom-call | tf_op jit(solution)/shard_map/channel_mixer/pallas_call | solution.py:280
  125.9 1.7 %collective-permute-start.12 = (bf16[64,2048]{1,0:T(8,128)(2,1)}, bf16[64,2048]{1,0:T(8,128)(2,1)S(1)}, u32[]{:S(2)}, u32[]{:S(2)}) collective-permute-start(bf16[64,2048]{1,0:T(8,128)(2,1)} %get-tuple-element.38), channel_id=1, source_target_pairs={{0,1},{1,2},{2,3},{3,0},{4,5},{5,6},{6,7},{7,4},{8,9},{9,10},{10,1... | collective-permute-start | bytes 786440 | tf_op jit(solution)/shard_map/ppermute | solution.py:189
  127.6 3.0 %collective-permute-start.11 = (bf16[64,2048]{1,0:T(8,128)(2,1)}, bf16[64,2048]{1,0:T(8,128)(2,1)S(1)}, u32[]{:S(2)}, u32[]{:S(2)}) collective-permute-start(bf16[64,2048]{1,0:T(8,128)(2,1)} %get-tuple-element.37), channel_id=1, source_target_pairs={{0,2},{1,3},{2,0},{3,1},{4,6},{5,7},{6,4},{7,5},{8,10},{9,11},{10,... | collective-permute-start | bytes 786440 | tf_op jit(solution)/shard_map/ppermute | solution.py:189
  130.6 0.0 collective-permute-start.10
  130.6 4.0 %collective-permute-done.12 = bf16[64,2048]{1,0:T(8,128)(2,1)S(1)} collective-permute-done((bf16[64,2048]{1,0:T(8,128)(2,1)}, bf16[64,2048]{1,0:T(8,128)(2,1)S(1)}, u32[]{:S(2)}, u32[]{:S(2)}) %collective-permute-start.12) | collective-permute-done | bytes 262176 | tf_op jit(solution)/shard_map/ppermute | solution.py:189
  134.6 7.4 %collective-permute-done.11 = bf16[64,2048]{1,0:T(8,128)(2,1)S(1)} collective-permute-done((bf16[64,2048]{1,0:T(8,128)(2,1)}, bf16[64,2048]{1,0:T(8,128)(2,1)S(1)}, u32[]{:S(2)}, u32[]{:S(2)}) %collective-permute-start.11) | collective-permute-done | bytes 262176 | tf_op jit(solution)/shard_map/ppermute | solution.py:189
  142.0 0.0 collective-permute-done.10
  142.0 1.2 convert_add_fusion
  143.2 1.2 collective-permute-start.13
  144.4 2.7 %collective-permute-done.13 = bf16[32,2048]{1,0:T(8,128)(2,1)S(1)} collective-permute-done((bf16[32,2048]{1,0:T(8,128)(2,1)S(1)}, bf16[32,2048]{1,0:T(8,128)(2,1)S(1)}, u32[]{:S(2)}, u32[]{:S(2)}) %collective-permute-start.13) | collective-permute-done | bytes 131104 | tf_op jit(solution)/shard_map/ppermute | solution.py:297
  147.1 0.7 fusion.4
  (8 shorter events, 0.1 us)
Async XLA Ops:
  6.5 110.5 %all-gather.2.cloned.1.call-start = ((), (), s32[]{:S(2)}) async-start(), calls=%async_computation.2 | async-start | bytes 10027008 | tf_op jit(solution)/shard_map/all_gather | solution.py:243
  11.7 8.1 %collective-permute-start.9 = (bf16[32,2304]{1,0:T(8,128)(2,1)}, bf16[32,2304]{1,0:T(8,128)(2,1)S(1)}, u32[]{:S(2)}, u32[]{:S(2)}) collective-permute-start(bf16[32,2304]{1,0:T(8,128)(2,1)} %get-tuple-element.34), channel_id=1, source_target_pairs={{0,24},{8,0},{16,8},{24,16},{1,25},{9,1},{17,9},{25,17},{2,26},{10... | collective-permute-start | bytes 442376 | tf_op jit(solution)/shard_map/ppermute | solution.py:189
  15.2 6.2 %collective-permute-start.8 = (bf16[32,2304]{1,0:T(8,128)(2,1)}, bf16[32,2304]{1,0:T(8,128)(2,1)S(1)}, u32[]{:S(2)}, u32[]{:S(2)}) collective-permute-start(bf16[32,2304]{1,0:T(8,128)(2,1)} %get-tuple-element.33), channel_id=1, source_target_pairs={{0,16},{8,24},{16,0},{24,8},{1,17},{9,25},{17,1},{25,9},{2,18},{10... | collective-permute-start | bytes 442376 | tf_op jit(solution)/shard_map/ppermute | solution.py:189
  15.6 10.3 %collective-permute-start.7 = (bf16[32,2304]{1,0:T(8,128)(2,1)}, bf16[32,2304]{1,0:T(8,128)(2,1)S(1)}, u32[]{:S(2)}, u32[]{:S(2)}) collective-permute-start(bf16[32,2304]{1,0:T(8,128)(2,1)} %get-tuple-element.34), channel_id=1, source_target_pairs={{0,8},{8,16},{16,24},{24,0},{1,9},{9,17},{17,25},{25,1},{2,10},{10... | collective-permute-start | bytes 442376 | tf_op jit(solution)/shard_map/ppermute | solution.py:189
  27.7 27.7 %all-to-all-start = ((bf16[64,24,128]{2,1,0:T(8,128)(2,1)}), bf16[64,24,128]{2,1,0:T(8,128)(2,1)S(1)}, u32[]{:S(2)}, u32[]{:S(2)}) async-start(bf16[64,24,128]{2,1,0:T(8,128)(2,1)} %get-tuple-element.25), calls=%async_computation | async-start | bytes 786432 | tf_op jit(solution)/shard_map/all_to_all | solution.py:234
  55.4 0.7 copy-start
  58.0 21.1 %all-to-all-start.1 = ((bf16[64,16,128]{2,1,0:T(8,128)(2,1)}), bf16[64,16,128]{2,1,0:T(8,128)(2,1)S(1)}, u32[]{:S(2)}, u32[]{:S(2)}) async-start(bf16[64,16,128]{2,1,0:T(8,128)(2,1)} %block_scan.1), calls=%async_computation.1 | async-start | bytes 524288 | tf_op jit(solution)/shard_map/all_to_all | solution.py:253
  79.1 0.7 copy-start.2
  79.8 8.1 %copy-start.3 = (bf16[2048]{0:T(1024)(128)(2,1)S(1)}, bf16[2048]{0:T(1024)(128)(2,1)}, u32[]{:S(2)}) copy-start(bf16[2048]{0:T(1024)(128)(2,1)} %param.22) | copy-start | bytes 12292
  84.3 8.0 %collective-permute-start.2 = (bf16[32,2048]{1,0:T(8,128)(2,1)}, bf16[32,2048]{1,0:T(8,128)(2,1)S(1)}, u32[]{:S(2)}, u32[]{:S(2)}) collective-permute-start(bf16[32,2048]{1,0:T(8,128)(2,1)} %get-tuple-element.29), channel_id=1, source_target_pairs={{0,3},{1,0},{2,1},{3,2},{4,7},{5,4},{6,5},{7,6},{8,11},{9,8},{10,9... | collective-permute-start | bytes 393224 | tf_op jit(solution)/shard_map/ppermute | solution.py:189
  86.8 6.2 %collective-permute-start.1 = (bf16[32,2048]{1,0:T(8,128)(2,1)}, bf16[32,2048]{1,0:T(8,128)(2,1)S(1)}, u32[]{:S(2)}, u32[]{:S(2)}) collective-permute-start(bf16[32,2048]{1,0:T(8,128)(2,1)} %get-tuple-element.28), channel_id=1, source_target_pairs={{0,2},{1,3},{2,0},{3,1},{4,6},{5,7},{6,4},{7,5},{8,10},{9,11},{10,... | collective-permute-start | bytes 393224 | tf_op jit(solution)/shard_map/ppermute | solution.py:189
  87.3 9.5 %collective-permute-start = (bf16[32,2048]{1,0:T(8,128)(2,1)}, bf16[32,2048]{1,0:T(8,128)(2,1)S(1)}, u32[]{:S(2)}, u32[]{:S(2)}) collective-permute-start(bf16[32,2048]{1,0:T(8,128)(2,1)} %get-tuple-element.27), channel_id=1, source_target_pairs={{0,1},{1,2},{2,3},{3,0},{4,5},{5,6},{6,7},{7,4},{8,9},{9,10},{10,1... | collective-permute-start | bytes 393224 | tf_op jit(solution)/shard_map/ppermute | solution.py:189
  98.1 4.7 %collective-permute-start.3 = (bf16[32,2048]{1,0:T(8,128)(2,1)S(1)}, bf16[32,2048]{1,0:T(8,128)(2,1)S(1)}, u32[]{:S(2)}, u32[]{:S(2)}) collective-permute-start(bf16[32,2048]{1,0:T(8,128)(2,1)S(1)} %get-tuple-element.40), channel_id=1, source_target_pairs={{0,8},{8,0},{16,24},{24,16},{1,9},{9,1},{17,25},{25,17},{2,10},{10... | collective-permute-start | bytes 393224 | tf_op jit(solution)/shard_map/ppermute | solution.py:278
  102.9 14.0 %collective-permute-start.4 = (bf16[64,2048]{1,0:T(8,128)(2,1)S(1)}, bf16[64,2048]{1,0:T(8,128)(2,1)S(1)}, u32[]{:S(2)}, u32[]{:S(2)}) collective-permute-start(bf16[64,2048]{1,0:T(8,128)(2,1)S(1)} %pad_maximum_fusion.1), channel_id=1, source_target_pairs={{0,1},{1,2},{2,3},{3,0},{4,5},{5,6},{6,7},{7,4},{8,9},{9,10},{10,1... | collective-permute-start | bytes 786440 | tf_op jit(solution)/shard_map/ppermute | solution.py:189
  103.0 13.9 %collective-permute-start.5 = (bf16[64,2048]{1,0:T(8,128)(2,1)S(1)}, bf16[64,2048]{1,0:T(8,128)(2,1)S(1)}, u32[]{:S(2)}, u32[]{:S(2)}) collective-permute-start(bf16[64,2048]{1,0:T(8,128)(2,1)S(1)} %pad_maximum_fusion.1), channel_id=1, source_target_pairs={{0,2},{1,3},{2,0},{3,1},{4,6},{5,7},{6,4},{7,5},{8,10},{9,11},{10,... | collective-permute-start | bytes 786440 | tf_op jit(solution)/shard_map/ppermute | solution.py:189
  103.3 13.7 %collective-permute-start.6 = (bf16[64,2048]{1,0:T(8,128)(2,1)S(1)}, bf16[64,2048]{1,0:T(8,128)(2,1)S(1)}, u32[]{:S(2)}, u32[]{:S(2)}) collective-permute-start(bf16[64,2048]{1,0:T(8,128)(2,1)S(1)} %pad_maximum_fusion.1), channel_id=1, source_target_pairs={{0,3},{1,0},{2,1},{3,2},{4,7},{5,4},{6,5},{7,6},{8,11},{9,8},{10,9... | collective-permute-start | bytes 786440 | tf_op jit(solution)/shard_map/ppermute | solution.py:189
  117.0 1.0 copy-start.1
  125.9 8.7 %collective-permute-start.12 = (bf16[64,2048]{1,0:T(8,128)(2,1)}, bf16[64,2048]{1,0:T(8,128)(2,1)S(1)}, u32[]{:S(2)}, u32[]{:S(2)}) collective-permute-start(bf16[64,2048]{1,0:T(8,128)(2,1)} %get-tuple-element.38), channel_id=1, source_target_pairs={{0,1},{1,2},{2,3},{3,0},{4,5},{5,6},{6,7},{7,4},{8,9},{9,10},{10,1... | collective-permute-start | bytes 786440 | tf_op jit(solution)/shard_map/ppermute | solution.py:189
  127.6 14.4 %collective-permute-start.11 = (bf16[64,2048]{1,0:T(8,128)(2,1)}, bf16[64,2048]{1,0:T(8,128)(2,1)S(1)}, u32[]{:S(2)}, u32[]{:S(2)}) collective-permute-start(bf16[64,2048]{1,0:T(8,128)(2,1)} %get-tuple-element.37), channel_id=1, source_target_pairs={{0,2},{1,3},{2,0},{3,1},{4,6},{5,7},{6,4},{7,5},{8,10},{9,11},{10,... | collective-permute-start | bytes 786440 | tf_op jit(solution)/shard_map/ppermute | solution.py:189
  130.6 11.4 %collective-permute-start.10 = (bf16[64,2048]{1,0:T(8,128)(2,1)}, bf16[64,2048]{1,0:T(8,128)(2,1)S(1)}, u32[]{:S(2)}, u32[]{:S(2)}) collective-permute-start(bf16[64,2048]{1,0:T(8,128)(2,1)} %get-tuple-element.36), channel_id=1, source_target_pairs={{0,3},{1,0},{2,1},{3,2},{4,7},{5,4},{6,5},{7,6},{8,11},{9,8},{10,9... | collective-permute-start | bytes 786440 | tf_op jit(solution)/shard_map/ppermute | solution.py:189
  143.2 3.9 %collective-permute-start.13 = (bf16[32,2048]{1,0:T(8,128)(2,1)S(1)}, bf16[32,2048]{1,0:T(8,128)(2,1)S(1)}, u32[]{:S(2)}, u32[]{:S(2)}) collective-permute-start(bf16[32,2048]{1,0:T(8,128)(2,1)S(1)} %slice.13), channel_id=1, source_target_pairs={{0,8},{8,0},{16,24},{24,16},{1,9},{9,1},{17,25},{25,17},{2,10},{10... | collective-permute-start | bytes 393224 | tf_op jit(solution)/shard_map/ppermute | solution.py:297
Sparse Core Ops, SparseCore 0:
  27.8 73.4 all-gather.1
where the time goes:
time: 156 us; the launch traced here: 155 us
  waiting for transfers between devices  81 us (52%)
  starting transfers between devices  33.4 us (21%)
  Pallas kernels  19.3 us (12%)
  between operations  13.5 us (9%)
  other arithmetic  4.94 us (3%)
  local copies, waits for them, and re-layouts  2.52 us (2%)
    ppermute x12, waiting for transfers between devices, shift(): lax.ppermute(array, axis, [(k, (k + by) % size) for k in range(size)])  41.2 us
    all_to_all x1, waiting for transfers between devices, local(): got = lax.all_to_all(send, SP, 0, 0, tiled=True)  18.1 us
    ppermute x12, starting transfers between devices, shift(): lax.ppermute(array, axis, [(k, (k + by) % size) for k in range(size)])  15.6 us
    all_to_all x1, waiting for transfers between devices, local(): lax.all_to_all(give, SP, 0, 0, tiled=True).reshape(2 * heads, HEAD, HEAD)  15.4 us
    all_to_all x1, starting transfers between devices, local(): got = lax.all_to_all(send, SP, 0, 0, tiled=True)  9.59 us
    pallas_call x1, Pallas kernels, local(): pl.pallas_call(lambda *refs: mixer_body(*refs, hidden=hidden), out_shape=...  7.85 us
    all_to_all x1, starting transfers between devices, local(): lax.all_to_all(give, SP, 0, 0, tiled=True).reshape(2 * heads, HEAD, HEAD)  5.71 us
    pallas_call x1, Pallas kernels, local(): pl.pallas_call(project_body, out_shape=(jax.ShapeDtypeStruct((part, model...  4.49 us
  transfers between devices with their start and end apart: 17, of which 14 were waited for; matrix products, arithmetic and copies ran while one was open for 1% of the time, Pallas kernels for 4%

commit v1 on v0

--- a/solution.py
+++ b/solution.py
@@ -107,11 +107,16 @@
     outs = (o0, o1, o2, o3)
     part = o0.shape[0]
     own = own_ref[0]
-    for d in range(len(outs)):
-        at = pl.multiple_of(lax.rem(own + d, len(outs)) * part, part)
-        outs[d][...] = jnp.dot(
-            mixed_ref[pl.ds(at, part), :], weight_ref[...], preferred_element_type=F32
-        ).astype(BF16)
+    turned = jnp.concatenate(
+        [
+            mixed_ref[pl.ds(pl.multiple_of(lax.rem(own + d, len(outs)) * part, part), part), :]
+            for d in range(len(outs))
+        ],
+        axis=0,
+    )
+    lowered = jnp.dot(turned, weight_ref[...], preferred_element_type=F32).astype(BF16)
+    for d, out_ref in enumerate(outs):
+        out_ref[...] = lowered[d * part : (d + 1) * part]
 
 
 def halves_body(parity_ref, gate_ref, up_ref, down_ref, keep_ref, give_ref):
@@ -133,7 +138,9 @@
         write(give_ref, 0)
 
 
-def mixer_body(at_ref, tokens_ref, whole_ref, o0, o1, o2, o3, weights_ref, act_ref, sems, *, hidden):
+def mixer_body(at_ref, *refs, hidden):
+    rows_in, whole_ref, outs = refs[:8], refs[8], refs[9:17]
+    tokens_ref, weights_ref, act_ref, sems = refs[17:]
     z_size, y_size, cores, _, wide = weights_ref.shape
     model = tokens_ref.shape[1]
     y = at_ref[0]
@@ -158,6 +165,9 @@
     for group in groups:
         for copy in group:
             copy.start()
+    part = outs[0].shape[0]
+    for n, ref in enumerate(rows_in):
+        tokens_ref[n * part : (n + 1) * part, :] = ref[...]
     weights = weights_ref.reshape(model, wide)
     for n, group in enumerate(groups):
         for copy in group:
@@ -174,8 +184,7 @@
     low = jnp.where(lax.rem(y, 2) == 0, 0, width - hidden // 2)
     inner = jnp.where((lane >= low) & (lane < low + hidden // 2), inner, 0.0).astype(BF16)
     lowered = nt_dot(inner, weights[:, 2 * width :])
-    part = o0.shape[0]
-    for d, out_ref in enumerate((o0, o1, o2, o3)):
+    for d, out_ref in enumerate(outs):
         out_ref[...] = lowered[d * part : (d + 1) * part].astype(out_ref.dtype)
 
 
@@ -275,27 +284,30 @@
         * mixer_norm_gain.astype(F32)
     ).astype(BF16)
     swap = [(k, k ^ 1) for k in range(y_size)]
-    both = jnp.concatenate([normed, lax.ppermute(normed, "sp_1", swap)], axis=0)
-    tokens = jnp.concatenate([both] + [shift(both, "tp", d) for d in range(1, n_tp)], axis=0)
+    theirs = lax.ppermute(normed, "sp_1", swap)
+    tokens = [normed] + [shift(normed, "tp", d) for d in range(1, n_tp)]
+    tokens += [theirs] + [shift(theirs, "tp", d) for d in range(1, n_tp)]
+    kept = (jax.ShapeDtypeStruct((part, model), F32),)
+    sent = (jax.ShapeDtypeStruct((part, model), BF16),) * (n_tp - 1)
     lowered = pl.pallas_call(
         lambda *refs: mixer_body(*refs, hidden=hidden),
-        out_shape=(jax.ShapeDtypeStruct((2 * part, model), F32),)
-        + (jax.ShapeDtypeStruct((2 * part, model), BF16),) * (n_tp - 1),
-        in_specs=[SMEM, VMEM, ANY],
-        out_specs=(VMEM,) * n_tp,
+        out_shape=(kept + sent) * 2,
+        in_specs=[SMEM] + [VMEM] * (2 * n_tp) + [ANY],
+        out_specs=(VMEM,) * (2 * n_tp),
         scratch_shapes=[
+            pltpu.VMEM((2 * rows, model), BF16),
             pltpu.VMEM((z_size, y_size, cores, slab, 3 * half), BF16),
             pltpu.VMEM((2 * rows, 2 * half), F32),
             pltpu.SemaphoreType.DMA((2 * y_size * cores,)),
         ],
-        compiler_params=pltpu.CompilerParams(vmem_limit_bytes=56 * 1024 * 1024),
+        compiler_params=pltpu.CompilerParams(vmem_limit_bytes=54 * 1024 * 1024),
         name="channel_mixer",
-    )(y_at[None], tokens, whole)
-    summed = lowered[0]
-    for d in range(1, n_tp):
-        summed = summed + shift(lowered[d], "tp", n_tp - d).astype(F32)
-    theirs = lax.ppermute(summed[part:].astype(BF16), "sp_1", swap)
-    return (hidden_state.astype(F32) + summed[:part] + theirs.astype(F32)).astype(BF16)
+    )(y_at[None], *tokens, whole)
+    mine, other = lowered[:n_tp], lowered[n_tp:]
+    other = [other[0]] + [shift(other[d], "tp", n_tp - d) for d in range(1, n_tp)]
+    mine = [mine[0]] + [shift(mine[d], "tp", n_tp - d) for d in range(1, n_tp)]
+    theirs = lax.ppermute(sum(a.astype(F32) for a in other).astype(BF16), "sp_1", swap)
+    return (sum((a.astype(F32) for a in mine), hidden_state.astype(F32)) + theirs.astype(F32)).astype(BF16)
 
 
 def solution(mesh):

time: 156 us -> 147 us (0.942)
  the two profiles are of different devices: /device:TPU:1 before, /device:TPU:16 now
where the time goes in v1:
time: 147 us; the launch traced here: 146 us
  waiting for transfers between devices  62.1 us (42%)
  starting transfers between devices  44.4 us (30%)
  Pallas kernels  18.5 us (13%)
  between operations  13.5 us (9%)
  other arithmetic  5.8 us (4%)
  local copies, waits for them, and re-layouts  2.09 us (1%)
    ppermute x18, waiting for transfers between devices, shift(): lax.ppermute(array, axis, [(k, (k + by) % size) for k in range(size)])  25.4 us
    ppermute x18, starting transfers between devices, shift(): lax.ppermute(array, axis, [(k, (k + by) % size) for k in range(size)])  25.2 us
    all_to_all x1, waiting for transfers between devices, local(): got = lax.all_to_all(send, SP, 0, 0, tiled=True)  18.1 us
    all_to_all x1, waiting for transfers between devices, local(): lax.all_to_all(give, SP, 0, 0, tiled=True).reshape(2 * heads, HEAD, HEAD)  15.1 us
    all_to_all x1, starting transfers between devices, local(): got = lax.all_to_all(send, SP, 0, 0, tiled=True)  12 us
    pallas_call x1, Pallas kernels, local(): pl.pallas_call(lambda *refs: mixer_body(*refs, hidden=hidden), out_shape=...  7.9 us
    all_to_all x1, starting transfers between devices, local(): lax.all_to_all(give, SP, 0, 0, tiled=True).reshape(2 * heads, HEAD, HEAD)  5.61 us
    pallas_call x1, Pallas kernels, local(): pl.pallas_call(project_body, out_shape=(jax.ShapeDtypeStruct((part, model...  3.54 us
  transfers between devices with their start and end apart: 23, of which 17 were waited for; matrix products, arithmetic and copies ran while one was open for 2% of the time, Pallas kernels for 4%

profile of v1, /device:TPU:16, one launch (start us, length us, event | category | flops | bytes accessed | tf_op | source)
XLA Modules:
  0.0 146.3 jit_solution(9335966319019285972)
XLA Ops:
  6.5 0.0 all-gather.2.cloned.1.call-start
  6.5 3.4 %local_sweep.1 = (bf16[64,24,128]{2,1,0:T(8,128)(2,1)}, f32[128,512]{1,0:T(8,128)}, bf16[2,128,512]{2,1,0:T(8,128)(2,1)}) custom-call(bf16[128,512]{1,0:T(8,128)(2,1)} %q_ref.1, bf16[2,128,512]{2,1,0:T(8,128)(2,1)} %f_ref.1, bf16[128,512]{1,0:T(8,128)(2,1)} %v_ref.1, f32[1,512]{1,0:T(1,128)} %bitcast.13, f32[4,128]{1,0:T(4,128)} %bitcast.14), custom_call_target="tpu_custom_call" | custom-call | tf_op jit(solution)/shard_map/local_sweep/pallas_call | solution.py:230
  10.0 1.7 %weight_halves.1 = (bf16[32,2304]{1,0:T(8,128)(2,1)}, bf16[32,2304]{1,0:T(8,128)(2,1)}) custom-call(s32[1]{0:T(128)} %bitcast.8.parity_ref, bf16[32,1408]{1,0:T(8,128)(2,1)} %gate_ref.2, bf16[32,1408]{1,0:T(8,128)(2,1)} %up_ref, bf16[32,1408]{1,0:T(8,128)(2,1)} %bitcast.12), custom_call_target="tpu_custom_call" | custom-call | tf_op jit(solution)/shard_map/weight_halves/pallas_call | solution.py:244
  11.7 2.0 %collective-permute-start.11 = (bf16[32,2304]{1,0:T(8,128)(2,1)}, bf16[32,2304]{1,0:T(8,128)(2,1)S(1)}, u32[]{:S(2)}, u32[]{:S(2)}) collective-permute-start(bf16[32,2304]{1,0:T(8,128)(2,1)} %get-tuple-element.37), channel_id=1, source_target_pairs={{0,16},{8,24},{16,0},{24,8},{1,17},{9,25},{17,1},{25,9},{2,18},{10... | collective-permute-start | bytes 442376 | tf_op jit(solution)/shard_map/ppermute | solution.py:198
  13.7 0.7 collective-permute-start.12
  14.4 1.3 collective-permute-start.10
  15.7 4.4 %collective-permute-done.11 = bf16[32,2304]{1,0:T(8,128)(2,1)S(1)} collective-permute-done((bf16[32,2304]{1,0:T(8,128)(2,1)}, bf16[32,2304]{1,0:T(8,128)(2,1)S(1)}, u32[]{:S(2)}, u32[]{:S(2)}) %collective-permute-start.11) | collective-permute-done | bytes 147488 | tf_op jit(solution)/shard_map/ppermute | solution.py:198
  20.1 1.0 collective-permute-done.12
  21.1 1.0 collective-permute-done.10
  22.1 1.8 %pad_maximum_fusion = bf16[128,2304]{1,0:T(8,128)(2,1)} fusion(bf16[32,2304]{1,0:T(8,128)(2,1)S(1)} %collective-permute-done.12, bf16[32,2304]{1,0:T(8,128)(2,1)S(1)} %collective-permute-done.11, bf16[32,2304]{1,0:T(8,128)(2,1)S(1)} %collective-permute-done.10, bf16[32,2304]{1,0:T(8,128)(2,1)} %get-tuple-element.37), kind=kLoop, calls=%fused_computation | loop fusion | flops 2359296 | bytes 1179648 | tf_op jit(solution)/shard_map/concatenate | solution.py:253
  23.9 0.0 all-gather.2.cloned.1.call-update
  23.9 12.0 %all-to-all-start = ((bf16[64,24,128]{2,1,0:T(8,128)(2,1)}), bf16[64,24,128]{2,1,0:T(8,128)(2,1)S(1)}, u32[]{:S(2)}, u32[]{:S(2)}) async-start(bf16[64,24,128]{2,1,0:T(8,128)(2,1)} %get-tuple-element.29), calls=%async_computation | async-start | bytes 786432 | tf_op jit(solution)/shard_map/all_to_all | solution.py:243
  35.9 18.1 %all-to-all-done.got_ref = bf16[64,24,128]{2,1,0:T(8,128)(2,1)S(1)} async-done(((bf16[64,24,128]{2,1,0:T(8,128)(2,1)}), bf16[64,24,128]{2,1,0:T(8,128)(2,1)S(1)}, u32[]{:S(2)}, u32[]{:S(2)}) %all-to-all-start) | async-done | bytes 393248 | tf_op jit(solution)/shard_map/all_to_all | solution.py:243
  54.1 0.8 copy-done
  54.8 1.9 %block_scan.1 = bf16[64,16,128]{2,1,0:T(8,128)(2,1)} custom-call(s32[1]{0:T(128)} %bitcast.3.back_ref, bf16[64,24,128]{2,1,0:T(8,128)(2,1)} %copy-done), custom_call_target="tpu_custom_call" | custom-call | tf_op jit(solution)/shard_map/block_scan/pallas_call | solution.py:255
  56.8 5.6 %all-to-all-start.1 = ((bf16[64,16,128]{2,1,0:T(8,128)(2,1)}), bf16[64,16,128]{2,1,0:T(8,128)(2,1)S(1)}, u32[]{:S(2)}, u32[]{:S(2)}) async-start(bf16[64,16,128]{2,1,0:T(8,128)(2,1)} %block_scan.1), calls=%async_computation.1 | async-start | bytes 524288 | tf_op jit(solution)/shard_map/all_to_all | solution.py:262
  62.4 15.1 %all-to-all-done.1 = bf16[64,16,128]{2,1,0:T(8,128)(2,1)S(1)} async-done(((bf16[64,16,128]{2,1,0:T(8,128)(2,1)}), bf16[64,16,128]{2,1,0:T(8,128)(2,1)S(1)}, u32[]{:S(2)}, u32[]{:S(2)}) %all-to-all-start.1) | async-done | bytes 262176 | tf_op jit(solution)/shard_map/all_to_all | solution.py:262
  77.4 0.7 copy-done.1
  78.2 3.5 %norm_project.1 = (bf16[32,2048]{1,0:T(8,128)(2,1)}, bf16[32,2048]{1,0:T(8,128)(2,1)}, bf16[32,2048]{1,0:T(8,128)(2,1)}, bf16[32,2048]{1,0:T(8,128)(2,1)}) custom-call(s32[1]{0:T(128)} %bitcast.own_ref, f32[128,512]{1,0:T(8,128)} %get-tuple-element.26.near_ref, bf16[2,128,512]{2,1,0:T(8,128)(2,1)} %get-tuple-element.27.reach_ref, ...), custom_call_target="tpu_custom_call" | custom-call | tf_op jit(solution)/shard_map/norm_project/pallas_call | solution.py:265
  81.7 1.5 %collective-permute-start = (bf16[32,2048]{1,0:T(8,128)(2,1)}, bf16[32,2048]{1,0:T(8,128)(2,1)S(1)}, u32[]{:S(2)}, u32[]{:S(2)}) collective-permute-start(bf16[32,2048]{1,0:T(8,128)(2,1)} %get-tuple-element.31), channel_id=1, source_target_pairs={{0,1},{1,2},{2,3},{3,0},{4,5},{5,6},{6,7},{7,4},{8,9},{9,10},{10,1... | collective-permute-start | bytes 393224 | tf_op jit(solution)/shard_map/ppermute | solution.py:198
  83.2 2.7 %collective-permute-start.1 = (bf16[32,2048]{1,0:T(8,128)(2,1)}, bf16[32,2048]{1,0:T(8,128)(2,1)S(1)}, u32[]{:S(2)}, u32[]{:S(2)}) collective-permute-start(bf16[32,2048]{1,0:T(8,128)(2,1)} %get-tuple-element.32), channel_id=1, source_target_pairs={{0,2},{1,3},{2,0},{3,1},{4,6},{5,7},{6,4},{7,5},{8,10},{9,11},{10,... | collective-permute-start | bytes 393224 | tf_op jit(solution)/shard_map/ppermute | solution.py:198
  85.9 1.4 collective-permute-start.2
  87.4 0.0 copy-done.10
  87.4 1.1 collective-permute-done
  88.5 3.8 %collective-permute-done.1 = bf16[32,2048]{1,0:T(8,128)(2,1)S(1)} collective-permute-done((bf16[32,2048]{1,0:T(8,128)(2,1)}, bf16[32,2048]{1,0:T(8,128)(2,1)S(1)}, u32[]{:S(2)}, u32[]{:S(2)}) %collective-permute-start.1) | collective-permute-done | bytes 131104 | tf_op jit(solution)/shard_map/ppermute | solution.py:198
  92.3 0.0 collective-permute-done.2
  92.3 1.2 fusion
  93.5 0.1 fusion.2.refs_1_
  93.6 0.0 copy-start.2
  93.6 0.8 collective-permute-start.6
  94.4 2.7 %collective-permute-start.5 = (bf16[32,2048]{1,0:T(8,128)(2,1)S(1)}, bf16[32,2048]{1,0:T(8,128)(2,1)S(1)}, u32[]{:S(2)}, u32[]{:S(2)}) collective-permute-start(bf16[32,2048]{1,0:T(8,128)(2,1)S(1)} %fusion.2.refs_1_), channel_id=1, source_target_pairs={{0,3},{1,0},{2,1},{3,2},{4,7},{5,4},{6,5},{7,6},{8,11},{9,8},{10,9... | collective-permute-start | bytes 393224 | tf_op jit(solution)/shard_map/ppermute | solution.py:198
  97.0 0.8 collective-permute-start.4
  97.8 0.7 collective-permute-start.3
  98.5 0.2 collective-permute-done.6.refs_5_
  98.7 2.4 %collective-permute-start.9 = (bf16[32,2048]{1,0:T(8,128)(2,1)S(1)}, bf16[32,2048]{1,0:T(8,128)(2,1)S(1)}, u32[]{:S(2)}, u32[]{:S(2)}) collective-permute-start(bf16[32,2048]{1,0:T(8,128)(2,1)S(1)} %collective-permute-done.6.refs_5_), channel_id=1, source_target_pairs={{0,3},{1,0},{2,1},{3,2},{4,7},{5,4},{6,5},{7,6},{8,11},{9,8},{10,9... | collective-permute-start | bytes 393224 | tf_op jit(solution)/shard_map/ppermute | solution.py:198
  101.0 1.6 %collective-permute-start.8 = (bf16[32,2048]{1,0:T(8,128)(2,1)S(1)}, bf16[32,2048]{1,0:T(8,128)(2,1)S(1)}, u32[]{:S(2)}, u32[]{:S(2)}) collective-permute-start(bf16[32,2048]{1,0:T(8,128)(2,1)S(1)} %collective-permute-done.6.refs_5_), channel_id=1, source_target_pairs={{0,2},{1,3},{2,0},{3,1},{4,6},{5,7},{6,4},{7,5},{8,10},{9,11},{10,... | collective-permute-start | bytes 393224 | tf_op jit(solution)/shard_map/ppermute | solution.py:198
  102.6 0.0 collective-permute-done.5.refs_4_
  102.6 0.1 collective-permute-start.7
  102.7 1.8 %collective-permute-done.4.refs_3_ = bf16[32,2048]{1,0:T(8,128)(2,1)S(1)} collective-permute-done((bf16[32,2048]{1,0:T(8,128)(2,1)S(1)}, bf16[32,2048]{1,0:T(8,128)(2,1)S(1)}, u32[]{:S(2)}, u32[]{:S(2)}) %collective-permute-start.4) | collective-permute-done | bytes 131104 | tf_op jit(solution)/shard_map/ppermute | solution.py:198
  104.6 4.0 %collective-permute-done.3.refs_2_ = bf16[32,2048]{1,0:T(8,128)(2,1)S(1)} collective-permute-done((bf16[32,2048]{1,0:T(8,128)(2,1)S(1)}, bf16[32,2048]{1,0:T(8,128)(2,1)S(1)}, u32[]{:S(2)}, u32[]{:S(2)}) %collective-permute-start.3) | collective-permute-done | bytes 131104 | tf_op jit(solution)/shard_map/ppermute | solution.py:198
  108.5 0.0 collective-permute-done.9.refs_8_
  108.5 1.2 collective-permute-done.8.refs_7_
  109.7 1.3 collective-permute-done.7.refs_6_
  111.0 0.0 copy-done.2
  111.0 0.0 copy-done.3
  111.0 0.0 copy-done.4
  111.1 0.6 copy-done.9
  111.7 7.9 %channel_mixer.1 = (f32[32,2048]{1,0:T(8,128)}, bf16[32,2048]{1,0:T(8,128)(2,1)}, bf16[32,2048]{1,0:T(8,128)(2,1)}, bf16[32,2048]{1,0:T(8,128)(2,1)}, f32[32,204...) custom-call(s32[1]{0:T(128)} %bitcast.7.refs_0_, ...), custom_call_target="tpu_custom_call" | custom-call | tf_op jit(solution)/shard_map/channel_mixer/pallas_call | solution.py:292
  119.6 0.8 collective-permute-start.16
  120.3 0.5 collective-permute-start.17
  120.8 0.9 collective-permute-start.18
  121.7 2.6 %collective-permute-start.13 = (bf16[32,2048]{1,0:T(8,128)(2,1)}, bf16[32,2048]{1,0:T(8,128)(2,1)S(1)}, u32[]{:S(2)}, u32[]{:S(2)}) collective-permute-start(bf16[32,2048]{1,0:T(8,128)(2,1)} %get-tuple-element.40), channel_id=1, source_target_pairs={{0,3},{1,0},{2,1},{3,2},{4,7},{5,4},{6,5},{7,6},{8,11},{9,8},{10,9... | collective-permute-start | bytes 393224 | tf_op jit(solution)/shard_map/ppermute | solution.py:198
  124.3 1.5 %collective-permute-start.14 = (bf16[32,2048]{1,0:T(8,128)(2,1)}, bf16[32,2048]{1,0:T(8,128)(2,1)S(1)}, u32[]{:S(2)}, u32[]{:S(2)}) collective-permute-start(bf16[32,2048]{1,0:T(8,128)(2,1)} %get-tuple-element.41), channel_id=1, source_target_pairs={{0,2},{1,3},{2,0},{3,1},{4,6},{5,7},{6,4},{7,5},{8,10},{9,11},{10,... | collective-permute-start | bytes 393224 | tf_op jit(solution)/shard_map/ppermute | solution.py:198
  125.9 0.3 collective-permute-done.16
  126.2 1.0 collective-permute-start.15
  127.2 1.2 collective-permute-done.17
  128.4 3.3 %collective-permute-done.18 = bf16[32,2048]{1,0:T(8,128)(2,1)S(1)} collective-permute-done((bf16[32,2048]{1,0:T(8,128)(2,1)}, bf16[32,2048]{1,0:T(8,128)(2,1)S(1)}, u32[]{:S(2)}, u32[]{:S(2)}) %collective-permute-start.18) | collective-permute-done | bytes 131104 | tf_op jit(solution)/shard_map/ppermute | solution.py:198
  131.7 1.0 add_convert_fusion
  132.7 0.8 collective-permute-start.19
  133.5 0.0 collective-permute-done.13
  133.5 0.0 collective-permute-done.14
  133.5 1.0 collective-permute-done.15
  134.5 3.2 %collective-permute-done.19 = bf16[32,2048]{1,0:T(8,128)(2,1)S(1)} collective-permute-done((bf16[32,2048]{1,0:T(8,128)(2,1)S(1)}, bf16[32,2048]{1,0:T(8,128)(2,1)S(1)}, u32[]{:S(2)}, u32[]{:S(2)}) %collective-permute-start.19) | collective-permute-done | bytes 131104 | tf_op jit(solution)/shard_map/ppermute | solution.py:309
  137.8 1.7 %fusion.7 = bf16[32,2048]{1,0:T(8,128)(2,1)} fusion(f32[32,2048]{1,0:T(8,128)} %get-tuple-element.39, bf16[32,2048]{1,0:T(8,128)(2,1)S(1)} %get-tuple-element.48, bf16[32,2048]{1,0:T(8,128)(2,1)S(1)} %collective-permute-done.19, bf16[32,2048]{1,0:T(8,128)(2,1)S(1)} %collective-permute-done.15, bf16[32,2048]{1,0:T(8,128)(2,1)S(1)} %collective-permute-done.14, ...), kind=kLoop, calls=%fused_computation.11 | loop fusion | flops 720896 | bytes 1048576 | tf_op jit(solution)/shard_map/convert_element_type | solution.py:310
  (17 shorter events, 0.0 us)
Async XLA Ops:
  6.5 104.5 %all-gather.2.cloned.1.call-start = ((), (), s32[]{:S(2)}) async-start(), calls=%async_computation.2 | async-start | bytes 10027008 | tf_op jit(solution)/shard_map/all_gather | solution.py:252
  11.7 8.4 %collective-permute-start.11 = (bf16[32,2304]{1,0:T(8,128)(2,1)}, bf16[32,2304]{1,0:T(8,128)(2,1)S(1)}, u32[]{:S(2)}, u32[]{:S(2)}) collective-permute-start(bf16[32,2304]{1,0:T(8,128)(2,1)} %get-tuple-element.37), channel_id=1, source_target_pairs={{0,16},{8,24},{16,0},{24,8},{1,17},{9,25},{17,1},{25,9},{2,18},{10... | collective-permute-start | bytes 442376 | tf_op jit(solution)/shard_map/ppermute | solution.py:198
  13.7 7.4 %collective-permute-start.12 = (bf16[32,2304]{1,0:T(8,128)(2,1)}, bf16[32,2304]{1,0:T(8,128)(2,1)S(1)}, u32[]{:S(2)}, u32[]{:S(2)}) collective-permute-start(bf16[32,2304]{1,0:T(8,128)(2,1)} %get-tuple-element.38), channel_id=1, source_target_pairs={{0,24},{8,0},{16,8},{24,16},{1,25},{9,1},{17,9},{25,17},{2,26},{10... | collective-permute-start | bytes 442376 | tf_op jit(solution)/shard_map/ppermute | solution.py:198
  14.4 7.7 %collective-permute-start.10 = (bf16[32,2304]{1,0:T(8,128)(2,1)}, bf16[32,2304]{1,0:T(8,128)(2,1)S(1)}, u32[]{:S(2)}, u32[]{:S(2)}) collective-permute-start(bf16[32,2304]{1,0:T(8,128)(2,1)} %get-tuple-element.38), channel_id=1, source_target_pairs={{0,8},{8,16},{16,24},{24,0},{1,9},{9,17},{17,25},{25,1},{2,10},{10... | collective-permute-start | bytes 442376 | tf_op jit(solution)/shard_map/ppermute | solution.py:198
  23.9 30.2 %all-to-all-start = ((bf16[64,24,128]{2,1,0:T(8,128)(2,1)}), bf16[64,24,128]{2,1,0:T(8,128)(2,1)S(1)}, u32[]{:S(2)}, u32[]{:S(2)}) async-start(bf16[64,24,128]{2,1,0:T(8,128)(2,1)} %get-tuple-element.29), calls=%async_computation | async-start | bytes 786432 | tf_op jit(solution)/shard_map/all_to_all | solution.py:243
  54.1 0.8 copy-start
  56.8 20.7 %all-to-all-start.1 = ((bf16[64,16,128]{2,1,0:T(8,128)(2,1)}), bf16[64,16,128]{2,1,0:T(8,128)(2,1)S(1)}, u32[]{:S(2)}, u32[]{:S(2)}) async-start(bf16[64,16,128]{2,1,0:T(8,128)(2,1)} %block_scan.1), calls=%async_computation.1 | async-start | bytes 524288 | tf_op jit(solution)/shard_map/all_to_all | solution.py:262
  77.4 0.7 copy-start.1
  78.2 9.2 %copy-start.10 = (bf16[2048]{0:T(1024)(128)(2,1)S(1)}, bf16[2048]{0:T(1024)(128)(2,1)}, u32[]{:S(2)}) copy-start(bf16[2048]{0:T(1024)(128)(2,1)} %param.22) | copy-start | bytes 12292
  81.7 6.8 %collective-permute-start = (bf16[32,2048]{1,0:T(8,128)(2,1)}, bf16[32,2048]{1,0:T(8,128)(2,1)S(1)}, u32[]{:S(2)}, u32[]{:S(2)}) collective-permute-start(bf16[32,2048]{1,0:T(8,128)(2,1)} %get-tuple-element.31), channel_id=1, source_target_pairs={{0,1},{1,2},{2,3},{3,0},{4,5},{5,6},{6,7},{7,4},{8,9},{9,10},{10,1... | collective-permute-start | bytes 393224 | tf_op jit(solution)/shard_map/ppermute | solution.py:198
  83.2 9.1 %collective-permute-start.1 = (bf16[32,2048]{1,0:T(8,128)(2,1)}, bf16[32,2048]{1,0:T(8,128)(2,1)S(1)}, u32[]{:S(2)}, u32[]{:S(2)}) collective-permute-start(bf16[32,2048]{1,0:T(8,128)(2,1)} %get-tuple-element.32), channel_id=1, source_target_pairs={{0,2},{1,3},{2,0},{3,1},{4,6},{5,7},{6,4},{7,5},{8,10},{9,11},{10,... | collective-permute-start | bytes 393224 | tf_op jit(solution)/shard_map/ppermute | solution.py:198
  85.9 6.3 %collective-permute-start.2 = (bf16[32,2048]{1,0:T(8,128)(2,1)}, bf16[32,2048]{1,0:T(8,128)(2,1)S(1)}, u32[]{:S(2)}, u32[]{:S(2)}) collective-permute-start(bf16[32,2048]{1,0:T(8,128)(2,1)} %get-tuple-element.33), channel_id=1, source_target_pairs={{0,3},{1,0},{2,1},{3,2},{4,7},{5,4},{6,5},{7,6},{8,11},{9,8},{10,9... | collective-permute-start | bytes 393224 | tf_op jit(solution)/shard_map/ppermute | solution.py:198
  93.6 17.4 %copy-start.2 = (bf16[32,2048]{1,0:T(8,128)(2,1)}, bf16[32,2048]{1,0:T(8,128)(2,1)S(1)}, u32[]{:S(2)}) copy-start(bf16[32,2048]{1,0:T(8,128)(2,1)S(1)} %fusion.2.refs_1_) | copy-start | bytes 393220
  93.6 5.1 %collective-permute-start.6 = (bf16[32,2048]{1,0:T(8,128)(2,1)S(1)}, bf16[32,2048]{1,0:T(8,128)(2,1)S(1)}, u32[]{:S(2)}, u32[]{:S(2)}) collective-permute-start(bf16[32,2048]{1,0:T(8,128)(2,1)S(1)} %fusion.2.refs_1_), channel_id=1, source_target_pairs={{0,8},{8,0},{16,24},{24,16},{1,9},{9,1},{17,25},{25,17},{2,10},{10... | collective-permute-start | bytes 393224 | tf_op jit(solution)/shard_map/ppermute | solution.py:287
  94.4 8.2 %collective-permute-start.5 = (bf16[32,2048]{1,0:T(8,128)(2,1)S(1)}, bf16[32,2048]{1,0:T(8,128)(2,1)S(1)}, u32[]{:S(2)}, u32[]{:S(2)}) collective-permute-start(bf16[32,2048]{1,0:T(8,128)(2,1)S(1)} %fusion.2.refs_1_), channel_id=1, source_target_pairs={{0,3},{1,0},{2,1},{3,2},{4,7},{5,4},{6,5},{7,6},{8,11},{9,8},{10,9... | collective-permute-start | bytes 393224 | tf_op jit(solution)/shard_map/ppermute | solution.py:198
  97.0 7.5 %collective-permute-start.4 = (bf16[32,2048]{1,0:T(8,128)(2,1)S(1)}, bf16[32,2048]{1,0:T(8,128)(2,1)S(1)}, u32[]{:S(2)}, u32[]{:S(2)}) collective-permute-start(bf16[32,2048]{1,0:T(8,128)(2,1)S(1)} %fusion.2.refs_1_), channel_id=1, source_target_pairs={{0,2},{1,3},{2,0},{3,1},{4,6},{5,7},{6,4},{7,5},{8,10},{9,11},{10,... | collective-permute-start | bytes 393224 | tf_op jit(solution)/shard_map/ppermute | solution.py:198
  97.8 10.7 %collective-permute-start.3 = (bf16[32,2048]{1,0:T(8,128)(2,1)S(1)}, bf16[32,2048]{1,0:T(8,128)(2,1)S(1)}, u32[]{:S(2)}, u32[]{:S(2)}) collective-permute-start(bf16[32,2048]{1,0:T(8,128)(2,1)S(1)} %fusion.2.refs_1_), channel_id=1, source_target_pairs={{0,1},{1,2},{2,3},{3,0},{4,5},{5,6},{6,7},{7,4},{8,9},{9,10},{10,1... | collective-permute-start | bytes 393224 | tf_op jit(solution)/shard_map/ppermute | solution.py:198
  98.7 12.4 %copy-start.3 = (bf16[32,2048]{1,0:T(8,128)(2,1)}, bf16[32,2048]{1,0:T(8,128)(2,1)S(1)}, u32[]{:S(2)}) copy-start(bf16[32,2048]{1,0:T(8,128)(2,1)S(1)} %collective-permute-done.6.refs_5_) | copy-start | bytes 393220
  98.7 9.9 %collective-permute-start.9 = (bf16[32,2048]{1,0:T(8,128)(2,1)S(1)}, bf16[32,2048]{1,0:T(8,128)(2,1)S(1)}, u32[]{:S(2)}, u32[]{:S(2)}) collective-permute-start(bf16[32,2048]{1,0:T(8,128)(2,1)S(1)} %collective-permute-done.6.refs_5_), channel_id=1, source_target_pairs={{0,3},{1,0},{2,1},{3,2},{4,7},{5,4},{6,5},{7,6},{8,11},{9,8},{10,9... | collective-permute-start | bytes 393224 | tf_op jit(solution)/shard_map/ppermute | solution.py:198
  101.0 8.7 %collective-permute-start.8 = (bf16[32,2048]{1,0:T(8,128)(2,1)S(1)}, bf16[32,2048]{1,0:T(8,128)(2,1)S(1)}, u32[]{:S(2)}, u32[]{:S(2)}) collective-permute-start(bf16[32,2048]{1,0:T(8,128)(2,1)S(1)} %collective-permute-done.6.refs_5_), channel_id=1, source_target_pairs={{0,2},{1,3},{2,0},{3,1},{4,6},{5,7},{6,4},{7,5},{8,10},{9,11},{10,... | collective-permute-start | bytes 393224 | tf_op jit(solution)/shard_map/ppermute | solution.py:198
  102.6 8.4 %copy-start.4 = (bf16[32,2048]{1,0:T(8,128)(2,1)}, bf16[32,2048]{1,0:T(8,128)(2,1)S(1)}, u32[]{:S(2)}) copy-start(bf16[32,2048]{1,0:T(8,128)(2,1)S(1)} %collective-permute-done.5.refs_4_) | copy-start | bytes 393220
  102.6 8.4 %collective-permute-start.7 = (bf16[32,2048]{1,0:T(8,128)(2,1)S(1)}, bf16[32,2048]{1,0:T(8,128)(2,1)S(1)}, u32[]{:S(2)}, u32[]{:S(2)}) collective-permute-start(bf16[32,2048]{1,0:T(8,128)(2,1)S(1)} %collective-permute-done.6.refs_5_), channel_id=1, source_target_pairs={{0,1},{1,2},{2,3},{3,0},{4,5},{5,6},{6,7},{7,4},{8,9},{9,10},{10,1... | collective-permute-start | bytes 393224 | tf_op jit(solution)/shard_map/ppermute | solution.py:198
  104.6 6.5 %copy-start.5 = (bf16[32,2048]{1,0:T(8,128)(2,1)}, bf16[32,2048]{1,0:T(8,128)(2,1)S(1)}, u32[]{:S(2)}) copy-start(bf16[32,2048]{1,0:T(8,128)(2,1)S(1)} %collective-permute-done.4.refs_3_) | copy-start | bytes 393220
  108.5 2.5 %copy-start.6 = (bf16[32,2048]{1,0:T(8,128)(2,1)}, bf16[32,2048]{1,0:T(8,128)(2,1)S(1)}, u32[]{:S(2)}) copy-start(bf16[32,2048]{1,0:T(8,128)(2,1)S(1)} %collective-permute-done.3.refs_2_) | copy-start | bytes 393220
  108.5 2.5 %copy-start.7 = (bf16[32,2048]{1,0:T(8,128)(2,1)}, bf16[32,2048]{1,0:T(8,128)(2,1)S(1)}, u32[]{:S(2)}) copy-start(bf16[32,2048]{1,0:T(8,128)(2,1)S(1)} %collective-permute-done.9.refs_8_) | copy-start | bytes 393220
  109.7 1.4 copy-start.8
  111.0 0.6 copy-start.9
  119.6 6.7 %collective-permute-start.16 = (bf16[32,2048]{1,0:T(8,128)(2,1)}, bf16[32,2048]{1,0:T(8,128)(2,1)S(1)}, u32[]{:S(2)}, u32[]{:S(2)}) collective-permute-start(bf16[32,2048]{1,0:T(8,128)(2,1)} %get-tuple-element.44), channel_id=1, source_target_pairs={{0,3},{1,0},{2,1},{3,2},{4,7},{5,4},{6,5},{7,6},{8,11},{9,8},{10,9... | collective-permute-start | bytes 393224 | tf_op jit(solution)/shard_map/ppermute | solution.py:198
  120.3 8.1 %collective-permute-start.17 = (bf16[32,2048]{1,0:T(8,128)(2,1)}, bf16[32,2048]{1,0:T(8,128)(2,1)S(1)}, u32[]{:S(2)}, u32[]{:S(2)}) collective-permute-start(bf16[32,2048]{1,0:T(8,128)(2,1)} %get-tuple-element.45), channel_id=1, source_target_pairs={{0,2},{1,3},{2,0},{3,1},{4,6},{5,7},{6,4},{7,5},{8,10},{9,11},{10,... | collective-permute-start | bytes 393224 | tf_op jit(solution)/shard_map/ppermute | solution.py:198
  120.8 10.8 %collective-permute-start.18 = (bf16[32,2048]{1,0:T(8,128)(2,1)}, bf16[32,2048]{1,0:T(8,128)(2,1)S(1)}, u32[]{:S(2)}, u32[]{:S(2)}) collective-permute-start(bf16[32,2048]{1,0:T(8,128)(2,1)} %get-tuple-element.46), channel_id=1, source_target_pairs={{0,1},{1,2},{2,3},{3,0},{4,5},{5,6},{6,7},{7,4},{8,9},{9,10},{10,1... | collective-permute-start | bytes 393224 | tf_op jit(solution)/shard_map/ppermute | solution.py:198
  121.7 11.8 %collective-permute-start.13 = (bf16[32,2048]{1,0:T(8,128)(2,1)}, bf16[32,2048]{1,0:T(8,128)(2,1)S(1)}, u32[]{:S(2)}, u32[]{:S(2)}) collective-permute-start(bf16[32,2048]{1,0:T(8,128)(2,1)} %get-tuple-element.40), channel_id=1, source_target_pairs={{0,3},{1,0},{2,1},{3,2},{4,7},{5,4},{6,5},{7,6},{8,11},{9,8},{10,9... | collective-permute-start | bytes 393224 | tf_op jit(solution)/shard_map/ppermute | solution.py:198
  124.3 9.2 %collective-permute-start.14 = (bf16[32,2048]{1,0:T(8,128)(2,1)}, bf16[32,2048]{1,0:T(8,128)(2,1)S(1)}, u32[]{:S(2)}, u32[]{:S(2)}) collective-permute-start(bf16[32,2048]{1,0:T(8,128)(2,1)} %get-tuple-element.41), channel_id=1, source_target_pairs={{0,2},{1,3},{2,0},{3,1},{4,6},{5,7},{6,4},{7,5},{8,10},{9,11},{10,... | collective-permute-start | bytes 393224 | tf_op jit(solution)/shard_map/ppermute | solution.py:198
  126.2 8.3 %collective-permute-start.15 = (bf16[32,2048]{1,0:T(8,128)(2,1)}, bf16[32,2048]{1,0:T(8,128)(2,1)S(1)}, u32[]{:S(2)}, u32[]{:S(2)}) collective-permute-start(bf16[32,2048]{1,0:T(8,128)(2,1)} %get-tuple-element.42), channel_id=1, source_target_pairs={{0,1},{1,2},{2,3},{3,0},{4,5},{5,6},{6,7},{7,4},{8,9},{9,10},{10,1... | collective-permute-start | bytes 393224 | tf_op jit(solution)/shard_map/ppermute | solution.py:198
  132.7 5.1 %collective-permute-start.19 = (bf16[32,2048]{1,0:T(8,128)(2,1)S(1)}, bf16[32,2048]{1,0:T(8,128)(2,1)S(1)}, u32[]{:S(2)}, u32[]{:S(2)}) collective-permute-start(bf16[32,2048]{1,0:T(8,128)(2,1)S(1)} %add_convert_fusion), channel_id=1, source_target_pairs={{0,8},{8,0},{16,24},{24,16},{1,9},{9,1},{17,25},{25,17},{2,10},{10... | collective-permute-start | bytes 393224 | tf_op jit(solution)/shard_map/ppermute | solution.py:309
Sparse Core Ops, SparseCore 0:
  24.0 75.6 all-gather.1

commit v2 on v1

--- a/solution.py
+++ b/solution.py
@@ -139,12 +139,12 @@
 
 
 def mixer_body(at_ref, *refs, hidden):
-    rows_in, whole_ref, outs = refs[:8], refs[8], refs[9:17]
-    tokens_ref, weights_ref, act_ref, sems = refs[17:]
+    (own_ref, near_ref), x_refs, whole_ref, outs = refs[:2], refs[2:6], refs[6], refs[7:13]
+    tokens_ref, weights_ref, act_ref, sems = refs[13:]
     z_size, y_size, cores, _, wide = weights_ref.shape
     model = tokens_ref.shape[1]
     y = at_ref[0]
-    chunks = 2
+    chunks = 4
     z_step = z_size // chunks
     step = model // chunks
     width = wide // 3
@@ -165,9 +165,14 @@
     for group in groups:
         for copy in group:
             copy.start()
-    part = outs[0].shape[0]
-    for n, ref in enumerate(rows_in):
-        tokens_ref[n * part : (n + 1) * part, :] = ref[...]
+    split = model // 2
+    rows = own_ref.shape[0]
+    part = rows // len(x_refs)
+    tokens_ref[:rows, :split] = own_ref[...]
+    tokens_ref[rows:, :split] = near_ref[...]
+    for d, ref in enumerate(x_refs):
+        tokens_ref[d * part : (d + 1) * part, split:] = ref[:part]
+        tokens_ref[rows + d * part : rows + (d + 1) * part, split:] = ref[part:]
     weights = weights_ref.reshape(model, wide)
     for n, group in enumerate(groups):
         for copy in group:
@@ -184,8 +189,12 @@
     low = jnp.where(lax.rem(y, 2) == 0, 0, width - hidden // 2)
     inner = jnp.where((lane >= low) & (lane < low + hidden // 2), inner, 0.0).astype(BF16)
     lowered = nt_dot(inner, weights[:, 2 * width :])
-    for d, out_ref in enumerate(outs):
-        out_ref[...] = lowered[d * part : (d + 1) * part].astype(out_ref.dtype)
+    for d, out_ref in enumerate(outs[:4]):
+        at = slice(d * part, (d + 1) * part)
+        out_ref[:part] = lowered[:rows][at, :split].astype(out_ref.dtype)
+        out_ref[part:] = lowered[rows:][at, :split].astype(out_ref.dtype)
+    outs[4][...] = lowered[:rows, split:]
+    outs[5][...] = lowered[rows:, split:].astype(BF16)
 
 
 VMEM = pl.BlockSpec(memory_space=pltpu.VMEM)
@@ -249,9 +258,8 @@
         name="weight_halves",
     )((y_at % 2)[None], *weights)
     line = [keep] + [shift(give if d % 2 else keep, "sp_1", d) for d in range(1, y_size)]
-    whole = lax.all_gather(
-        jnp.concatenate(line, axis=0), ("sp_0", "sp_2"), axis=0, tiled=True
-    ).reshape(z_size, cores, y_size, slab, 3 * half)
+    line = jnp.concatenate(line, axis=0)
+    whole = lax.all_gather(line, ("sp_0", "sp_2"), axis=0, tiled=True).reshape(z_size, cores, y_size, slab, 3 * half)
     give = pl.pallas_call(
         scan_body,
         out_shape=jax.ShapeDtypeStruct((blocks, chunk, HEAD), BF16),
@@ -284,30 +292,40 @@
         * mixer_norm_gain.astype(F32)
     ).astype(BF16)
     swap = [(k, k ^ 1) for k in range(y_size)]
-    theirs = lax.ppermute(normed, "sp_1", swap)
-    tokens = [normed] + [shift(normed, "tp", d) for d in range(1, n_tp)]
-    tokens += [theirs] + [shift(theirs, "tp", d) for d in range(1, n_tp)]
-    kept = (jax.ShapeDtypeStruct((part, model), F32),)
-    sent = (jax.ShapeDtypeStruct((part, model), BF16),) * (n_tp - 1)
+    split = model // 2
+    left, right = normed[:, :split], normed[:, split:]
+    both = jnp.concatenate([right, lax.ppermute(right, "sp_1", swap)], axis=0)
+    own = jnp.concatenate([left] + [shift(left, "tp", d) for d in range(1, n_tp)], axis=0)
+    tokens = [own, lax.ppermute(own, "sp_1", swap)]
+    tokens += [both] + [shift(both, "tp", d) for d in range(1, n_tp)]
     lowered = pl.pallas_call(
         lambda *refs: mixer_body(*refs, hidden=hidden),
-        out_shape=(kept + sent) * 2,
-        in_specs=[SMEM] + [VMEM] * (2 * n_tp) + [ANY],
-        out_specs=(VMEM,) * (2 * n_tp),
+        out_shape=(jax.ShapeDtypeStruct((2 * part, split), F32),)
+        + (jax.ShapeDtypeStruct((2 * part, split), BF16),) * (n_tp - 1)
+        + (jax.ShapeDtypeStruct((rows, split), F32), jax.ShapeDtypeStruct((rows, split), BF16)),
+        in_specs=[SMEM] + [VMEM] * len(tokens) + [ANY],
+        out_specs=(VMEM,) * (n_tp + 2),
         scratch_shapes=[
             pltpu.VMEM((2 * rows, model), BF16),
             pltpu.VMEM((z_size, y_size, cores, slab, 3 * half), BF16),
             pltpu.VMEM((2 * rows, 2 * half), F32),
-            pltpu.SemaphoreType.DMA((2 * y_size * cores,)),
+            pltpu.SemaphoreType.DMA((4 * y_size * cores,)),
         ],
         compiler_params=pltpu.CompilerParams(vmem_limit_bytes=54 * 1024 * 1024),
         name="channel_mixer",
     )(y_at[None], *tokens, whole)
-    mine, other = lowered[:n_tp], lowered[n_tp:]
-    other = [other[0]] + [shift(other[d], "tp", n_tp - d) for d in range(1, n_tp)]
-    mine = [mine[0]] + [shift(mine[d], "tp", n_tp - d) for d in range(1, n_tp)]
-    theirs = lax.ppermute(sum(a.astype(F32) for a in other).astype(BF16), "sp_1", swap)
-    return (sum((a.astype(F32) for a in mine), hidden_state.astype(F32)) + theirs.astype(F32)).astype(BF16)
+    crossed = lax.ppermute(lowered[n_tp + 1], "sp_1", swap)
+    sums = lowered[0]
+    for d in range(1, n_tp):
+        sums = sums + shift(lowered[d], "tp", n_tp - d).astype(F32)
+    added = lowered[n_tp] + crossed.astype(F32)
+    out_right = hidden_state[:, split:].astype(F32) + added[:part]
+    for d in range(1, n_tp):
+        back = added[d * part : (d + 1) * part].astype(BF16)
+        out_right = out_right + shift(back, "tp", n_tp - d).astype(F32)
+    theirs = lax.ppermute(sums[part:].astype(BF16), "sp_1", swap)
+    out_left = hidden_state[:, :split].astype(F32) + sums[:part] + theirs.astype(F32)
+    return jnp.concatenate([out_left, out_right], axis=1).astype(BF16)
 
 
 def solution(mesh):

time: 147 us -> 149 us (1.014)
  the two profiles are of different devices: /device:TPU:16 before, /device:TPU:6 now
where the time goes in v2:
time: 149 us; the launch traced here: 148 us
  waiting for transfers between devices  60.9 us (41%)
  starting transfers between devices  48.9 us (33%)
  Pallas kernels  17.9 us (12%)
  between operations  13.6 us (9%)
  other arithmetic  4.98 us (3%)
  local copies, waits for them, and re-layouts  2.23 us (1%)
    ppermute x18, waiting for transfers between devices, shift(): lax.ppermute(array, axis, [(k, (k + by) % size) for k in range(size)])  27 us
    ppermute x18, starting transfers between devices, shift(): lax.ppermute(array, axis, [(k, (k + by) % size) for k in range(size)])  25.9 us
    all_to_all x1, waiting for transfers between devices, local(): got = lax.all_to_all(send, SP, 0, 0, tiled=True)  18.1 us
    all_to_all x1, waiting for transfers between devices, local(): lax.all_to_all(give, SP, 0, 0, tiled=True).reshape(2 * heads, HEAD, HEAD)  15.2 us
    all_to_all x1, starting transfers between devices, local(): got = lax.all_to_all(send, SP, 0, 0, tiled=True)  11.5 us
    pallas_call x1, Pallas kernels, local(): pl.pallas_call(lambda *refs: mixer_body(*refs, hidden=hidden), out_shape=...  7.38 us
    all_to_all x1, starting transfers between devices, local(): lax.all_to_all(give, SP, 0, 0, tiled=True).reshape(2 * heads, HEAD, HEAD)  5.65 us
    pallas_call x1, Pallas kernels, local(): pl.pallas_call(project_body, out_shape=(jax.ShapeDtypeStruct((part, model...  3.54 us
  transfers between devices with their start and end apart: 25, of which 19 were waited for; matrix products, arithmetic and copies ran while one was open for 2% of the time, Pallas kernels for 4%

profile of v2, /device:TPU:6, one launch (start us, length us, event | category | flops | bytes accessed | tf_op | source)
XLA Modules:
  0.0 148.4 jit_solution(14782172553790142586)
XLA Ops:
  6.5 3.4 %local_sweep.1 = (bf16[64,24,128]{2,1,0:T(8,128)(2,1)}, f32[128,512]{1,0:T(8,128)}, bf16[2,128,512]{2,1,0:T(8,128)(2,1)}) custom-call(bf16[128,512]{1,0:T(8,128)(2,1)} %q_ref.1, bf16[2,128,512]{2,1,0:T(8,128)(2,1)} %f_ref.1, bf16[128,512]{1,0:T(8,128)(2,1)} %v_ref.1, f32[1,512]{1,0:T(1,128)} %bitcast.13, f32[4,128]{1,0:T(4,128)} %bitcast.14), custom_call_target="tpu_custom_call" | custom-call | tf_op jit(solution)/shard_map/local_sweep/pallas_call | solution.py:239
  9.9 1.7 %weight_halves.1 = (bf16[32,2304]{1,0:T(8,128)(2,1)}, bf16[32,2304]{1,0:T(8,128)(2,1)}) custom-call(s32[1]{0:T(128)} %bitcast.8.parity_ref, bf16[32,1408]{1,0:T(8,128)(2,1)} %gate_ref.2, bf16[32,1408]{1,0:T(8,128)(2,1)} %up_ref, bf16[32,1408]{1,0:T(8,128)(2,1)} %bitcast.12), custom_call_target="tpu_custom_call" | custom-call | tf_op jit(solution)/shard_map/weight_halves/pallas_call | solution.py:253
  11.7 3.2 %collective-permute-start.12 = (bf16[32,2304]{1,0:T(8,128)(2,1)}, bf16[32,2304]{1,0:T(8,128)(2,1)S(1)}, u32[]{:S(2)}, u32[]{:S(2)}) collective-permute-start(bf16[32,2304]{1,0:T(8,128)(2,1)} %get-tuple-element.35), channel_id=1, source_target_pairs={{0,16},{8,24},{16,0},{24,8},{1,17},{9,25},{17,1},{25,9},{2,18},{10... | collective-permute-start | bytes 442376 | tf_op jit(solution)/shard_map/ppermute | solution.py:207
  14.9 1.1 collective-permute-start.13
  15.9 1.0 collective-permute-start.11
  16.9 3.1 %collective-permute-done.12 = bf16[32,2304]{1,0:T(8,128)(2,1)S(1)} collective-permute-done((bf16[32,2304]{1,0:T(8,128)(2,1)}, bf16[32,2304]{1,0:T(8,128)(2,1)S(1)}, u32[]{:S(2)}, u32[]{:S(2)}) %collective-permute-start.12) | collective-permute-done | bytes 147488 | tf_op jit(solution)/shard_map/ppermute | solution.py:207
  20.0 2.5 %collective-permute-done.13 = bf16[32,2304]{1,0:T(8,128)(2,1)S(1)} collective-permute-done((bf16[32,2304]{1,0:T(8,128)(2,1)}, bf16[32,2304]{1,0:T(8,128)(2,1)S(1)}, u32[]{:S(2)}, u32[]{:S(2)}) %collective-permute-start.13) | collective-permute-done | bytes 147488 | tf_op jit(solution)/shard_map/ppermute | solution.py:207
  22.5 0.3 collective-permute-done.11
  22.7 1.8 %pad_maximum_fusion = bf16[128,2304]{1,0:T(8,128)(2,1)} fusion(bf16[32,2304]{1,0:T(8,128)(2,1)S(1)} %collective-permute-done.13, bf16[32,2304]{1,0:T(8,128)(2,1)S(1)} %collective-permute-done.12, bf16[32,2304]{1,0:T(8,128)(2,1)S(1)} %collective-permute-done.11, bf16[32,2304]{1,0:T(8,128)(2,1)} %get-tuple-element.35), kind=kLoop, calls=%fused_computation | loop fusion | flops 2359296 | bytes 1179648 | tf_op jit(solution)/shard_map/concatenate | solution.py:261
  24.5 0.0 all-gather.2.cloned.1.call-update
  24.6 11.5 %all-to-all-start = ((bf16[64,24,128]{2,1,0:T(8,128)(2,1)}), bf16[64,24,128]{2,1,0:T(8,128)(2,1)S(1)}, u32[]{:S(2)}, u32[]{:S(2)}) async-start(bf16[64,24,128]{2,1,0:T(8,128)(2,1)} %get-tuple-element.27), calls=%async_computation | async-start | bytes 786432 | tf_op jit(solution)/shard_map/all_to_all | solution.py:252
  36.1 18.1 %all-to-all-done.got_ref = bf16[64,24,128]{2,1,0:T(8,128)(2,1)S(1)} async-done(((bf16[64,24,128]{2,1,0:T(8,128)(2,1)}), bf16[64,24,128]{2,1,0:T(8,128)(2,1)S(1)}, u32[]{:S(2)}, u32[]{:S(2)}) %all-to-all-start) | async-done | bytes 393248 | tf_op jit(solution)/shard_map/all_to_all | solution.py:252
  54.2 0.7 copy-done
  55.0 1.8 %block_scan.1 = bf16[64,16,128]{2,1,0:T(8,128)(2,1)} custom-call(s32[1]{0:T(128)} %bitcast.3.back_ref, bf16[64,24,128]{2,1,0:T(8,128)(2,1)} %copy-done), custom_call_target="tpu_custom_call" | custom-call | tf_op jit(solution)/shard_map/block_scan/pallas_call | solution.py:263
  56.8 5.7 %all-to-all-start.1 = ((bf16[64,16,128]{2,1,0:T(8,128)(2,1)}), bf16[64,16,128]{2,1,0:T(8,128)(2,1)S(1)}, u32[]{:S(2)}, u32[]{:S(2)}) async-start(bf16[64,16,128]{2,1,0:T(8,128)(2,1)} %block_scan.1), calls=%async_computation.1 | async-start | bytes 524288 | tf_op jit(solution)/shard_map/all_to_all | solution.py:270
  62.5 15.2 %all-to-all-done.1 = bf16[64,16,128]{2,1,0:T(8,128)(2,1)S(1)} async-done(((bf16[64,16,128]{2,1,0:T(8,128)(2,1)}), bf16[64,16,128]{2,1,0:T(8,128)(2,1)S(1)}, u32[]{:S(2)}, u32[]{:S(2)}) %all-to-all-start.1) | async-done | bytes 262176 | tf_op jit(solution)/shard_map/all_to_all | solution.py:270
  77.7 0.7 copy-done.1
  78.4 3.5 %norm_project.1 = (bf16[32,2048]{1,0:T(8,128)(2,1)}, bf16[32,2048]{1,0:T(8,128)(2,1)}, bf16[32,2048]{1,0:T(8,128)(2,1)}, bf16[32,2048]{1,0:T(8,128)(2,1)}) custom-call(s32[1]{0:T(128)} %bitcast.own_ref, f32[128,512]{1,0:T(8,128)} %get-tuple-element.24.near_ref, bf16[2,128,512]{2,1,0:T(8,128)(2,1)} %get-tuple-element.25.reach_ref, ...), custom_call_target="tpu_custom_call" | custom-call | tf_op jit(solution)/shard_map/norm_project/pallas_call | solution.py:273
  82.0 0.5 collective-permute-start
  82.4 2.4 %collective-permute-start.1 = (bf16[32,2048]{1,0:T(8,128)(2,1)}, bf16[32,2048]{1,0:T(8,128)(2,1)S(1)}, u32[]{:S(2)}, u32[]{:S(2)}) collective-permute-start(bf16[32,2048]{1,0:T(8,128)(2,1)} %get-tuple-element.30), channel_id=1, source_target_pairs={{0,2},{1,3},{2,0},{3,1},{4,6},{5,7},{6,4},{7,5},{8,10},{9,11},{10,... | collective-permute-start | bytes 393224 | tf_op jit(solution)/shard_map/ppermute | solution.py:207
  84.9 0.0 collective-permute-start.2
  84.9 3.7 %collective-permute-done = bf16[32,2048]{1,0:T(8,128)(2,1)S(1)} collective-permute-done((bf16[32,2048]{1,0:T(8,128)(2,1)}, bf16[32,2048]{1,0:T(8,128)(2,1)S(1)}, u32[]{:S(2)}, u32[]{:S(2)}) %collective-permute-start) | collective-permute-done | bytes 131104 | tf_op jit(solution)/shard_map/ppermute | solution.py:207
  88.5 1.9 %collective-permute-done.1 = bf16[32,2048]{1,0:T(8,128)(2,1)S(1)} collective-permute-done((bf16[32,2048]{1,0:T(8,128)(2,1)}, bf16[32,2048]{1,0:T(8,128)(2,1)S(1)}, u32[]{:S(2)}, u32[]{:S(2)}) %collective-permute-start.1) | collective-permute-done | bytes 131104 | tf_op jit(solution)/shard_map/ppermute | solution.py:207
  90.5 1.9 %collective-permute-done.2 = bf16[32,2048]{1,0:T(8,128)(2,1)S(1)} collective-permute-done((bf16[32,2048]{1,0:T(8,128)(2,1)}, bf16[32,2048]{1,0:T(8,128)(2,1)S(1)}, u32[]{:S(2)}, u32[]{:S(2)}) %collective-permute-start.2) | collective-permute-done | bytes 131104 | tf_op jit(solution)/shard_map/ppermute | solution.py:207
  92.3 1.2 fusion
  93.6 0.1 fusion.2
  93.7 1.0 collective-permute-start.5
  94.7 1.5 collective-permute-start.4
  96.2 1.9 %collective-permute-start.3 = (bf16[32,1024]{1,0:T(8,128)(2,1)S(1)}, bf16[32,1024]{1,0:T(8,128)(2,1)S(1)}, u32[]{:S(2)}, u32[]{:S(2)}) collective-permute-start(bf16[32,1024]{1,0:T(8,128)(2,1)S(1)} %get-tuple-element.53), channel_id=1, source_target_pairs={{0,1},{1,2},{2,3},{3,0},{4,5},{5,6},{6,7},{7,4},{8,9},{9,10},{10,1... | collective-permute-start | bytes 196616 | tf_op jit(solution)/shard_map/ppermute | solution.py:207
  98.1 1.4 collective-permute-start.7
  99.5 0.0 collective-permute-done.5
  99.6 0.9 collective-permute-done.4
  100.5 0.4 collective-permute-done.3
  100.9 1.5 %collective-permute-start.6 = (bf16[128,1024]{1,0:T(8,128)(2,1)S(1)}, bf16[128,1024]{1,0:T(8,128)(2,1)S(1)}, u32[]{:S(2)}, u32[]{:S(2)}) collective-permute-start(bf16[128,1024]{1,0:T(8,128)(2,1)S(1)} %pad_maximum_fusion.1.refs_1_), channel_id=1, source_target_pairs={{0,8},{8,0},{16,24},{24,16},{1,9},{9,1},{17,25},{25,17},{2,10},{10... | collective-permute-start | bytes 786440 | tf_op jit(solution)/shard_map/ppermute | solution.py:299
  102.4 0.5 collective-permute-done.7
  102.8 0.0 copy-start.3
  102.9 1.1 collective-permute-start.10
  104.0 2.9 %collective-permute-start.9 = (bf16[64,1024]{1,0:T(8,128)(2,1)S(1)}, bf16[64,1024]{1,0:T(8,128)(2,1)S(1)}, u32[]{:S(2)}, u32[]{:S(2)}) collective-permute-start(bf16[64,1024]{1,0:T(8,128)(2,1)S(1)} %pad_maximum_fusion.2.refs_3_), channel_id=1, source_target_pairs={{0,2},{1,3},{2,0},{3,1},{4,6},{5,7},{6,4},{7,5},{8,10},{9,11},{10,... | collective-permute-start | bytes 393224 | tf_op jit(solution)/shard_map/ppermute | solution.py:207
  106.9 1.0 collective-permute-start.8
  107.8 1.5 %collective-permute-done.10.refs_6_ = bf16[64,1024]{1,0:T(8,128)(2,1)S(1)} collective-permute-done((bf16[64,1024]{1,0:T(8,128)(2,1)S(1)}, bf16[64,1024]{1,0:T(8,128)(2,1)S(1)}, u32[]{:S(2)}, u32[]{:S(2)}) %collective-permute-start.10) | collective-permute-done | bytes 131104 | tf_op jit(solution)/shard_map/ppermute | solution.py:207
  109.4 1.9 %collective-permute-done.9.refs_5_ = bf16[64,1024]{1,0:T(8,128)(2,1)S(1)} collective-permute-done((bf16[64,1024]{1,0:T(8,128)(2,1)S(1)}, bf16[64,1024]{1,0:T(8,128)(2,1)S(1)}, u32[]{:S(2)}, u32[]{:S(2)}) %collective-permute-start.9) | collective-permute-done | bytes 131104 | tf_op jit(solution)/shard_map/ppermute | solution.py:207
  111.2 0.6 collective-permute-done.8.refs_4_
  111.8 0.0 collective-permute-done.6.refs_2_
  111.8 0.0 all-gather.2.cloned.1.call-done
  111.9 0.6 copy-done.8
  112.5 0.1 copy-done.5
  112.6 7.4 %channel_mixer.1 = (f32[64,1024]{1,0:T(8,128)}, bf16[64,1024]{1,0:T(8,128)(2,1)}, bf16[64,1024]{1,0:T(8,128)(2,1)}, bf16[64,1024]{1,0:T(8,128)(2,1)}, f32[128,1024]{1,0:T(8,128)}, /*index=5*/bf16[128,1024]{1,0:T(8,128)(2,1)}) custom-call(s32[1]{0:T(128)} %bitcast.7.refs_0_, bf16[128,1024]{1,0:T(8,128)(2,1)} %copy-done.2, bf16[128,1024]{1,0:T(8,128)(2,1)} %copy-done.5, ...), custom_call_target="tpu_custom_call" | custom-call | tf_op jit(solution)/shard_map/channel_mixer/pallas_call | solution.py:301
  120.0 1.3 collective-permute-start.14
  121.3 2.7 %collective-permute-start.15 = (bf16[64,1024]{1,0:T(8,128)(2,1)}, bf16[64,1024]{1,0:T(8,128)(2,1)S(1)}, u32[]{:S(2)}, u32[]{:S(2)}) collective-permute-start(bf16[64,1024]{1,0:T(8,128)(2,1)} %get-tuple-element.39), channel_id=1, source_target_pairs={{0,2},{1,3},{2,0},{3,1},{4,6},{5,7},{6,4},{7,5},{8,10},{9,11},{10,... | collective-permute-start | bytes 393224 | tf_op jit(solution)/shard_map/ppermute | solution.py:207
  123.9 0.6 collective-permute-start.16
  124.5 1.4 collective-permute-start.18
  125.9 0.5 collective-permute-done.14
  126.5 2.0 %collective-permute-done.15 = bf16[64,1024]{1,0:T(8,128)(2,1)S(1)} collective-permute-done((bf16[64,1024]{1,0:T(8,128)(2,1)}, bf16[64,1024]{1,0:T(8,128)(2,1)S(1)}, u32[]{:S(2)}, u32[]{:S(2)}) %collective-permute-start.15) | collective-permute-done | bytes 131104 | tf_op jit(solution)/shard_map/ppermute | solution.py:207
  128.5 0.6 collective-permute-done.16
  129.1 1.0 convert_add_fusion.1
  130.2 1.5 %collective-permute-start.17 = (bf16[32,1024]{1,0:T(8,128)(2,1)S(1)}, bf16[32,1024]{1,0:T(8,128)(2,1)S(1)}, u32[]{:S(2)}, u32[]{:S(2)}) collective-permute-start(bf16[32,1024]{1,0:T(8,128)(2,1)S(1)} %slice.71), channel_id=1, source_target_pairs={{0,8},{8,0},{16,24},{24,16},{1,9},{9,1},{17,25},{25,17},{2,10},{10... | collective-permute-start | bytes 196616 | tf_op jit(solution)/shard_map/ppermute | solution.py:326
  131.7 0.1 fusion.9
  131.8 1.2 collective-permute-start.19
  133.0 2.1 %collective-permute-start.21 = (bf16[32,1024]{1,0:T(8,128)(2,1)S(1)}, bf16[32,1024]{1,0:T(8,128)(2,1)S(1)}, u32[]{:S(2)}, u32[]{:S(2)}) collective-permute-start(bf16[32,1024]{1,0:T(8,128)(2,1)S(1)} %get-tuple-element.48), channel_id=1, source_target_pairs={{0,1},{1,2},{2,3},{3,0},{4,5},{5,6},{6,7},{7,4},{8,9},{9,10},{10,1... | collective-permute-start | bytes 196616 | tf_op jit(solution)/shard_map/ppermute | solution.py:207
  135.1 0.6 collective-permute-start.20
  135.7 1.7 %collective-permute-done.19 = bf16[32,1024]{1,0:T(8,128)(2,1)S(1)} collective-permute-done((bf16[32,1024]{1,0:T(8,128)(2,1)S(1)}, bf16[32,1024]{1,0:T(8,128)(2,1)S(1)}, u32[]{:S(2)}, u32[]{:S(2)}) %collective-permute-start.19) | collective-permute-done | bytes 65568 | tf_op jit(solution)/shard_map/ppermute | solution.py:207
  137.3 3.5 %collective-permute-done.20 = bf16[32,1024]{1,0:T(8,128)(2,1)S(1)} collective-permute-done((bf16[32,1024]{1,0:T(8,128)(2,1)S(1)}, bf16[32,1024]{1,0:T(8,128)(2,1)S(1)}, u32[]{:S(2)}, u32[]{:S(2)}) %collective-permute-start.20) | collective-permute-done | bytes 65568 | tf_op jit(solution)/shard_map/ppermute | solution.py:207
  140.9 0.1 fusion.8
  140.9 0.7 pad_maximum_fusion.3
  (26 shorter events, 0.1 us)
Async XLA Ops:
  6.5 105.3 %all-gather.2.cloned.1.call-start = ((), (), s32[]{:S(2)}) async-start(), calls=%async_computation.2 | async-start | bytes 10027008 | tf_op jit(solution)/shard_map/all_gather | solution.py:262
  11.7 8.3 %collective-permute-start.12 = (bf16[32,2304]{1,0:T(8,128)(2,1)}, bf16[32,2304]{1,0:T(8,128)(2,1)S(1)}, u32[]{:S(2)}, u32[]{:S(2)}) collective-permute-start(bf16[32,2304]{1,0:T(8,128)(2,1)} %get-tuple-element.35), channel_id=1, source_target_pairs={{0,16},{8,24},{16,0},{24,8},{1,17},{9,25},{17,1},{25,9},{2,18},{10... | collective-permute-start | bytes 442376 | tf_op jit(solution)/shard_map/ppermute | solution.py:207
  14.9 7.6 %collective-permute-start.13 = (bf16[32,2304]{1,0:T(8,128)(2,1)}, bf16[32,2304]{1,0:T(8,128)(2,1)S(1)}, u32[]{:S(2)}, u32[]{:S(2)}) collective-permute-start(bf16[32,2304]{1,0:T(8,128)(2,1)} %get-tuple-element.36), channel_id=1, source_target_pairs={{0,24},{8,0},{16,8},{24,16},{1,25},{9,1},{17,9},{25,17},{2,26},{10... | collective-permute-start | bytes 442376 | tf_op jit(solution)/shard_map/ppermute | solution.py:207
  15.9 6.8 %collective-permute-start.11 = (bf16[32,2304]{1,0:T(8,128)(2,1)}, bf16[32,2304]{1,0:T(8,128)(2,1)S(1)}, u32[]{:S(2)}, u32[]{:S(2)}) collective-permute-start(bf16[32,2304]{1,0:T(8,128)(2,1)} %get-tuple-element.36), channel_id=1, source_target_pairs={{0,8},{8,16},{16,24},{24,0},{1,9},{9,17},{17,25},{25,1},{2,10},{10... | collective-permute-start | bytes 442376 | tf_op jit(solution)/shard_map/ppermute | solution.py:207
  24.6 29.7 %all-to-all-start = ((bf16[64,24,128]{2,1,0:T(8,128)(2,1)}), bf16[64,24,128]{2,1,0:T(8,128)(2,1)S(1)}, u32[]{:S(2)}, u32[]{:S(2)}) async-start(bf16[64,24,128]{2,1,0:T(8,128)(2,1)} %get-tuple-element.27), calls=%async_computation | async-start | bytes 786432 | tf_op jit(solution)/shard_map/all_to_all | solution.py:252
  54.2 0.8 copy-start
  56.8 20.9 %all-to-all-start.1 = ((bf16[64,16,128]{2,1,0:T(8,128)(2,1)}), bf16[64,16,128]{2,1,0:T(8,128)(2,1)S(1)}, u32[]{:S(2)}, u32[]{:S(2)}) async-start(bf16[64,16,128]{2,1,0:T(8,128)(2,1)} %block_scan.1), calls=%async_computation.1 | async-start | bytes 524288 | tf_op jit(solution)/shard_map/all_to_all | solution.py:270
  77.7 0.7 copy-start.1
  78.4 6.5 %copy-start.9 = (bf16[2048]{0:T(1024)(128)(2,1)S(1)}, bf16[2048]{0:T(1024)(128)(2,1)}, u32[]{:S(2)}) copy-start(bf16[2048]{0:T(1024)(128)(2,1)} %param.22) | copy-start | bytes 12292
  82.0 6.6 %collective-permute-start = (bf16[32,2048]{1,0:T(8,128)(2,1)}, bf16[32,2048]{1,0:T(8,128)(2,1)S(1)}, u32[]{:S(2)}, u32[]{:S(2)}) collective-permute-start(bf16[32,2048]{1,0:T(8,128)(2,1)} %get-tuple-element.29), channel_id=1, source_target_pairs={{0,1},{1,2},{2,3},{3,0},{4,5},{5,6},{6,7},{7,4},{8,9},{9,10},{10,1... | collective-permute-start | bytes 393224 | tf_op jit(solution)/shard_map/ppermute | solution.py:207
  82.4 8.0 %collective-permute-start.1 = (bf16[32,2048]{1,0:T(8,128)(2,1)}, bf16[32,2048]{1,0:T(8,128)(2,1)S(1)}, u32[]{:S(2)}, u32[]{:S(2)}) collective-permute-start(bf16[32,2048]{1,0:T(8,128)(2,1)} %get-tuple-element.30), channel_id=1, source_target_pairs={{0,2},{1,3},{2,0},{3,1},{4,6},{5,7},{6,4},{7,5},{8,10},{9,11},{10,... | collective-permute-start | bytes 393224 | tf_op jit(solution)/shard_map/ppermute | solution.py:207
  84.9 7.5 %collective-permute-start.2 = (bf16[32,2048]{1,0:T(8,128)(2,1)}, bf16[32,2048]{1,0:T(8,128)(2,1)S(1)}, u32[]{:S(2)}, u32[]{:S(2)}) collective-permute-start(bf16[32,2048]{1,0:T(8,128)(2,1)} %get-tuple-element.31), channel_id=1, source_target_pairs={{0,3},{1,0},{2,1},{3,2},{4,7},{5,4},{6,5},{7,6},{8,11},{9,8},{10,9... | collective-permute-start | bytes 393224 | tf_op jit(solution)/shard_map/ppermute | solution.py:207
  93.7 5.9 %collective-permute-start.5 = (bf16[32,1024]{1,0:T(8,128)(2,1)S(1)}, bf16[32,1024]{1,0:T(8,128)(2,1)S(1)}, u32[]{:S(2)}, u32[]{:S(2)}) collective-permute-start(bf16[32,1024]{1,0:T(8,128)(2,1)S(1)} %get-tuple-element.53), channel_id=1, source_target_pairs={{0,3},{1,0},{2,1},{3,2},{4,7},{5,4},{6,5},{7,6},{8,11},{9,8},{10,9... | collective-permute-start | bytes 196616 | tf_op jit(solution)/shard_map/ppermute | solution.py:207
  94.7 5.8 %collective-permute-start.4 = (bf16[32,1024]{1,0:T(8,128)(2,1)S(1)}, bf16[32,1024]{1,0:T(8,128)(2,1)S(1)}, u32[]{:S(2)}, u32[]{:S(2)}) collective-permute-start(bf16[32,1024]{1,0:T(8,128)(2,1)S(1)} %get-tuple-element.53), channel_id=1, source_target_pairs={{0,2},{1,3},{2,0},{3,1},{4,6},{5,7},{6,4},{7,5},{8,10},{9,11},{10,... | collective-permute-start | bytes 196616 | tf_op jit(solution)/shard_map/ppermute | solution.py:207
  96.2 4.6 %collective-permute-start.3 = (bf16[32,1024]{1,0:T(8,128)(2,1)S(1)}, bf16[32,1024]{1,0:T(8,128)(2,1)S(1)}, u32[]{:S(2)}, u32[]{:S(2)}) collective-permute-start(bf16[32,1024]{1,0:T(8,128)(2,1)S(1)} %get-tuple-element.53), channel_id=1, source_target_pairs={{0,1},{1,2},{2,3},{3,0},{4,5},{5,6},{6,7},{7,4},{8,9},{9,10},{10,1... | collective-permute-start | bytes 196616 | tf_op jit(solution)/shard_map/ppermute | solution.py:207
  98.1 4.7 %collective-permute-start.7 = (bf16[32,1024]{1,0:T(8,128)(2,1)S(1)}, bf16[32,1024]{1,0:T(8,128)(2,1)S(1)}, u32[]{:S(2)}, u32[]{:S(2)}) collective-permute-start(bf16[32,1024]{1,0:T(8,128)(2,1)S(1)} %get-tuple-element.52), channel_id=1, source_target_pairs={{0,8},{8,0},{16,24},{24,16},{1,9},{9,1},{17,25},{25,17},{2,10},{10... | collective-permute-start | bytes 196616 | tf_op jit(solution)/shard_map/ppermute | solution.py:297
  100.8 11.0 %copy-start.2 = (bf16[128,1024]{1,0:T(8,128)(2,1)}, bf16[128,1024]{1,0:T(8,128)(2,1)S(1)}, u32[]{:S(2)}) copy-start(bf16[128,1024]{1,0:T(8,128)(2,1)S(1)} %pad_maximum_fusion.1.refs_1_) | copy-start | bytes 786436
  100.9 11.0 %collective-permute-start.6 = (bf16[128,1024]{1,0:T(8,128)(2,1)S(1)}, bf16[128,1024]{1,0:T(8,128)(2,1)S(1)}, u32[]{:S(2)}, u32[]{:S(2)}) collective-permute-start(bf16[128,1024]{1,0:T(8,128)(2,1)S(1)} %pad_maximum_fusion.1.refs_1_), channel_id=1, source_target_pairs={{0,8},{8,0},{16,24},{24,16},{1,9},{9,1},{17,25},{25,17},{2,10},{10... | collective-permute-start | bytes 786440 | tf_op jit(solution)/shard_map/ppermute | solution.py:299
  102.8 9.0 %copy-start.3 = (bf16[64,1024]{1,0:T(8,128)(2,1)}, bf16[64,1024]{1,0:T(8,128)(2,1)S(1)}, u32[]{:S(2)}) copy-start(bf16[64,1024]{1,0:T(8,128)(2,1)S(1)} %pad_maximum_fusion.2.refs_3_) | copy-start | bytes 393220
  102.9 6.5 %collective-permute-start.10 = (bf16[64,1024]{1,0:T(8,128)(2,1)S(1)}, bf16[64,1024]{1,0:T(8,128)(2,1)S(1)}, u32[]{:S(2)}, u32[]{:S(2)}) collective-permute-start(bf16[64,1024]{1,0:T(8,128)(2,1)S(1)} %pad_maximum_fusion.2.refs_3_), channel_id=1, source_target_pairs={{0,3},{1,0},{2,1},{3,2},{4,7},{5,4},{6,5},{7,6},{8,11},{9,8},{10,9... | collective-permute-start | bytes 393224 | tf_op jit(solution)/shard_map/ppermute | solution.py:207
  104.0 7.3 %collective-permute-start.9 = (bf16[64,1024]{1,0:T(8,128)(2,1)S(1)}, bf16[64,1024]{1,0:T(8,128)(2,1)S(1)}, u32[]{:S(2)}, u32[]{:S(2)}) collective-permute-start(bf16[64,1024]{1,0:T(8,128)(2,1)S(1)} %pad_maximum_fusion.2.refs_3_), channel_id=1, source_target_pairs={{0,2},{1,3},{2,0},{3,1},{4,6},{5,7},{6,4},{7,5},{8,10},{9,11},{10,... | collective-permute-start | bytes 393224 | tf_op jit(solution)/shard_map/ppermute | solution.py:207
  106.9 5.0 %collective-permute-start.8 = (bf16[64,1024]{1,0:T(8,128)(2,1)S(1)}, bf16[64,1024]{1,0:T(8,128)(2,1)S(1)}, u32[]{:S(2)}, u32[]{:S(2)}) collective-permute-start(bf16[64,1024]{1,0:T(8,128)(2,1)S(1)} %pad_maximum_fusion.2.refs_3_), channel_id=1, source_target_pairs={{0,1},{1,2},{2,3},{3,0},{4,5},{5,6},{6,7},{7,4},{8,9},{9,10},{10,1... | collective-permute-start | bytes 393224 | tf_op jit(solution)/shard_map/ppermute | solution.py:207
  109.4 2.5 %copy-start.6 = (bf16[64,1024]{1,0:T(8,128)(2,1)}, bf16[64,1024]{1,0:T(8,128)(2,1)S(1)}, u32[]{:S(2)}) copy-start(bf16[64,1024]{1,0:T(8,128)(2,1)S(1)} %collective-permute-done.10.refs_6_) | copy-start | bytes 393220
  111.2 0.7 copy-start.7
  111.8 0.7 copy-start.8
  111.8 0.8 copy-start.5
  120.0 11.7 %copy-start.4 = (f32[128,1024]{1,0:T(8,128)S(1)}, f32[128,1024]{1,0:T(8,128)}, u32[]{:S(2)}) copy-start(f32[128,1024]{1,0:T(8,128)} %get-tuple-element.41) | copy-start | bytes 1572868
  120.0 6.5 %collective-permute-start.14 = (bf16[64,1024]{1,0:T(8,128)(2,1)}, bf16[64,1024]{1,0:T(8,128)(2,1)S(1)}, u32[]{:S(2)}, u32[]{:S(2)}) collective-permute-start(bf16[64,1024]{1,0:T(8,128)(2,1)} %get-tuple-element.38), channel_id=1, source_target_pairs={{0,3},{1,0},{2,1},{3,2},{4,7},{5,4},{6,5},{7,6},{8,11},{9,8},{10,9... | collective-permute-start | bytes 393224 | tf_op jit(solution)/shard_map/ppermute | solution.py:207
  121.3 7.2 %collective-permute-start.15 = (bf16[64,1024]{1,0:T(8,128)(2,1)}, bf16[64,1024]{1,0:T(8,128)(2,1)S(1)}, u32[]{:S(2)}, u32[]{:S(2)}) collective-permute-start(bf16[64,1024]{1,0:T(8,128)(2,1)} %get-tuple-element.39), channel_id=1, source_target_pairs={{0,2},{1,3},{2,0},{3,1},{4,6},{5,7},{6,4},{7,5},{8,10},{9,11},{10,... | collective-permute-start | bytes 393224 | tf_op jit(solution)/shard_map/ppermute | solution.py:207
  123.9 5.2 %collective-permute-start.16 = (bf16[64,1024]{1,0:T(8,128)(2,1)}, bf16[64,1024]{1,0:T(8,128)(2,1)S(1)}, u32[]{:S(2)}, u32[]{:S(2)}) collective-permute-start(bf16[64,1024]{1,0:T(8,128)(2,1)} %get-tuple-element.40), channel_id=1, source_target_pairs={{0,1},{1,2},{2,3},{3,0},{4,5},{5,6},{6,7},{7,4},{8,9},{9,10},{10,1... | collective-permute-start | bytes 393224 | tf_op jit(solution)/shard_map/ppermute | solution.py:207
  124.5 7.2 %collective-permute-start.18 = (bf16[128,1024]{1,0:T(8,128)(2,1)}, bf16[128,1024]{1,0:T(8,128)(2,1)S(1)}, u32[]{:S(2)}, u32[]{:S(2)}) collective-permute-start(bf16[128,1024]{1,0:T(8,128)(2,1)} %get-tuple-element.42), channel_id=1, source_target_pairs={{0,8},{8,0},{16,24},{24,16},{1,9},{9,1},{17,25},{25,17},{2,10},{10... | collective-permute-start | bytes 786440 | tf_op jit(solution)/shard_map/ppermute | solution.py:317
  130.2 5.5 %collective-permute-start.17 = (bf16[32,1024]{1,0:T(8,128)(2,1)S(1)}, bf16[32,1024]{1,0:T(8,128)(2,1)S(1)}, u32[]{:S(2)}, u32[]{:S(2)}) collective-permute-start(bf16[32,1024]{1,0:T(8,128)(2,1)S(1)} %slice.71), channel_id=1, source_target_pairs={{0,8},{8,0},{16,24},{24,16},{1,9},{9,1},{17,25},{25,17},{2,10},{10... | collective-permute-start | bytes 196616 | tf_op jit(solution)/shard_map/ppermute | solution.py:326
  131.8 5.6 %collective-permute-start.19 = (bf16[32,1024]{1,0:T(8,128)(2,1)S(1)}, bf16[32,1024]{1,0:T(8,128)(2,1)S(1)}, u32[]{:S(2)}, u32[]{:S(2)}) collective-permute-start(bf16[32,1024]{1,0:T(8,128)(2,1)S(1)} %get-tuple-element.47), channel_id=1, source_target_pairs={{0,3},{1,0},{2,1},{3,2},{4,7},{5,4},{6,5},{7,6},{8,11},{9,8},{10,9... | collective-permute-start | bytes 196616 | tf_op jit(solution)/shard_map/ppermute | solution.py:207
  133.0 4.3 %collective-permute-start.21 = (bf16[32,1024]{1,0:T(8,128)(2,1)S(1)}, bf16[32,1024]{1,0:T(8,128)(2,1)S(1)}, u32[]{:S(2)}, u32[]{:S(2)}) collective-permute-start(bf16[32,1024]{1,0:T(8,128)(2,1)S(1)} %get-tuple-element.48), channel_id=1, source_target_pairs={{0,1},{1,2},{2,3},{3,0},{4,5},{5,6},{6,7},{7,4},{8,9},{9,10},{10,1... | collective-permute-start | bytes 196616 | tf_op jit(solution)/shard_map/ppermute | solution.py:207
  135.1 5.8 %collective-permute-start.20 = (bf16[32,1024]{1,0:T(8,128)(2,1)S(1)}, bf16[32,1024]{1,0:T(8,128)(2,1)S(1)}, u32[]{:S(2)}, u32[]{:S(2)}) collective-permute-start(bf16[32,1024]{1,0:T(8,128)(2,1)S(1)} %get-tuple-element.49), channel_id=1, source_target_pairs={{0,2},{1,3},{2,0},{3,1},{4,6},{5,7},{6,4},{7,5},{8,10},{9,11},{10,... | collective-permute-start | bytes 196616 | tf_op jit(solution)/shard_map/ppermute | solution.py:207
Sparse Core Ops, SparseCore 0:
  24.7 75.1 all-gather.1

commit v3 on v2

--- a/solution.py
+++ b/solution.py
@@ -30,7 +30,23 @@
     return high, middle, (rest - middle.astype(F32)).astype(BF16)
 
 
-def local_body(q_ref, f_ref, v_ref, slack_ref, spike_ref, send_ref, near_ref, reach_ref):
+def local_body(
+    parity_ref,
+    q_ref,
+    f_ref,
+    v_ref,
+    slack_ref,
+    spike_ref,
+    w_gate_ref,
+    w_up_ref,
+    w_down_ref,
+    send_ref,
+    near_ref,
+    reach_ref,
+    keep_ref,
+    give_ref,
+):
+    halves_body(parity_ref, w_gate_ref, w_up_ref, w_down_ref, keep_ref, give_ref)
     rows = q_ref.shape[0]
     heads = spike_ref.shape[0]
     chunk = send_ref.shape[1] - 8
@@ -138,33 +154,31 @@
         write(give_ref, 0)
 
 
+def in_order_body(at_ref, whole_ref, weights_ref, sems):
+    _, y_size, cores, _, _ = weights_ref.shape
+    y = at_ref[0]
+    copies = []
+    for c in range(cores):
+        for k in range(y_size):
+            copies.append(
+                pltpu.make_async_copy(
+                    whole_ref.at[:, c, k],
+                    weights_ref.at[:, lax.rem(y + y_size - k, y_size), c],
+                    sems.at[c * y_size + k],
+                )
+            )
+    for copy in copies:
+        copy.start()
+    for copy in copies:
+        copy.wait()
+
+
 def mixer_body(at_ref, *refs, hidden):
-    (own_ref, near_ref), x_refs, whole_ref, outs = refs[:2], refs[2:6], refs[6], refs[7:13]
-    tokens_ref, weights_ref, act_ref, sems = refs[13:]
-    z_size, y_size, cores, _, wide = weights_ref.shape
-    model = tokens_ref.shape[1]
+    (own_ref, near_ref), x_refs, weights_ref, outs = refs[:2], refs[2:6], refs[6], refs[7:13]
+    tokens_ref = refs[13]
+    model, wide = weights_ref.shape
     y = at_ref[0]
-    chunks = 4
-    z_step = z_size // chunks
-    step = model // chunks
     width = wide // 3
-    groups = []
-    for n in range(chunks):
-        z = slice(n * z_step, (n + 1) * z_step)
-        group = []
-        for c in range(cores):
-            for k in range(y_size):
-                group.append(
-                    pltpu.make_async_copy(
-                        whole_ref.at[z, c, k],
-                        weights_ref.at[z, lax.rem(y + y_size - k, y_size), c],
-                        sems.at[(n * cores + c) * y_size + k],
-                    )
-                )
-        groups.append(group)
-    for group in groups:
-        for copy in group:
-            copy.start()
     split = model // 2
     rows = own_ref.shape[0]
     part = rows // len(x_refs)
@@ -173,22 +187,13 @@
     for d, ref in enumerate(x_refs):
         tokens_ref[d * part : (d + 1) * part, split:] = ref[:part]
         tokens_ref[rows + d * part : rows + (d + 1) * part, split:] = ref[part:]
-    weights = weights_ref.reshape(model, wide)
-    for n, group in enumerate(groups):
-        for copy in group:
-            copy.wait()
-        at = slice(n * step, (n + 1) * step)
-        term = jnp.dot(tokens_ref[:, at], weights[at, : 2 * width], preferred_element_type=F32)
-        if n == 0:
-            act_ref[...] = term
-        else:
-            act_ref[...] += term
-    gate, up = act_ref[:, :width], act_ref[:, width:]
+    act = jnp.dot(tokens_ref[...], weights_ref[:, : 2 * width], preferred_element_type=F32)
+    gate, up = act[:, :width], act[:, width:]
     inner = gate * jax.nn.sigmoid(gate) * up
     lane = lax.broadcasted_iota(jnp.int32, inner.shape, 1)
     low = jnp.where(lax.rem(y, 2) == 0, 0, width - hidden // 2)
     inner = jnp.where((lane >= low) & (lane < low + hidden // 2), inner, 0.0).astype(BF16)
-    lowered = nt_dot(inner, weights[:, 2 * width :])
+    lowered = nt_dot(inner, weights_ref[:, 2 * width :])
     for d, out_ref in enumerate(outs[:4]):
         at = slice(d * part, (d + 1) * part)
         out_ref[:part] = lowered[:rows][at, :split].astype(out_ref.dtype)
@@ -236,27 +241,30 @@
     y_at = lax.axis_index("sp_1")
     slab = mixer_gate_weight.shape[0]
     half = (hidden // 2 + HEAD - 1) // HEAD * HEAD
-    send, near, reach = pl.pallas_call(
+    send, near, reach, keep, give = pl.pallas_call(
         local_body,
         out_shape=(
             jax.ShapeDtypeStruct((blocks, chunk + 8, HEAD), BF16),
             jax.ShapeDtypeStruct((rows, width), F32),
             jax.ShapeDtypeStruct((2, rows, width), BF16),
+            jax.ShapeDtypeStruct((slab, 3 * half), BF16),
+            jax.ShapeDtypeStruct((slab, 3 * half), BF16),
         ),
-        in_specs=[VMEM] * 5,
-        out_specs=(VMEM,) * 3,
+        in_specs=[SMEM] + [VMEM] * 8,
+        out_specs=(VMEM,) * 5,
         name="local_sweep",
-    )(queries, forget_logits, value_matrix, forget_slack[None], spike_log_forget.T)
-    weights = (mixer_gate_weight, mixer_up_weight, mixer_down_weight.T)
-    weights, send = lax.optimization_barrier((weights, send))
+    )(
+        (y_at % 2)[None],
+        queries,
+        forget_logits,
+        value_matrix,
+        forget_slack[None],
+        spike_log_forget.T,
+        mixer_gate_weight,
+        mixer_up_weight,
+        mixer_down_weight.T,
+    )
     got = lax.all_to_all(send, SP, 0, 0, tiled=True)
-    keep, give = pl.pallas_call(
-        halves_body,
-        out_shape=(jax.ShapeDtypeStruct((slab, 3 * half), BF16),) * 2,
-        in_specs=[SMEM] + [VMEM] * 3,
-        out_specs=(VMEM,) * 2,
-        name="weight_halves",
-    )((y_at % 2)[None], *weights)
     line = [keep] + [shift(give if d % 2 else keep, "sp_1", d) for d in range(1, y_size)]
     line = jnp.concatenate(line, axis=0)
     whole = lax.all_gather(line, ("sp_0", "sp_2"), axis=0, tiled=True).reshape(z_size, cores, y_size, slab, 3 * half)
@@ -265,6 +273,7 @@
         out_shape=jax.ShapeDtypeStruct((blocks, chunk, HEAD), BF16),
         in_specs=[SMEM, VMEM],
         out_specs=VMEM,
+        compiler_params=pltpu.CompilerParams(vmem_limit_bytes=12 * 1024 * 1024),
         name="block_scan",
     )((sp_at >= blocks // 2).astype(jnp.int32)[None], got)
     enter = lax.all_to_all(give, SP, 0, 0, tiled=True).reshape(2 * heads, HEAD, HEAD)
@@ -296,24 +305,29 @@
     left, right = normed[:, :split], normed[:, split:]
     both = jnp.concatenate([right, lax.ppermute(right, "sp_1", swap)], axis=0)
     own = jnp.concatenate([left] + [shift(left, "tp", d) for d in range(1, n_tp)], axis=0)
-    tokens = [own, lax.ppermute(own, "sp_1", swap)]
-    tokens += [both] + [shift(both, "tp", d) for d in range(1, n_tp)]
+    lines = [both] + [shift(both, "tp", d) for d in range(1, n_tp)]
+    tokens = [own, lax.ppermute(own, "sp_1", swap)] + lines
+    weights = pl.pallas_call(
+        in_order_body,
+        out_shape=jax.ShapeDtypeStruct((z_size, y_size, cores, slab, 3 * half), BF16),
+        in_specs=[SMEM, ANY],
+        out_specs=VMEM,
+        scratch_shapes=[pltpu.SemaphoreType.DMA((y_size * cores,))],
+        compiler_params=pltpu.CompilerParams(vmem_limit_bytes=40 * 1024 * 1024),
+        name="weights_in_order",
+    )(y_at[None], whole)
+    weights = weights.reshape(model, 3 * half)
     lowered = pl.pallas_call(
         lambda *refs: mixer_body(*refs, hidden=hidden),
         out_shape=(jax.ShapeDtypeStruct((2 * part, split), F32),)
         + (jax.ShapeDtypeStruct((2 * part, split), BF16),) * (n_tp - 1)
         + (jax.ShapeDtypeStruct((rows, split), F32), jax.ShapeDtypeStruct((rows, split), BF16)),
-        in_specs=[SMEM] + [VMEM] * len(tokens) + [ANY],
+        in_specs=[SMEM] + [VMEM] * (len(tokens) + 1),
         out_specs=(VMEM,) * (n_tp + 2),
-        scratch_shapes=[
-            pltpu.VMEM((2 * rows, model), BF16),
-            pltpu.VMEM((z_size, y_size, cores, slab, 3 * half), BF16),
-            pltpu.VMEM((2 * rows, 2 * half), F32),
-            pltpu.SemaphoreType.DMA((4 * y_size * cores,)),
-        ],
-        compiler_params=pltpu.CompilerParams(vmem_limit_bytes=54 * 1024 * 1024),
+        scratch_shapes=[pltpu.VMEM((2 * rows, model), BF16)],
+        compiler_params=pltpu.CompilerParams(vmem_limit_bytes=24 * 1024 * 1024),
         name="channel_mixer",
-    )(y_at[None], *tokens, whole)
+    )(y_at[None], *tokens, weights)
     crossed = lax.ppermute(lowered[n_tp + 1], "sp_1", swap)
     sums = lowered[0]
     for d in range(1, n_tp):

time: 149 us -> 139 us (0.933)
  waiting for transfers between devices: 60.9 us -> 57.1 us
  Pallas kernels: 17.9 us -> 14.4 us
    pallas_call x1, Pallas kernels: 7.38 us -> 2.67 us  [local(): pl.pallas_call(lambda *refs: mixer_body(*refs, hidden=hidden), out_shape=...]
    ppermute x18, waiting for transfers between devices: 27 us -> 23.1 us  [shift(): lax.ppermute(array, axis, [(k, (k + by) % size) for k in range(size)])]
    pallas_call x1, Pallas kernels: 1.72 us -> 3.78 us  [local(): pl.pallas_call(in_order_body, out_shape=jax.ShapeDtypeStruct((z_size, y_s...]
  transfers between devices with their start and end apart: 25 -> 25, of which waited for: 19 -> 19; matrix products, arithmetic and copies ran while one was open for 2% -> 1% of each run, Pallas kernels for 4% -> 6%
where the time goes in v3:
time: 139 us
  waiting for transfers between devices  57.1 us (41%)
  starting transfers between devices  48.8 us (35%)
  Pallas kernels  14.4 us (10%)
  between operations  13.5 us (10%)
  other arithmetic  3.94 us (3%)
    ppermute x18, starting transfers between devices, shift(): lax.ppermute(array, axis, [(k, (k + by) % size) for k in range(size)])  25.8 us
    ppermute x18, waiting for transfers between devices, shift(): lax.ppermute(array, axis, [(k, (k + by) % size) for k in range(size)])  23.1 us
    all_to_all x1, waiting for transfers between devices, local(): got = lax.all_to_all(send, SP, 0, 0, tiled=True)  18.1 us
    all_to_all x1, waiting for transfers between devices, local(): lax.all_to_all(give, SP, 0, 0, tiled=True).reshape(2 * heads, HEAD, HEAD)  15.2 us
    all_to_all x1, starting transfers between devices, local(): got = lax.all_to_all(send, SP, 0, 0, tiled=True)  11.5 us
    all_to_all x1, starting transfers between devices, local(): lax.all_to_all(give, SP, 0, 0, tiled=True).reshape(2 * heads, HEAD, HEAD)  5.67 us
    pallas_call x1, Pallas kernels, local(): pl.pallas_call(in_order_body, out_shape=jax.ShapeDtypeStruct((z_size, y_s...  3.78 us
    pallas_call x1, Pallas kernels, local(): pl.pallas_call(local_body, out_shape=(jax.ShapeDtypeStruct((blocks, chunk...  3.56 us
  transfers between devices with their start and end apart: 25, of which 19 were waited for; matrix products, arithmetic and copies ran while one was open for 1% of the time, Pallas kernels for 6%

profile of v3, /device:TPU:6, one launch (start us, length us, event | category | flops | bytes accessed | tf_op | source)
XLA Modules:
  0.0 138.6 jit_solution(7889992360627179588)
XLA Ops:
  6.5 0.0 all-gather.2.cloned.1.call-start
  6.5 3.6 %local_sweep.1 = (bf16[64,24,128]{2,1,0:T(8,128)(2,1)}, f32[128,512]{1,0:T(8,128)}, bf16[2,128,512]{2,1,0:T(8,128)(2,1)}, bf16[32,2304]{1,0:T(8,128)(2,1)}, bf16[32,2304]{1,0:T(8,128)(2,1)}) custom-call(s32[1]{0:T(128)} %bitcast.1.parity_ref, bf16[128,512]{1,0:T(8,128)(2,1)} %q_ref.1, bf16[2,128,512]{2,1,0:T(8,128)(2,1)} %f_ref.1, bf16[128,512]{1,0:T(8,128)(2,1)} %v_ref.1, ...), custom_call_target="tpu_custom_call" | custom-call | tf_op jit(solution)/shard_map/local_sweep/pallas_call | solution.py:244
  10.1 3.2 %collective-permute-start.12 = (bf16[32,2304]{1,0:T(8,128)(2,1)}, bf16[32,2304]{1,0:T(8,128)(2,1)S(1)}, u32[]{:S(2)}, u32[]{:S(2)}) collective-permute-start(bf16[32,2304]{1,0:T(8,128)(2,1)} %get-tuple-element.27), channel_id=1, source_target_pairs={{0,16},{8,24},{16,0},{24,8},{1,17},{9,25},{17,1},{25,9},{2,18},{10... | collective-permute-start | bytes 442376 | tf_op jit(solution)/shard_map/ppermute | solution.py:212
  13.3 1.1 collective-permute-start.13
  14.4 1.0 collective-permute-start.11
  15.3 3.1 %collective-permute-done.12 = bf16[32,2304]{1,0:T(8,128)(2,1)S(1)} collective-permute-done((bf16[32,2304]{1,0:T(8,128)(2,1)}, bf16[32,2304]{1,0:T(8,128)(2,1)S(1)}, u32[]{:S(2)}, u32[]{:S(2)}) %collective-permute-start.12) | collective-permute-done | bytes 147488 | tf_op jit(solution)/shard_map/ppermute | solution.py:212
  18.4 2.5 %collective-permute-done.13 = bf16[32,2304]{1,0:T(8,128)(2,1)S(1)} collective-permute-done((bf16[32,2304]{1,0:T(8,128)(2,1)}, bf16[32,2304]{1,0:T(8,128)(2,1)S(1)}, u32[]{:S(2)}, u32[]{:S(2)}) %collective-permute-start.13) | collective-permute-done | bytes 147488 | tf_op jit(solution)/shard_map/ppermute | solution.py:212
  20.9 0.3 collective-permute-done.11
  21.2 1.8 %pad_maximum_fusion = bf16[128,2304]{1,0:T(8,128)(2,1)} fusion(bf16[32,2304]{1,0:T(8,128)(2,1)S(1)} %collective-permute-done.13, bf16[32,2304]{1,0:T(8,128)(2,1)S(1)} %collective-permute-done.12, bf16[32,2304]{1,0:T(8,128)(2,1)S(1)} %collective-permute-done.11, bf16[32,2304]{1,0:T(8,128)(2,1)} %get-tuple-element.27), kind=kLoop, calls=%fused_computation | loop fusion | flops 2359296 | bytes 1179648 | tf_op jit(solution)/shard_map/concatenate | solution.py:269
  22.9 0.0 all-gather.2.cloned.1.call-update
  23.0 11.5 %all-to-all-start = ((bf16[64,24,128]{2,1,0:T(8,128)(2,1)}), bf16[64,24,128]{2,1,0:T(8,128)(2,1)S(1)}, u32[]{:S(2)}, u32[]{:S(2)}) async-start(bf16[64,24,128]{2,1,0:T(8,128)(2,1)} %get-tuple-element.22), calls=%async_computation | async-start | bytes 786432 | tf_op jit(solution)/shard_map/all_to_all | solution.py:267
  34.5 18.1 %all-to-all-done.got_ref = bf16[64,24,128]{2,1,0:T(8,128)(2,1)S(1)} async-done(((bf16[64,24,128]{2,1,0:T(8,128)(2,1)}), bf16[64,24,128]{2,1,0:T(8,128)(2,1)S(1)}, u32[]{:S(2)}, u32[]{:S(2)}) %all-to-all-start) | async-done | bytes 393248 | tf_op jit(solution)/shard_map/all_to_all | solution.py:267
  52.6 0.9 block_scan.1
  53.5 5.7 %all-to-all-start.1 = ((bf16[64,16,128]{2,1,0:T(8,128)(2,1)}), bf16[64,16,128]{2,1,0:T(8,128)(2,1)S(1)}, u32[]{:S(2)}, u32[]{:S(2)}) async-start(bf16[64,16,128]{2,1,0:T(8,128)(2,1)} %block_scan.1), calls=%async_computation.1 | async-start | bytes 524288 | tf_op jit(solution)/shard_map/all_to_all | solution.py:279
  59.2 15.2 %all-to-all-done.1 = bf16[64,16,128]{2,1,0:T(8,128)(2,1)S(1)} async-done(((bf16[64,16,128]{2,1,0:T(8,128)(2,1)}), bf16[64,16,128]{2,1,0:T(8,128)(2,1)S(1)}, u32[]{:S(2)}, u32[]{:S(2)}) %all-to-all-start.1) | async-done | bytes 262176 | tf_op jit(solution)/shard_map/all_to_all | solution.py:279
  74.4 0.7 copy-done
  75.1 3.6 %norm_project.1 = (bf16[32,2048]{1,0:T(8,128)(2,1)}, bf16[32,2048]{1,0:T(8,128)(2,1)}, bf16[32,2048]{1,0:T(8,128)(2,1)}, bf16[32,2048]{1,0:T(8,128)(2,1)}) custom-call(s32[1]{0:T(128)} %bitcast.own_ref, f32[128,512]{1,0:T(8,128)} %get-tuple-element.20.near_ref, bf16[2,128,512]{2,1,0:T(8,128)(2,1)} %get-tuple-element.21.reach_ref, ...), custom_call_target="tpu_custom_call" | custom-call | tf_op jit(solution)/shard_map/norm_project/pallas_call | solution.py:282
  78.6 0.5 collective-permute-start
  79.1 2.4 %collective-permute-start.1 = (bf16[32,2048]{1,0:T(8,128)(2,1)}, bf16[32,2048]{1,0:T(8,128)(2,1)S(1)}, u32[]{:S(2)}, u32[]{:S(2)}) collective-permute-start(bf16[32,2048]{1,0:T(8,128)(2,1)} %get-tuple-element.25), channel_id=1, source_target_pairs={{0,2},{1,3},{2,0},{3,1},{4,6},{5,7},{6,4},{7,5},{8,10},{9,11},{10,... | collective-permute-start | bytes 393224 | tf_op jit(solution)/shard_map/ppermute | solution.py:212
  81.5 0.0 collective-permute-start.2
  81.5 0.0 copy-done.1
  81.5 3.7 %collective-permute-done = bf16[32,2048]{1,0:T(8,128)(2,1)S(1)} collective-permute-done((bf16[32,2048]{1,0:T(8,128)(2,1)}, bf16[32,2048]{1,0:T(8,128)(2,1)S(1)}, u32[]{:S(2)}, u32[]{:S(2)}) %collective-permute-start) | collective-permute-done | bytes 131104 | tf_op jit(solution)/shard_map/ppermute | solution.py:212
  85.2 1.9 %collective-permute-done.1 = bf16[32,2048]{1,0:T(8,128)(2,1)S(1)} collective-permute-done((bf16[32,2048]{1,0:T(8,128)(2,1)}, bf16[32,2048]{1,0:T(8,128)(2,1)S(1)}, u32[]{:S(2)}, u32[]{:S(2)}) %collective-permute-start.1) | collective-permute-done | bytes 131104 | tf_op jit(solution)/shard_map/ppermute | solution.py:212
  87.1 1.9 %collective-permute-done.2 = bf16[32,2048]{1,0:T(8,128)(2,1)S(1)} collective-permute-done((bf16[32,2048]{1,0:T(8,128)(2,1)}, bf16[32,2048]{1,0:T(8,128)(2,1)S(1)}, u32[]{:S(2)}, u32[]{:S(2)}) %collective-permute-start.2) | collective-permute-done | bytes 131104 | tf_op jit(solution)/shard_map/ppermute | solution.py:212
  89.0 1.2 fusion
  90.2 0.1 fusion.2
  90.3 1.1 collective-permute-start.5
  91.4 1.4 %collective-permute-start.4 = (bf16[32,1024]{1,0:T(8,128)(2,1)S(1)}, bf16[32,1024]{1,0:T(8,128)(2,1)S(1)}, u32[]{:S(2)}, u32[]{:S(2)}) collective-permute-start(bf16[32,1024]{1,0:T(8,128)(2,1)S(1)} %get-tuple-element.45), channel_id=1, source_target_pairs={{0,2},{1,3},{2,0},{3,1},{4,6},{5,7},{6,4},{7,5},{8,10},{9,11},{10,... | collective-permute-start | bytes 196616 | tf_op jit(solution)/shard_map/ppermute | solution.py:212
  92.8 1.9 %collective-permute-start.3 = (bf16[32,1024]{1,0:T(8,128)(2,1)S(1)}, bf16[32,1024]{1,0:T(8,128)(2,1)S(1)}, u32[]{:S(2)}, u32[]{:S(2)}) collective-permute-start(bf16[32,1024]{1,0:T(8,128)(2,1)S(1)} %get-tuple-element.45), channel_id=1, source_target_pairs={{0,1},{1,2},{2,3},{3,0},{4,5},{5,6},{6,7},{7,4},{8,9},{9,10},{10,1... | collective-permute-start | bytes 196616 | tf_op jit(solution)/shard_map/ppermute | solution.py:212
  94.8 1.4 %collective-permute-start.7 = (bf16[32,1024]{1,0:T(8,128)(2,1)S(1)}, bf16[32,1024]{1,0:T(8,128)(2,1)S(1)}, u32[]{:S(2)}, u32[]{:S(2)}) collective-permute-start(bf16[32,1024]{1,0:T(8,128)(2,1)S(1)} %get-tuple-element.44), channel_id=1, source_target_pairs={{0,8},{8,0},{16,24},{24,16},{1,9},{9,1},{17,25},{25,17},{2,10},{10... | collective-permute-start | bytes 196616 | tf_op jit(solution)/shard_map/ppermute | solution.py:306
  96.2 0.0 collective-permute-done.5
  96.2 1.0 collective-permute-done.4
  97.2 0.2 collective-permute-done.3
  97.4 1.5 %collective-permute-start.6 = (bf16[128,1024]{1,0:T(8,128)(2,1)S(1)}, bf16[128,1024]{1,0:T(8,128)(2,1)S(1)}, u32[]{:S(2)}, u32[]{:S(2)}) collective-permute-start(bf16[128,1024]{1,0:T(8,128)(2,1)S(1)} %pad_maximum_fusion.1.refs_1_), channel_id=1, source_target_pairs={{0,8},{8,0},{16,24},{24,16},{1,9},{9,1},{17,25},{25,17},{2,10},{10... | collective-permute-start | bytes 786440 | tf_op jit(solution)/shard_map/ppermute | solution.py:309
  99.0 0.5 collective-permute-done.7
  99.4 1.1 collective-permute-start.10
  100.5 3.0 %collective-permute-start.9 = (bf16[64,1024]{1,0:T(8,128)(2,1)S(1)}, bf16[64,1024]{1,0:T(8,128)(2,1)S(1)}, u32[]{:S(2)}, u32[]{:S(2)}) collective-permute-start(bf16[64,1024]{1,0:T(8,128)(2,1)S(1)} %pad_maximum_fusion.2.refs_3_), channel_id=1, source_target_pairs={{0,2},{1,3},{2,0},{3,1},{4,6},{5,7},{6,4},{7,5},{8,10},{9,11},{10,... | collective-permute-start | bytes 393224 | tf_op jit(solution)/shard_map/ppermute | solution.py:212
  103.5 0.7 collective-permute-start.8
  104.2 3.8 %weights_in_order.1 = bf16[8,4,2,32,2304]{4,3,2,1,0:T(8,128)(2,1)S(1)} custom-call(s32[1]{0:T(128)} %bitcast.8.at_ref.refs_0_, bf16[8,2,4,32,2304]{4,3,2,1,0:T(8,128)(2,1)} %bitcast.12), custom_call_target="tpu_custom_call" | custom-call | tf_op jit(solution)/shard_map/weights_in_order/pallas_call | solution.py:310
  108.0 0.0 collective-permute-done.10.refs_6_
  108.0 0.0 collective-permute-done.9.refs_5_
  108.1 0.4 collective-permute-done.8.refs_4_
  108.5 0.0 collective-permute-done.6.refs_2_
  108.5 2.7 %channel_mixer.1 = (f32[64,1024]{1,0:T(8,128)S(1)}, bf16[64,1024]{1,0:T(8,128)(2,1)S(1)}, bf16[64,1024]{1,0:T(8,128)(2,1)S(1)}, bf16[64,1024]{1,0:T(8,128)(2,1)S...) custom-call(s32[1]{0:T(128)} %bitcast.8.at_ref.refs_0_, bf16[128,1024]{1,0:T(8,128)(2,1)S(1)} %pad_maximum_fusion.1.refs_1_, ...), custom_call_target="tpu_custom_call" | custom-call | tf_op jit(solution)/shard_map/channel_mixer/pallas_call | solution.py:320
  111.2 1.0 collective-permute-start.14
  112.2 2.8 %collective-permute-start.15 = (bf16[64,1024]{1,0:T(8,128)(2,1)S(1)}, bf16[64,1024]{1,0:T(8,128)(2,1)S(1)}, u32[]{:S(2)}, u32[]{:S(2)}) collective-permute-start(bf16[64,1024]{1,0:T(8,128)(2,1)S(1)} %get-tuple-element.31), channel_id=1, source_target_pairs={{0,2},{1,3},{2,0},{3,1},{4,6},{5,7},{6,4},{7,5},{8,10},{9,11},{10,... | collective-permute-start | bytes 393224 | tf_op jit(solution)/shard_map/ppermute | solution.py:212
  115.0 0.4 collective-permute-start.16
  115.4 1.4 %collective-permute-start.18 = (bf16[128,1024]{1,0:T(8,128)(2,1)S(1)}, bf16[128,1024]{1,0:T(8,128)(2,1)S(1)}, u32[]{:S(2)}, u32[]{:S(2)}) collective-permute-start(bf16[128,1024]{1,0:T(8,128)(2,1)S(1)} %get-tuple-element.34), channel_id=1, source_target_pairs={{0,8},{8,0},{16,24},{24,16},{1,9},{9,1},{17,25},{25,17},{2,10},{10... | collective-permute-start | bytes 786440 | tf_op jit(solution)/shard_map/ppermute | solution.py:331
  116.8 0.6 collective-permute-done.14
  117.4 1.9 %collective-permute-done.15 = bf16[64,1024]{1,0:T(8,128)(2,1)S(1)} collective-permute-done((bf16[64,1024]{1,0:T(8,128)(2,1)S(1)}, bf16[64,1024]{1,0:T(8,128)(2,1)S(1)}, u32[]{:S(2)}, u32[]{:S(2)}) %collective-permute-start.15) | collective-permute-done | bytes 131104 | tf_op jit(solution)/shard_map/ppermute | solution.py:212
  119.3 0.6 collective-permute-done.16
  120.0 0.1 convert_add_fusion.1
  120.0 1.6 %collective-permute-start.17 = (bf16[32,1024]{1,0:T(8,128)(2,1)S(1)}, bf16[32,1024]{1,0:T(8,128)(2,1)S(1)}, u32[]{:S(2)}, u32[]{:S(2)}) collective-permute-start(bf16[32,1024]{1,0:T(8,128)(2,1)S(1)} %slice.71), channel_id=1, source_target_pairs={{0,8},{8,0},{16,24},{24,16},{1,9},{9,1},{17,25},{25,17},{2,10},{10... | collective-permute-start | bytes 196616 | tf_op jit(solution)/shard_map/ppermute | solution.py:340
  121.6 0.2 collective-permute-done.18
  121.8 0.1 fusion.9
  121.9 1.7 %collective-permute-start.19 = (bf16[32,1024]{1,0:T(8,128)(2,1)S(1)}, bf16[32,1024]{1,0:T(8,128)(2,1)S(1)}, u32[]{:S(2)}, u32[]{:S(2)}) collective-permute-start(bf16[32,1024]{1,0:T(8,128)(2,1)S(1)} %get-tuple-element.39), channel_id=1, source_target_pairs={{0,3},{1,0},{2,1},{3,2},{4,7},{5,4},{6,5},{7,6},{8,11},{9,8},{10,9... | collective-permute-start | bytes 196616 | tf_op jit(solution)/shard_map/ppermute | solution.py:212
  123.6 1.6 %collective-permute-start.21 = (bf16[32,1024]{1,0:T(8,128)(2,1)S(1)}, bf16[32,1024]{1,0:T(8,128)(2,1)S(1)}, u32[]{:S(2)}, u32[]{:S(2)}) collective-permute-start(bf16[32,1024]{1,0:T(8,128)(2,1)S(1)} %get-tuple-element.40), channel_id=1, source_target_pairs={{0,1},{1,2},{2,3},{3,0},{4,5},{5,6},{6,7},{7,4},{8,9},{9,10},{10,1... | collective-permute-start | bytes 196616 | tf_op jit(solution)/shard_map/ppermute | solution.py:212
  125.2 0.8 collective-permute-start.20
  126.0 0.0 collective-permute-done.17
  126.0 1.5 %collective-permute-done.19 = bf16[32,1024]{1,0:T(8,128)(2,1)S(1)} collective-permute-done((bf16[32,1024]{1,0:T(8,128)(2,1)S(1)}, bf16[32,1024]{1,0:T(8,128)(2,1)S(1)}, u32[]{:S(2)}, u32[]{:S(2)}) %collective-permute-start.19) | collective-permute-done | bytes 65568 | tf_op jit(solution)/shard_map/ppermute | solution.py:212
  127.4 0.4 collective-permute-done.21
  127.8 3.1 %collective-permute-done.20 = bf16[32,1024]{1,0:T(8,128)(2,1)S(1)} collective-permute-done((bf16[32,1024]{1,0:T(8,128)(2,1)S(1)}, bf16[32,1024]{1,0:T(8,128)(2,1)S(1)}, u32[]{:S(2)}, u32[]{:S(2)}) %collective-permute-start.20) | collective-permute-done | bytes 65568 | tf_op jit(solution)/shard_map/ppermute | solution.py:212
  131.0 0.1 fusion.8
  131.1 0.7 pad_maximum_fusion.3
  (10 shorter events, 0.1 us)
Async XLA Ops:
  6.5 97.7 %all-gather.2.cloned.1.call-start = ((), (), s32[]{:S(2)}) async-start(), calls=%async_computation.2 | async-start | bytes 10027008 | tf_op jit(solution)/shard_map/all_gather | solution.py:270
  10.1 8.3 %collective-permute-start.12 = (bf16[32,2304]{1,0:T(8,128)(2,1)}, bf16[32,2304]{1,0:T(8,128)(2,1)S(1)}, u32[]{:S(2)}, u32[]{:S(2)}) collective-permute-start(bf16[32,2304]{1,0:T(8,128)(2,1)} %get-tuple-element.27), channel_id=1, source_target_pairs={{0,16},{8,24},{16,0},{24,8},{1,17},{9,25},{17,1},{25,9},{2,18},{10... | collective-permute-start | bytes 442376 | tf_op jit(solution)/shard_map/ppermute | solution.py:212
  13.3 7.6 %collective-permute-start.13 = (bf16[32,2304]{1,0:T(8,128)(2,1)}, bf16[32,2304]{1,0:T(8,128)(2,1)S(1)}, u32[]{:S(2)}, u32[]{:S(2)}) collective-permute-start(bf16[32,2304]{1,0:T(8,128)(2,1)} %get-tuple-element.28), channel_id=1, source_target_pairs={{0,24},{8,0},{16,8},{24,16},{1,25},{9,1},{17,9},{25,17},{2,26},{10... | collective-permute-start | bytes 442376 | tf_op jit(solution)/shard_map/ppermute | solution.py:212
  14.4 6.8 %collective-permute-start.11 = (bf16[32,2304]{1,0:T(8,128)(2,1)}, bf16[32,2304]{1,0:T(8,128)(2,1)S(1)}, u32[]{:S(2)}, u32[]{:S(2)}) collective-permute-start(bf16[32,2304]{1,0:T(8,128)(2,1)} %get-tuple-element.28), channel_id=1, source_target_pairs={{0,8},{8,16},{16,24},{24,0},{1,9},{9,17},{17,25},{25,1},{2,10},{10... | collective-permute-start | bytes 442376 | tf_op jit(solution)/shard_map/ppermute | solution.py:212
  23.0 29.7 %all-to-all-start = ((bf16[64,24,128]{2,1,0:T(8,128)(2,1)}), bf16[64,24,128]{2,1,0:T(8,128)(2,1)S(1)}, u32[]{:S(2)}, u32[]{:S(2)}) async-start(bf16[64,24,128]{2,1,0:T(8,128)(2,1)} %get-tuple-element.22), calls=%async_computation | async-start | bytes 786432 | tf_op jit(solution)/shard_map/all_to_all | solution.py:267
  53.5 20.9 %all-to-all-start.1 = ((bf16[64,16,128]{2,1,0:T(8,128)(2,1)}), bf16[64,16,128]{2,1,0:T(8,128)(2,1)S(1)}, u32[]{:S(2)}, u32[]{:S(2)}) async-start(bf16[64,16,128]{2,1,0:T(8,128)(2,1)} %block_scan.1), calls=%async_computation.1 | async-start | bytes 524288 | tf_op jit(solution)/shard_map/all_to_all | solution.py:279
  74.4 0.7 copy-start
  75.1 6.5 %copy-start.1 = (bf16[2048]{0:T(1024)(128)(2,1)S(1)}, bf16[2048]{0:T(1024)(128)(2,1)}, u32[]{:S(2)}) copy-start(bf16[2048]{0:T(1024)(128)(2,1)} %param.22) | copy-start | bytes 12292
  78.6 6.6 %collective-permute-start = (bf16[32,2048]{1,0:T(8,128)(2,1)}, bf16[32,2048]{1,0:T(8,128)(2,1)S(1)}, u32[]{:S(2)}, u32[]{:S(2)}) collective-permute-start(bf16[32,2048]{1,0:T(8,128)(2,1)} %get-tuple-element.24), channel_id=1, source_target_pairs={{0,1},{1,2},{2,3},{3,0},{4,5},{5,6},{6,7},{7,4},{8,9},{9,10},{10,1... | collective-permute-start | bytes 393224 | tf_op jit(solution)/shard_map/ppermute | solution.py:212
  79.1 8.0 %collective-permute-start.1 = (bf16[32,2048]{1,0:T(8,128)(2,1)}, bf16[32,2048]{1,0:T(8,128)(2,1)S(1)}, u32[]{:S(2)}, u32[]{:S(2)}) collective-permute-start(bf16[32,2048]{1,0:T(8,128)(2,1)} %get-tuple-element.25), channel_id=1, source_target_pairs={{0,2},{1,3},{2,0},{3,1},{4,6},{5,7},{6,4},{7,5},{8,10},{9,11},{10,... | collective-permute-start | bytes 393224 | tf_op jit(solution)/shard_map/ppermute | solution.py:212
  81.5 7.5 %collective-permute-start.2 = (bf16[32,2048]{1,0:T(8,128)(2,1)}, bf16[32,2048]{1,0:T(8,128)(2,1)S(1)}, u32[]{:S(2)}, u32[]{:S(2)}) collective-permute-start(bf16[32,2048]{1,0:T(8,128)(2,1)} %get-tuple-element.26), channel_id=1, source_target_pairs={{0,3},{1,0},{2,1},{3,2},{4,7},{5,4},{6,5},{7,6},{8,11},{9,8},{10,9... | collective-permute-start | bytes 393224 | tf_op jit(solution)/shard_map/ppermute | solution.py:212
  90.3 5.9 %collective-permute-start.5 = (bf16[32,1024]{1,0:T(8,128)(2,1)S(1)}, bf16[32,1024]{1,0:T(8,128)(2,1)S(1)}, u32[]{:S(2)}, u32[]{:S(2)}) collective-permute-start(bf16[32,1024]{1,0:T(8,128)(2,1)S(1)} %get-tuple-element.45), channel_id=1, source_target_pairs={{0,3},{1,0},{2,1},{3,2},{4,7},{5,4},{6,5},{7,6},{8,11},{9,8},{10,9... | collective-permute-start | bytes 196616 | tf_op jit(solution)/shard_map/ppermute | solution.py:212
  91.4 5.8 %collective-permute-start.4 = (bf16[32,1024]{1,0:T(8,128)(2,1)S(1)}, bf16[32,1024]{1,0:T(8,128)(2,1)S(1)}, u32[]{:S(2)}, u32[]{:S(2)}) collective-permute-start(bf16[32,1024]{1,0:T(8,128)(2,1)S(1)} %get-tuple-element.45), channel_id=1, source_target_pairs={{0,2},{1,3},{2,0},{3,1},{4,6},{5,7},{6,4},{7,5},{8,10},{9,11},{10,... | collective-permute-start | bytes 196616 | tf_op jit(solution)/shard_map/ppermute | solution.py:212
  92.8 4.6 %collective-permute-start.3 = (bf16[32,1024]{1,0:T(8,128)(2,1)S(1)}, bf16[32,1024]{1,0:T(8,128)(2,1)S(1)}, u32[]{:S(2)}, u32[]{:S(2)}) collective-permute-start(bf16[32,1024]{1,0:T(8,128)(2,1)S(1)} %get-tuple-element.45), channel_id=1, source_target_pairs={{0,1},{1,2},{2,3},{3,0},{4,5},{5,6},{6,7},{7,4},{8,9},{9,10},{10,1... | collective-permute-start | bytes 196616 | tf_op jit(solution)/shard_map/ppermute | solution.py:212
  94.8 4.6 %collective-permute-start.7 = (bf16[32,1024]{1,0:T(8,128)(2,1)S(1)}, bf16[32,1024]{1,0:T(8,128)(2,1)S(1)}, u32[]{:S(2)}, u32[]{:S(2)}) collective-permute-start(bf16[32,1024]{1,0:T(8,128)(2,1)S(1)} %get-tuple-element.44), channel_id=1, source_target_pairs={{0,8},{8,0},{16,24},{24,16},{1,9},{9,1},{17,25},{25,17},{2,10},{10... | collective-permute-start | bytes 196616 | tf_op jit(solution)/shard_map/ppermute | solution.py:306
  97.4 11.0 %collective-permute-start.6 = (bf16[128,1024]{1,0:T(8,128)(2,1)S(1)}, bf16[128,1024]{1,0:T(8,128)(2,1)S(1)}, u32[]{:S(2)}, u32[]{:S(2)}) collective-permute-start(bf16[128,1024]{1,0:T(8,128)(2,1)S(1)} %pad_maximum_fusion.1.refs_1_), channel_id=1, source_target_pairs={{0,8},{8,0},{16,24},{24,16},{1,9},{9,1},{17,25},{25,17},{2,10},{10... | collective-permute-start | bytes 786440 | tf_op jit(solution)/shard_map/ppermute | solution.py:309
  99.4 8.6 %collective-permute-start.10 = (bf16[64,1024]{1,0:T(8,128)(2,1)S(1)}, bf16[64,1024]{1,0:T(8,128)(2,1)S(1)}, u32[]{:S(2)}, u32[]{:S(2)}) collective-permute-start(bf16[64,1024]{1,0:T(8,128)(2,1)S(1)} %pad_maximum_fusion.2.refs_3_), channel_id=1, source_target_pairs={{0,3},{1,0},{2,1},{3,2},{4,7},{5,4},{6,5},{7,6},{8,11},{9,8},{10,9... | collective-permute-start | bytes 393224 | tf_op jit(solution)/shard_map/ppermute | solution.py:212
  100.5 7.5 %collective-permute-start.9 = (bf16[64,1024]{1,0:T(8,128)(2,1)S(1)}, bf16[64,1024]{1,0:T(8,128)(2,1)S(1)}, u32[]{:S(2)}, u32[]{:S(2)}) collective-permute-start(bf16[64,1024]{1,0:T(8,128)(2,1)S(1)} %pad_maximum_fusion.2.refs_3_), channel_id=1, source_target_pairs={{0,2},{1,3},{2,0},{3,1},{4,6},{5,7},{6,4},{7,5},{8,10},{9,11},{10,... | collective-permute-start | bytes 393224 | tf_op jit(solution)/shard_map/ppermute | solution.py:212
  103.5 5.0 %collective-permute-start.8 = (bf16[64,1024]{1,0:T(8,128)(2,1)S(1)}, bf16[64,1024]{1,0:T(8,128)(2,1)S(1)}, u32[]{:S(2)}, u32[]{:S(2)}) collective-permute-start(bf16[64,1024]{1,0:T(8,128)(2,1)S(1)} %pad_maximum_fusion.2.refs_3_), channel_id=1, source_target_pairs={{0,1},{1,2},{2,3},{3,0},{4,5},{5,6},{6,7},{7,4},{8,9},{9,10},{10,1... | collective-permute-start | bytes 393224 | tf_op jit(solution)/shard_map/ppermute | solution.py:212
  111.2 6.3 %collective-permute-start.14 = (bf16[64,1024]{1,0:T(8,128)(2,1)S(1)}, bf16[64,1024]{1,0:T(8,128)(2,1)S(1)}, u32[]{:S(2)}, u32[]{:S(2)}) collective-permute-start(bf16[64,1024]{1,0:T(8,128)(2,1)S(1)} %get-tuple-element.30), channel_id=1, source_target_pairs={{0,3},{1,0},{2,1},{3,2},{4,7},{5,4},{6,5},{7,6},{8,11},{9,8},{10,9... | collective-permute-start | bytes 393224 | tf_op jit(solution)/shard_map/ppermute | solution.py:212
  112.2 7.2 %collective-permute-start.15 = (bf16[64,1024]{1,0:T(8,128)(2,1)S(1)}, bf16[64,1024]{1,0:T(8,128)(2,1)S(1)}, u32[]{:S(2)}, u32[]{:S(2)}) collective-permute-start(bf16[64,1024]{1,0:T(8,128)(2,1)S(1)} %get-tuple-element.31), channel_id=1, source_target_pairs={{0,2},{1,3},{2,0},{3,1},{4,6},{5,7},{6,4},{7,5},{8,10},{9,11},{10,... | collective-permute-start | bytes 393224 | tf_op jit(solution)/shard_map/ppermute | solution.py:212
  115.0 5.0 %collective-permute-start.16 = (bf16[64,1024]{1,0:T(8,128)(2,1)S(1)}, bf16[64,1024]{1,0:T(8,128)(2,1)S(1)}, u32[]{:S(2)}, u32[]{:S(2)}) collective-permute-start(bf16[64,1024]{1,0:T(8,128)(2,1)S(1)} %get-tuple-element.32), channel_id=1, source_target_pairs={{0,1},{1,2},{2,3},{3,0},{4,5},{5,6},{6,7},{7,4},{8,9},{9,10},{10,1... | collective-permute-start | bytes 393224 | tf_op jit(solution)/shard_map/ppermute | solution.py:212
  115.4 6.4 %collective-permute-start.18 = (bf16[128,1024]{1,0:T(8,128)(2,1)S(1)}, bf16[128,1024]{1,0:T(8,128)(2,1)S(1)}, u32[]{:S(2)}, u32[]{:S(2)}) collective-permute-start(bf16[128,1024]{1,0:T(8,128)(2,1)S(1)} %get-tuple-element.34), channel_id=1, source_target_pairs={{0,8},{8,0},{16,24},{24,16},{1,9},{9,1},{17,25},{25,17},{2,10},{10... | collective-permute-start | bytes 786440 | tf_op jit(solution)/shard_map/ppermute | solution.py:331
  120.0 5.9 %collective-permute-start.17 = (bf16[32,1024]{1,0:T(8,128)(2,1)S(1)}, bf16[32,1024]{1,0:T(8,128)(2,1)S(1)}, u32[]{:S(2)}, u32[]{:S(2)}) collective-permute-start(bf16[32,1024]{1,0:T(8,128)(2,1)S(1)} %slice.71), channel_id=1, source_target_pairs={{0,8},{8,0},{16,24},{24,16},{1,9},{9,1},{17,25},{25,17},{2,10},{10... | collective-permute-start | bytes 196616 | tf_op jit(solution)/shard_map/ppermute | solution.py:340
  121.9 5.6 %collective-permute-start.19 = (bf16[32,1024]{1,0:T(8,128)(2,1)S(1)}, bf16[32,1024]{1,0:T(8,128)(2,1)S(1)}, u32[]{:S(2)}, u32[]{:S(2)}) collective-permute-start(bf16[32,1024]{1,0:T(8,128)(2,1)S(1)} %get-tuple-element.39), channel_id=1, source_target_pairs={{0,3},{1,0},{2,1},{3,2},{4,7},{5,4},{6,5},{7,6},{8,11},{9,8},{10,9... | collective-permute-start | bytes 196616 | tf_op jit(solution)/shard_map/ppermute | solution.py:212
  123.6 4.3 %collective-permute-start.21 = (bf16[32,1024]{1,0:T(8,128)(2,1)S(1)}, bf16[32,1024]{1,0:T(8,128)(2,1)S(1)}, u32[]{:S(2)}, u32[]{:S(2)}) collective-permute-start(bf16[32,1024]{1,0:T(8,128)(2,1)S(1)} %get-tuple-element.40), channel_id=1, source_target_pairs={{0,1},{1,2},{2,3},{3,0},{4,5},{5,6},{6,7},{7,4},{8,9},{9,10},{10,1... | collective-permute-start | bytes 196616 | tf_op jit(solution)/shard_map/ppermute | solution.py:212
  125.2 5.8 %collective-permute-start.20 = (bf16[32,1024]{1,0:T(8,128)(2,1)S(1)}, bf16[32,1024]{1,0:T(8,128)(2,1)S(1)}, u32[]{:S(2)}, u32[]{:S(2)}) collective-permute-start(bf16[32,1024]{1,0:T(8,128)(2,1)S(1)} %get-tuple-element.41), channel_id=1, source_target_pairs={{0,2},{1,3},{2,0},{3,1},{4,6},{5,7},{6,4},{7,5},{8,10},{9,11},{10,... | collective-permute-start | bytes 196616 | tf_op jit(solution)/shard_map/ppermute | solution.py:212
Sparse Core Ops, SparseCore 0:
  23.1 75.1 all-gather.1

commit v4 on v3

--- a/solution.py
+++ b/solution.py
@@ -137,21 +137,31 @@
 
 def halves_body(parity_ref, gate_ref, up_ref, down_ref, keep_ref, give_ref):
     hidden = gate_ref.shape[1]
-    width = keep_ref.shape[1] // 3
-
-    def write(out_ref, start):
-        for k, ref in enumerate((gate_ref, up_ref, down_ref)):
-            out_ref[:, k * width : (k + 1) * width] = ref[:, start : start + width]
+    full = hidden // HEAD // 2 * HEAD
+    shared = slice(full, full + HEAD)
+    gate = gate_ref[:, shared].astype(F32)
+    up = pltpu.roll(up_ref[:, shared].astype(F32), HEAD // 2, 1)
+    lane = lax.broadcasted_iota(jnp.int32, gate.shape, 1)
+
+    def write(out_ref, second):
+        start = hidden - full if second else 0
+        for k, ref in enumerate((gate_ref, up_ref)):
+            out_ref[:, k * full : (k + 1) * full] = ref[:, start : start + full]
+        at = 2 * full + HEAD
+        joint = jnp.where(lane < HEAD // 2, up, gate) if second else jnp.where(lane < HEAD // 2, gate, up)
+        out_ref[:, 2 * full : at] = joint.astype(BF16)
+        out_ref[:, at : at + full] = down_ref[:, start : start + full]
+        out_ref[:, at + full :] = down_ref[:, shared]
 
     @pl.when(parity_ref[0] == 0)
     def _():
-        write(keep_ref, 0)
-        write(give_ref, hidden - width)
+        write(keep_ref, False)
+        write(give_ref, True)
 
     @pl.when(parity_ref[0] != 0)
     def _():
-        write(keep_ref, hidden - width)
-        write(give_ref, 0)
+        write(keep_ref, True)
+        write(give_ref, False)
 
 
 def in_order_body(at_ref, whole_ref, weights_ref, sems):
@@ -176,9 +186,9 @@
 def mixer_body(at_ref, *refs, hidden):
     (own_ref, near_ref), x_refs, weights_ref, outs = refs[:2], refs[2:6], refs[6], refs[7:13]
     tokens_ref = refs[13]
-    model, wide = weights_ref.shape
+    model, _ = weights_ref.shape
     y = at_ref[0]
-    width = wide // 3
+    full = hidden // HEAD // 2 * HEAD
     split = model // 2
     rows = own_ref.shape[0]
     part = rows // len(x_refs)
@@ -187,13 +197,16 @@
     for d, ref in enumerate(x_refs):
         tokens_ref[d * part : (d + 1) * part, split:] = ref[:part]
         tokens_ref[rows + d * part : rows + (d + 1) * part, split:] = ref[part:]
-    act = jnp.dot(tokens_ref[...], weights_ref[:, : 2 * width], preferred_element_type=F32)
-    gate, up = act[:, :width], act[:, width:]
+    at = 2 * full + HEAD
+    act = jnp.dot(tokens_ref[...], weights_ref[:, :at], preferred_element_type=F32)
+    gate, up, joint = act[:, :full], act[:, full : 2 * full], act[:, 2 * full :]
     inner = gate * jax.nn.sigmoid(gate) * up
-    lane = lax.broadcasted_iota(jnp.int32, inner.shape, 1)
-    low = jnp.where(lax.rem(y, 2) == 0, 0, width - hidden // 2)
-    inner = jnp.where((lane >= low) & (lane < low + hidden // 2), inner, 0.0).astype(BF16)
-    lowered = nt_dot(inner, weights_ref[:, 2 * width :])
+    shared = joint * jax.nn.sigmoid(joint) * pltpu.roll(joint, HEAD // 2, 1)
+    lane = lax.broadcasted_iota(jnp.int32, shared.shape, 1)
+    low = jnp.where(lax.rem(y, 2) == 0, 0, HEAD // 2)
+    shared = jnp.where((lane >= low) & (lane < low + HEAD // 2), shared, 0.0)
+    inner = jnp.concatenate([inner.astype(BF16), shared.astype(BF16)], axis=1)
+    lowered = nt_dot(inner, weights_ref[:, at:])
     for d, out_ref in enumerate(outs[:4]):
         at = slice(d * part, (d + 1) * part)
         out_ref[:part] = lowered[:rows][at, :split].astype(out_ref.dtype)
@@ -240,15 +253,15 @@
     z_size, y_size, cores = (lax.axis_size(axis) for axis in SP)
     y_at = lax.axis_index("sp_1")
     slab = mixer_gate_weight.shape[0]
-    half = (hidden // 2 + HEAD - 1) // HEAD * HEAD
+    wide = hidden // HEAD // 2 * HEAD * 3 + 2 * HEAD
     send, near, reach, keep, give = pl.pallas_call(
         local_body,
         out_shape=(
             jax.ShapeDtypeStruct((blocks, chunk + 8, HEAD), BF16),
             jax.ShapeDtypeStruct((rows, width), F32),
             jax.ShapeDtypeStruct((2, rows, width), BF16),
-            jax.ShapeDtypeStruct((slab, 3 * half), BF16),
-            jax.ShapeDtypeStruct((slab, 3 * half), BF16),
+            jax.ShapeDtypeStruct((slab, wide), BF16),
+            jax.ShapeDtypeStruct((slab, wide), BF16),
         ),
         in_specs=[SMEM] + [VMEM] * 8,
         out_specs=(VMEM,) * 5,
@@ -267,7 +280,7 @@
     got = lax.all_to_all(send, SP, 0, 0, tiled=True)
     line = [keep] + [shift(give if d % 2 else keep, "sp_1", d) for d in range(1, y_size)]
     line = jnp.concatenate(line, axis=0)
-    whole = lax.all_gather(line, ("sp_0", "sp_2"), axis=0, tiled=True).reshape(z_size, cores, y_size, slab, 3 * half)
+    whole = lax.all_gather(line, ("sp_0", "sp_2"), axis=0, tiled=True).reshape(z_size, cores, y_size, slab, wide)
     give = pl.pallas_call(
         scan_body,
         out_shape=jax.ShapeDtypeStruct((blocks, chunk, HEAD), BF16),
@@ -309,14 +322,14 @@
     tokens = [own, lax.ppermute(own, "sp_1", swap)] + lines
     weights = pl.pallas_call(
         in_order_body,
-        out_shape=jax.ShapeDtypeStruct((z_size, y_size, cores, slab, 3 * half), BF16),
+        out_shape=jax.ShapeDtypeStruct((z_size, y_size, cores, slab, wide), BF16),
         in_specs=[SMEM, ANY],
         out_specs=VMEM,
         scratch_shapes=[pltpu.SemaphoreType.DMA((y_size * cores,))],
         compiler_params=pltpu.CompilerParams(vmem_limit_bytes=40 * 1024 * 1024),
         name="weights_in_order",
     )(y_at[None], whole)
-    weights = weights.reshape(model, 3 * half)
+    weights = weights.reshape(model, wide)
     lowered = pl.pallas_call(
         lambda *refs: mixer_body(*refs, hidden=hidden),
         out_shape=(jax.ShapeDtypeStruct((2 * part, split), F32),)

time: 139 us -> 139 us (level)
  no operation moved by 1% of the time
where the time goes in v4:
time: 139 us
  waiting for transfers between devices  56.9 us (41%)
  starting transfers between devices  49 us (35%)
  Pallas kernels  14.4 us (10%)
  between operations  13.5 us (10%)
  other arithmetic  3.94 us (3%)
    ppermute x18, starting transfers between devices, shift(): lax.ppermute(array, axis, [(k, (k + by) % size) for k in range(size)])  25.9 us
    ppermute x18, waiting for transfers between devices, shift(): lax.ppermute(array, axis, [(k, (k + by) % size) for k in range(size)])  22.8 us
    all_to_all x1, waiting for transfers between devices, local(): got = lax.all_to_all(send, SP, 0, 0, tiled=True)  18.1 us
    all_to_all x1, waiting for transfers between devices, local(): lax.all_to_all(give, SP, 0, 0, tiled=True).reshape(2 * heads, HEAD, HEAD)  15.2 us
    all_to_all x1, starting transfers between devices, local(): got = lax.all_to_all(send, SP, 0, 0, tiled=True)  11.5 us
    all_to_all x1, starting transfers between devices, local(): lax.all_to_all(give, SP, 0, 0, tiled=True).reshape(2 * heads, HEAD, HEAD)  5.66 us
    pallas_call x1, Pallas kernels, local(): pl.pallas_call(local_body, out_shape=(jax.ShapeDtypeStruct((blocks, chunk...  3.63 us
    pallas_call x1, Pallas kernels, local(): pl.pallas_call(project_body, out_shape=(jax.ShapeDtypeStruct((part, model...  3.63 us
  transfers between devices with their start and end apart: 25, of which 19 were waited for; matrix products, arithmetic and copies ran while one was open for 1% of the time, Pallas kernels for 6%

profile of v4, /device:TPU:6, one launch (start us, length us, event | category | flops | bytes accessed | tf_op | source)
XLA Modules:
  0.0 138.5 jit_solution(16747914466433373008)
XLA Ops:
  6.5 0.0 all-gather.2.cloned.1.call-start
  6.5 3.6 %local_sweep.1 = (bf16[64,24,128]{2,1,0:T(8,128)(2,1)}, f32[128,512]{1,0:T(8,128)}, bf16[2,128,512]{2,1,0:T(8,128)(2,1)}, bf16[32,2176]{1,0:T(8,128)(2,1)}, bf16[32,2176]{1,0:T(8,128)(2,1)}) custom-call(s32[1]{0:T(128)} %bitcast.1.parity_ref, bf16[128,512]{1,0:T(8,128)(2,1)} %q_ref.1, bf16[2,128,512]{2,1,0:T(8,128)(2,1)} %f_ref.1, bf16[128,512]{1,0:T(8,128)(2,1)} %v_ref.1, ...), custom_call_target="tpu_custom_call" | custom-call | tf_op jit(solution)/shard_map/local_sweep/pallas_call | solution.py:257
  10.2 3.2 %collective-permute-start.12 = (bf16[32,2176]{1,0:T(8,128)(2,1)}, bf16[32,2176]{1,0:T(8,128)(2,1)S(1)}, u32[]{:S(2)}, u32[]{:S(2)}) collective-permute-start(bf16[32,2176]{1,0:T(8,128)(2,1)} %get-tuple-element.27), channel_id=1, source_target_pairs={{0,16},{8,24},{16,0},{24,8},{1,17},{9,25},{17,1},{25,9},{2,18},{10... | collective-permute-start | bytes 417800 | tf_op jit(solution)/shard_map/ppermute | solution.py:225
  13.4 1.1 collective-permute-start.13
  14.4 1.0 collective-permute-start.11
  15.4 2.7 %collective-permute-done.12 = bf16[32,2176]{1,0:T(8,128)(2,1)S(1)} collective-permute-done((bf16[32,2176]{1,0:T(8,128)(2,1)}, bf16[32,2176]{1,0:T(8,128)(2,1)S(1)}, u32[]{:S(2)}, u32[]{:S(2)}) %collective-permute-start.12) | collective-permute-done | bytes 139296 | tf_op jit(solution)/shard_map/ppermute | solution.py:225
  18.1 2.5 %collective-permute-done.13 = bf16[32,2176]{1,0:T(8,128)(2,1)S(1)} collective-permute-done((bf16[32,2176]{1,0:T(8,128)(2,1)}, bf16[32,2176]{1,0:T(8,128)(2,1)S(1)}, u32[]{:S(2)}, u32[]{:S(2)}) %collective-permute-start.13) | collective-permute-done | bytes 139296 | tf_op jit(solution)/shard_map/ppermute | solution.py:225
  20.6 0.3 collective-permute-done.11
  20.9 1.8 %pad_maximum_fusion = bf16[128,2176]{1,0:T(8,128)(2,1)} fusion(bf16[32,2176]{1,0:T(8,128)(2,1)S(1)} %collective-permute-done.13, bf16[32,2176]{1,0:T(8,128)(2,1)S(1)} %collective-permute-done.12, bf16[32,2176]{1,0:T(8,128)(2,1)S(1)} %collective-permute-done.11, bf16[32,2176]{1,0:T(8,128)(2,1)} %get-tuple-element.27), kind=kLoop, calls=%fused_computation | loop fusion | flops 2228224 | bytes 1114112 | tf_op jit(solution)/shard_map/concatenate | solution.py:282
  22.7 0.0 all-gather.2.cloned.1.call-update
  22.7 11.5 %all-to-all-start = ((bf16[64,24,128]{2,1,0:T(8,128)(2,1)}), bf16[64,24,128]{2,1,0:T(8,128)(2,1)S(1)}, u32[]{:S(2)}, u32[]{:S(2)}) async-start(bf16[64,24,128]{2,1,0:T(8,128)(2,1)} %get-tuple-element.22), calls=%async_computation | async-start | bytes 786432 | tf_op jit(solution)/shard_map/all_to_all | solution.py:280
  34.2 18.1 %all-to-all-done.got_ref = bf16[64,24,128]{2,1,0:T(8,128)(2,1)S(1)} async-done(((bf16[64,24,128]{2,1,0:T(8,128)(2,1)}), bf16[64,24,128]{2,1,0:T(8,128)(2,1)S(1)}, u32[]{:S(2)}, u32[]{:S(2)}) %all-to-all-start) | async-done | bytes 393248 | tf_op jit(solution)/shard_map/all_to_all | solution.py:280
  52.3 0.8 block_scan.1
  53.2 5.7 %all-to-all-start.1 = ((bf16[64,16,128]{2,1,0:T(8,128)(2,1)}), bf16[64,16,128]{2,1,0:T(8,128)(2,1)S(1)}, u32[]{:S(2)}, u32[]{:S(2)}) async-start(bf16[64,16,128]{2,1,0:T(8,128)(2,1)} %block_scan.1), calls=%async_computation.1 | async-start | bytes 524288 | tf_op jit(solution)/shard_map/all_to_all | solution.py:292
  58.9 15.2 %all-to-all-done.1 = bf16[64,16,128]{2,1,0:T(8,128)(2,1)S(1)} async-done(((bf16[64,16,128]{2,1,0:T(8,128)(2,1)}), bf16[64,16,128]{2,1,0:T(8,128)(2,1)S(1)}, u32[]{:S(2)}, u32[]{:S(2)}) %all-to-all-start.1) | async-done | bytes 262176 | tf_op jit(solution)/shard_map/all_to_all | solution.py:292
  74.0 0.7 copy-done
  74.7 3.6 %norm_project.1 = (bf16[32,2048]{1,0:T(8,128)(2,1)}, bf16[32,2048]{1,0:T(8,128)(2,1)}, bf16[32,2048]{1,0:T(8,128)(2,1)}, bf16[32,2048]{1,0:T(8,128)(2,1)}) custom-call(s32[1]{0:T(128)} %bitcast.own_ref, f32[128,512]{1,0:T(8,128)} %get-tuple-element.20.near_ref, bf16[2,128,512]{2,1,0:T(8,128)(2,1)} %get-tuple-element.21.reach_ref, ...), custom_call_target="tpu_custom_call" | custom-call | tf_op jit(solution)/shard_map/norm_project/pallas_call | solution.py:295
  78.4 0.5 collective-permute-start
  78.8 2.4 %collective-permute-start.1 = (bf16[32,2048]{1,0:T(8,128)(2,1)}, bf16[32,2048]{1,0:T(8,128)(2,1)S(1)}, u32[]{:S(2)}, u32[]{:S(2)}) collective-permute-start(bf16[32,2048]{1,0:T(8,128)(2,1)} %get-tuple-element.25), channel_id=1, source_target_pairs={{0,2},{1,3},{2,0},{3,1},{4,6},{5,7},{6,4},{7,5},{8,10},{9,11},{10,... | collective-permute-start | bytes 393224 | tf_op jit(solution)/shard_map/ppermute | solution.py:225
  81.3 0.0 collective-permute-start.2
  81.3 0.0 copy-done.1
  81.3 3.7 %collective-permute-done = bf16[32,2048]{1,0:T(8,128)(2,1)S(1)} collective-permute-done((bf16[32,2048]{1,0:T(8,128)(2,1)}, bf16[32,2048]{1,0:T(8,128)(2,1)S(1)}, u32[]{:S(2)}, u32[]{:S(2)}) %collective-permute-start) | collective-permute-done | bytes 131104 | tf_op jit(solution)/shard_map/ppermute | solution.py:225
  84.9 1.9 %collective-permute-done.1 = bf16[32,2048]{1,0:T(8,128)(2,1)S(1)} collective-permute-done((bf16[32,2048]{1,0:T(8,128)(2,1)}, bf16[32,2048]{1,0:T(8,128)(2,1)S(1)}, u32[]{:S(2)}, u32[]{:S(2)}) %collective-permute-start.1) | collective-permute-done | bytes 131104 | tf_op jit(solution)/shard_map/ppermute | solution.py:225
  86.9 1.9 %collective-permute-done.2 = bf16[32,2048]{1,0:T(8,128)(2,1)S(1)} collective-permute-done((bf16[32,2048]{1,0:T(8,128)(2,1)}, bf16[32,2048]{1,0:T(8,128)(2,1)S(1)}, u32[]{:S(2)}, u32[]{:S(2)}) %collective-permute-start.2) | collective-permute-done | bytes 131104 | tf_op jit(solution)/shard_map/ppermute | solution.py:225
  88.7 1.2 fusion
  89.9 0.1 fusion.2
  90.1 1.1 collective-permute-start.5
  91.1 1.5 %collective-permute-start.4 = (bf16[32,1024]{1,0:T(8,128)(2,1)S(1)}, bf16[32,1024]{1,0:T(8,128)(2,1)S(1)}, u32[]{:S(2)}, u32[]{:S(2)}) collective-permute-start(bf16[32,1024]{1,0:T(8,128)(2,1)S(1)} %get-tuple-element.45), channel_id=1, source_target_pairs={{0,2},{1,3},{2,0},{3,1},{4,6},{5,7},{6,4},{7,5},{8,10},{9,11},{10,... | collective-permute-start | bytes 196616 | tf_op jit(solution)/shard_map/ppermute | solution.py:225
  92.6 1.9 %collective-permute-start.3 = (bf16[32,1024]{1,0:T(8,128)(2,1)S(1)}, bf16[32,1024]{1,0:T(8,128)(2,1)S(1)}, u32[]{:S(2)}, u32[]{:S(2)}) collective-permute-start(bf16[32,1024]{1,0:T(8,128)(2,1)S(1)} %get-tuple-element.45), channel_id=1, source_target_pairs={{0,1},{1,2},{2,3},{3,0},{4,5},{5,6},{6,7},{7,4},{8,9},{9,10},{10,1... | collective-permute-start | bytes 196616 | tf_op jit(solution)/shard_map/ppermute | solution.py:225
  94.5 1.4 %collective-permute-start.7 = (bf16[32,1024]{1,0:T(8,128)(2,1)S(1)}, bf16[32,1024]{1,0:T(8,128)(2,1)S(1)}, u32[]{:S(2)}, u32[]{:S(2)}) collective-permute-start(bf16[32,1024]{1,0:T(8,128)(2,1)S(1)} %get-tuple-element.44), channel_id=1, source_target_pairs={{0,8},{8,0},{16,24},{24,16},{1,9},{9,1},{17,25},{25,17},{2,10},{10... | collective-permute-start | bytes 196616 | tf_op jit(solution)/shard_map/ppermute | solution.py:319
  95.9 0.0 collective-permute-done.5
  96.0 0.9 collective-permute-done.4
  96.9 0.3 collective-permute-done.3
  97.2 1.5 %collective-permute-start.6 = (bf16[128,1024]{1,0:T(8,128)(2,1)S(1)}, bf16[128,1024]{1,0:T(8,128)(2,1)S(1)}, u32[]{:S(2)}, u32[]{:S(2)}) collective-permute-start(bf16[128,1024]{1,0:T(8,128)(2,1)S(1)} %pad_maximum_fusion.1.refs_1_), channel_id=1, source_target_pairs={{0,8},{8,0},{16,24},{24,16},{1,9},{9,1},{17,25},{25,17},{2,10},{10... | collective-permute-start | bytes 786440 | tf_op jit(solution)/shard_map/ppermute | solution.py:322
  98.7 0.5 collective-permute-done.7
  99.2 1.1 collective-permute-start.10
  100.3 3.0 %collective-permute-start.9 = (bf16[64,1024]{1,0:T(8,128)(2,1)S(1)}, bf16[64,1024]{1,0:T(8,128)(2,1)S(1)}, u32[]{:S(2)}, u32[]{:S(2)}) collective-permute-start(bf16[64,1024]{1,0:T(8,128)(2,1)S(1)} %pad_maximum_fusion.2.refs_3_), channel_id=1, source_target_pairs={{0,2},{1,3},{2,0},{3,1},{4,6},{5,7},{6,4},{7,5},{8,10},{9,11},{10,... | collective-permute-start | bytes 393224 | tf_op jit(solution)/shard_map/ppermute | solution.py:225
  103.3 0.9 collective-permute-start.8
  104.2 3.6 %weights_in_order.1 = bf16[8,4,2,32,2176]{4,3,2,1,0:T(8,128)(2,1)S(1)} custom-call(s32[1]{0:T(128)} %bitcast.8.at_ref.refs_0_, bf16[8,2,4,32,2176]{4,3,2,1,0:T(8,128)(2,1)} %bitcast.12), custom_call_target="tpu_custom_call" | custom-call | tf_op jit(solution)/shard_map/weights_in_order/pallas_call | solution.py:323
  107.8 0.0 collective-permute-done.10.refs_6_
  107.8 0.0 collective-permute-done.9.refs_5_
  107.8 0.4 collective-permute-done.8.refs_4_
  108.2 0.0 collective-permute-done.6.refs_2_
  108.2 2.7 %channel_mixer.1 = (f32[64,1024]{1,0:T(8,128)S(1)}, bf16[64,1024]{1,0:T(8,128)(2,1)S(1)}, bf16[64,1024]{1,0:T(8,128)(2,1)S(1)}, bf16[64,1024]{1,0:T(8,128)(2,1)S...) custom-call(s32[1]{0:T(128)} %bitcast.8.at_ref.refs_0_, bf16[128,1024]{1,0:T(8,128)(2,1)S(1)} %pad_maximum_fusion.1.refs_1_, ...), custom_call_target="tpu_custom_call" | custom-call | tf_op jit(solution)/shard_map/channel_mixer/pallas_call | solution.py:333
  110.9 1.2 collective-permute-start.14
  112.2 2.6 %collective-permute-start.15 = (bf16[64,1024]{1,0:T(8,128)(2,1)S(1)}, bf16[64,1024]{1,0:T(8,128)(2,1)S(1)}, u32[]{:S(2)}, u32[]{:S(2)}) collective-permute-start(bf16[64,1024]{1,0:T(8,128)(2,1)S(1)} %get-tuple-element.31), channel_id=1, source_target_pairs={{0,2},{1,3},{2,0},{3,1},{4,6},{5,7},{6,4},{7,5},{8,10},{9,11},{10,... | collective-permute-start | bytes 393224 | tf_op jit(solution)/shard_map/ppermute | solution.py:225
  114.8 0.6 collective-permute-start.16
  115.4 1.4 %collective-permute-start.18 = (bf16[128,1024]{1,0:T(8,128)(2,1)S(1)}, bf16[128,1024]{1,0:T(8,128)(2,1)S(1)}, u32[]{:S(2)}, u32[]{:S(2)}) collective-permute-start(bf16[128,1024]{1,0:T(8,128)(2,1)S(1)} %get-tuple-element.34), channel_id=1, source_target_pairs={{0,8},{8,0},{16,24},{24,16},{1,9},{9,1},{17,25},{25,17},{2,10},{10... | collective-permute-start | bytes 786440 | tf_op jit(solution)/shard_map/ppermute | solution.py:344
  116.8 0.4 collective-permute-done.14
  117.2 2.0 %collective-permute-done.15 = bf16[64,1024]{1,0:T(8,128)(2,1)S(1)} collective-permute-done((bf16[64,1024]{1,0:T(8,128)(2,1)S(1)}, bf16[64,1024]{1,0:T(8,128)(2,1)S(1)}, u32[]{:S(2)}, u32[]{:S(2)}) %collective-permute-start.15) | collective-permute-done | bytes 131104 | tf_op jit(solution)/shard_map/ppermute | solution.py:225
  119.1 0.6 collective-permute-done.16
  119.8 0.1 convert_add_fusion.1
  119.8 1.6 %collective-permute-start.17 = (bf16[32,1024]{1,0:T(8,128)(2,1)S(1)}, bf16[32,1024]{1,0:T(8,128)(2,1)S(1)}, u32[]{:S(2)}, u32[]{:S(2)}) collective-permute-start(bf16[32,1024]{1,0:T(8,128)(2,1)S(1)} %slice.71), channel_id=1, source_target_pairs={{0,8},{8,0},{16,24},{24,16},{1,9},{9,1},{17,25},{25,17},{2,10},{10... | collective-permute-start | bytes 196616 | tf_op jit(solution)/shard_map/ppermute | solution.py:353
  121.4 0.3 collective-permute-done.18
  121.8 0.1 fusion.9
  121.9 1.5 %collective-permute-start.19 = (bf16[32,1024]{1,0:T(8,128)(2,1)S(1)}, bf16[32,1024]{1,0:T(8,128)(2,1)S(1)}, u32[]{:S(2)}, u32[]{:S(2)}) collective-permute-start(bf16[32,1024]{1,0:T(8,128)(2,1)S(1)} %get-tuple-element.39), channel_id=1, source_target_pairs={{0,3},{1,0},{2,1},{3,2},{4,7},{5,4},{6,5},{7,6},{8,11},{9,8},{10,9... | collective-permute-start | bytes 196616 | tf_op jit(solution)/shard_map/ppermute | solution.py:225
  123.4 1.8 %collective-permute-start.21 = (bf16[32,1024]{1,0:T(8,128)(2,1)S(1)}, bf16[32,1024]{1,0:T(8,128)(2,1)S(1)}, u32[]{:S(2)}, u32[]{:S(2)}) collective-permute-start(bf16[32,1024]{1,0:T(8,128)(2,1)S(1)} %get-tuple-element.40), channel_id=1, source_target_pairs={{0,1},{1,2},{2,3},{3,0},{4,5},{5,6},{6,7},{7,4},{8,9},{9,10},{10,1... | collective-permute-start | bytes 196616 | tf_op jit(solution)/shard_map/ppermute | solution.py:225
  125.2 0.6 collective-permute-start.20
  125.7 0.0 collective-permute-done.17
  125.7 1.7 %collective-permute-done.19 = bf16[32,1024]{1,0:T(8,128)(2,1)S(1)} collective-permute-done((bf16[32,1024]{1,0:T(8,128)(2,1)S(1)}, bf16[32,1024]{1,0:T(8,128)(2,1)S(1)}, u32[]{:S(2)}, u32[]{:S(2)}) %collective-permute-start.19) | collective-permute-done | bytes 65568 | tf_op jit(solution)/shard_map/ppermute | solution.py:225
  127.4 0.2 collective-permute-done.21
  127.6 3.3 %collective-permute-done.20 = bf16[32,1024]{1,0:T(8,128)(2,1)S(1)} collective-permute-done((bf16[32,1024]{1,0:T(8,128)(2,1)S(1)}, bf16[32,1024]{1,0:T(8,128)(2,1)S(1)}, u32[]{:S(2)}, u32[]{:S(2)}) %collective-permute-start.20) | collective-permute-done | bytes 65568 | tf_op jit(solution)/shard_map/ppermute | solution.py:225
  130.9 0.1 fusion.8
  131.0 0.7 pad_maximum_fusion.3
  (10 shorter events, 0.1 us)
Async XLA Ops:
  6.5 97.6 %all-gather.2.cloned.1.call-start = ((), (), s32[]{:S(2)}) async-start(), calls=%async_computation.2 | async-start | bytes 9469952 | tf_op jit(solution)/shard_map/all_gather | solution.py:283
  10.2 7.9 %collective-permute-start.12 = (bf16[32,2176]{1,0:T(8,128)(2,1)}, bf16[32,2176]{1,0:T(8,128)(2,1)S(1)}, u32[]{:S(2)}, u32[]{:S(2)}) collective-permute-start(bf16[32,2176]{1,0:T(8,128)(2,1)} %get-tuple-element.27), channel_id=1, source_target_pairs={{0,16},{8,24},{16,0},{24,8},{1,17},{9,25},{17,1},{25,9},{2,18},{10... | collective-permute-start | bytes 417800 | tf_op jit(solution)/shard_map/ppermute | solution.py:225
  13.4 7.3 %collective-permute-start.13 = (bf16[32,2176]{1,0:T(8,128)(2,1)}, bf16[32,2176]{1,0:T(8,128)(2,1)S(1)}, u32[]{:S(2)}, u32[]{:S(2)}) collective-permute-start(bf16[32,2176]{1,0:T(8,128)(2,1)} %get-tuple-element.28), channel_id=1, source_target_pairs={{0,24},{8,0},{16,8},{24,16},{1,25},{9,1},{17,9},{25,17},{2,26},{10... | collective-permute-start | bytes 417800 | tf_op jit(solution)/shard_map/ppermute | solution.py:225
  14.4 6.5 %collective-permute-start.11 = (bf16[32,2176]{1,0:T(8,128)(2,1)}, bf16[32,2176]{1,0:T(8,128)(2,1)S(1)}, u32[]{:S(2)}, u32[]{:S(2)}) collective-permute-start(bf16[32,2176]{1,0:T(8,128)(2,1)} %get-tuple-element.28), channel_id=1, source_target_pairs={{0,8},{8,16},{16,24},{24,0},{1,9},{9,17},{17,25},{25,1},{2,10},{10... | collective-permute-start | bytes 417800 | tf_op jit(solution)/shard_map/ppermute | solution.py:225
  22.7 29.7 %all-to-all-start = ((bf16[64,24,128]{2,1,0:T(8,128)(2,1)}), bf16[64,24,128]{2,1,0:T(8,128)(2,1)S(1)}, u32[]{:S(2)}, u32[]{:S(2)}) async-start(bf16[64,24,128]{2,1,0:T(8,128)(2,1)} %get-tuple-element.22), calls=%async_computation | async-start | bytes 786432 | tf_op jit(solution)/shard_map/all_to_all | solution.py:280
  53.2 20.9 %all-to-all-start.1 = ((bf16[64,16,128]{2,1,0:T(8,128)(2,1)}), bf16[64,16,128]{2,1,0:T(8,128)(2,1)S(1)}, u32[]{:S(2)}, u32[]{:S(2)}) async-start(bf16[64,16,128]{2,1,0:T(8,128)(2,1)} %block_scan.1), calls=%async_computation.1 | async-start | bytes 524288 | tf_op jit(solution)/shard_map/all_to_all | solution.py:292
  74.0 0.7 copy-start
  74.7 6.5 %copy-start.1 = (bf16[2048]{0:T(1024)(128)(2,1)S(1)}, bf16[2048]{0:T(1024)(128)(2,1)}, u32[]{:S(2)}) copy-start(bf16[2048]{0:T(1024)(128)(2,1)} %param.22) | copy-start | bytes 12292
  78.4 6.6 %collective-permute-start = (bf16[32,2048]{1,0:T(8,128)(2,1)}, bf16[32,2048]{1,0:T(8,128)(2,1)S(1)}, u32[]{:S(2)}, u32[]{:S(2)}) collective-permute-start(bf16[32,2048]{1,0:T(8,128)(2,1)} %get-tuple-element.24), channel_id=1, source_target_pairs={{0,1},{1,2},{2,3},{3,0},{4,5},{5,6},{6,7},{7,4},{8,9},{9,10},{10,1... | collective-permute-start | bytes 393224 | tf_op jit(solution)/shard_map/ppermute | solution.py:225
  78.8 8.0 %collective-permute-start.1 = (bf16[32,2048]{1,0:T(8,128)(2,1)}, bf16[32,2048]{1,0:T(8,128)(2,1)S(1)}, u32[]{:S(2)}, u32[]{:S(2)}) collective-permute-start(bf16[32,2048]{1,0:T(8,128)(2,1)} %get-tuple-element.25), channel_id=1, source_target_pairs={{0,2},{1,3},{2,0},{3,1},{4,6},{5,7},{6,4},{7,5},{8,10},{9,11},{10,... | collective-permute-start | bytes 393224 | tf_op jit(solution)/shard_map/ppermute | solution.py:225
  81.3 7.5 %collective-permute-start.2 = (bf16[32,2048]{1,0:T(8,128)(2,1)}, bf16[32,2048]{1,0:T(8,128)(2,1)S(1)}, u32[]{:S(2)}, u32[]{:S(2)}) collective-permute-start(bf16[32,2048]{1,0:T(8,128)(2,1)} %get-tuple-element.26), channel_id=1, source_target_pairs={{0,3},{1,0},{2,1},{3,2},{4,7},{5,4},{6,5},{7,6},{8,11},{9,8},{10,9... | collective-permute-start | bytes 393224 | tf_op jit(solution)/shard_map/ppermute | solution.py:225
  90.1 5.9 %collective-permute-start.5 = (bf16[32,1024]{1,0:T(8,128)(2,1)S(1)}, bf16[32,1024]{1,0:T(8,128)(2,1)S(1)}, u32[]{:S(2)}, u32[]{:S(2)}) collective-permute-start(bf16[32,1024]{1,0:T(8,128)(2,1)S(1)} %get-tuple-element.45), channel_id=1, source_target_pairs={{0,3},{1,0},{2,1},{3,2},{4,7},{5,4},{6,5},{7,6},{8,11},{9,8},{10,9... | collective-permute-start | bytes 196616 | tf_op jit(solution)/shard_map/ppermute | solution.py:225
  91.1 5.8 %collective-permute-start.4 = (bf16[32,1024]{1,0:T(8,128)(2,1)S(1)}, bf16[32,1024]{1,0:T(8,128)(2,1)S(1)}, u32[]{:S(2)}, u32[]{:S(2)}) collective-permute-start(bf16[32,1024]{1,0:T(8,128)(2,1)S(1)} %get-tuple-element.45), channel_id=1, source_target_pairs={{0,2},{1,3},{2,0},{3,1},{4,6},{5,7},{6,4},{7,5},{8,10},{9,11},{10,... | collective-permute-start | bytes 196616 | tf_op jit(solution)/shard_map/ppermute | solution.py:225
  92.6 4.6 %collective-permute-start.3 = (bf16[32,1024]{1,0:T(8,128)(2,1)S(1)}, bf16[32,1024]{1,0:T(8,128)(2,1)S(1)}, u32[]{:S(2)}, u32[]{:S(2)}) collective-permute-start(bf16[32,1024]{1,0:T(8,128)(2,1)S(1)} %get-tuple-element.45), channel_id=1, source_target_pairs={{0,1},{1,2},{2,3},{3,0},{4,5},{5,6},{6,7},{7,4},{8,9},{9,10},{10,1... | collective-permute-start | bytes 196616 | tf_op jit(solution)/shard_map/ppermute | solution.py:225
  94.5 4.7 %collective-permute-start.7 = (bf16[32,1024]{1,0:T(8,128)(2,1)S(1)}, bf16[32,1024]{1,0:T(8,128)(2,1)S(1)}, u32[]{:S(2)}, u32[]{:S(2)}) collective-permute-start(bf16[32,1024]{1,0:T(8,128)(2,1)S(1)} %get-tuple-element.44), channel_id=1, source_target_pairs={{0,8},{8,0},{16,24},{24,16},{1,9},{9,1},{17,25},{25,17},{2,10},{10... | collective-permute-start | bytes 196616 | tf_op jit(solution)/shard_map/ppermute | solution.py:319
  97.2 11.0 %collective-permute-start.6 = (bf16[128,1024]{1,0:T(8,128)(2,1)S(1)}, bf16[128,1024]{1,0:T(8,128)(2,1)S(1)}, u32[]{:S(2)}, u32[]{:S(2)}) collective-permute-start(bf16[128,1024]{1,0:T(8,128)(2,1)S(1)} %pad_maximum_fusion.1.refs_1_), channel_id=1, source_target_pairs={{0,8},{8,0},{16,24},{24,16},{1,9},{9,1},{17,25},{25,17},{2,10},{10... | collective-permute-start | bytes 786440 | tf_op jit(solution)/shard_map/ppermute | solution.py:322
  99.2 8.6 %collective-permute-start.10 = (bf16[64,1024]{1,0:T(8,128)(2,1)S(1)}, bf16[64,1024]{1,0:T(8,128)(2,1)S(1)}, u32[]{:S(2)}, u32[]{:S(2)}) collective-permute-start(bf16[64,1024]{1,0:T(8,128)(2,1)S(1)} %pad_maximum_fusion.2.refs_3_), channel_id=1, source_target_pairs={{0,3},{1,0},{2,1},{3,2},{4,7},{5,4},{6,5},{7,6},{8,11},{9,8},{10,9... | collective-permute-start | bytes 393224 | tf_op jit(solution)/shard_map/ppermute | solution.py:225
  100.3 7.5 %collective-permute-start.9 = (bf16[64,1024]{1,0:T(8,128)(2,1)S(1)}, bf16[64,1024]{1,0:T(8,128)(2,1)S(1)}, u32[]{:S(2)}, u32[]{:S(2)}) collective-permute-start(bf16[64,1024]{1,0:T(8,128)(2,1)S(1)} %pad_maximum_fusion.2.refs_3_), channel_id=1, source_target_pairs={{0,2},{1,3},{2,0},{3,1},{4,6},{5,7},{6,4},{7,5},{8,10},{9,11},{10,... | collective-permute-start | bytes 393224 | tf_op jit(solution)/shard_map/ppermute | solution.py:225
  103.3 5.0 %collective-permute-start.8 = (bf16[64,1024]{1,0:T(8,128)(2,1)S(1)}, bf16[64,1024]{1,0:T(8,128)(2,1)S(1)}, u32[]{:S(2)}, u32[]{:S(2)}) collective-permute-start(bf16[64,1024]{1,0:T(8,128)(2,1)S(1)} %pad_maximum_fusion.2.refs_3_), channel_id=1, source_target_pairs={{0,1},{1,2},{2,3},{3,0},{4,5},{5,6},{6,7},{7,4},{8,9},{9,10},{10,1... | collective-permute-start | bytes 393224 | tf_op jit(solution)/shard_map/ppermute | solution.py:225
  110.9 6.3 %collective-permute-start.14 = (bf16[64,1024]{1,0:T(8,128)(2,1)S(1)}, bf16[64,1024]{1,0:T(8,128)(2,1)S(1)}, u32[]{:S(2)}, u32[]{:S(2)}) collective-permute-start(bf16[64,1024]{1,0:T(8,128)(2,1)S(1)} %get-tuple-element.30), channel_id=1, source_target_pairs={{0,3},{1,0},{2,1},{3,2},{4,7},{5,4},{6,5},{7,6},{8,11},{9,8},{10,9... | collective-permute-start | bytes 393224 | tf_op jit(solution)/shard_map/ppermute | solution.py:225
  112.2 7.0 %collective-permute-start.15 = (bf16[64,1024]{1,0:T(8,128)(2,1)S(1)}, bf16[64,1024]{1,0:T(8,128)(2,1)S(1)}, u32[]{:S(2)}, u32[]{:S(2)}) collective-permute-start(bf16[64,1024]{1,0:T(8,128)(2,1)S(1)} %get-tuple-element.31), channel_id=1, source_target_pairs={{0,2},{1,3},{2,0},{3,1},{4,6},{5,7},{6,4},{7,5},{8,10},{9,11},{10,... | collective-permute-start | bytes 393224 | tf_op jit(solution)/shard_map/ppermute | solution.py:225
  114.8 5.0 %collective-permute-start.16 = (bf16[64,1024]{1,0:T(8,128)(2,1)S(1)}, bf16[64,1024]{1,0:T(8,128)(2,1)S(1)}, u32[]{:S(2)}, u32[]{:S(2)}) collective-permute-start(bf16[64,1024]{1,0:T(8,128)(2,1)S(1)} %get-tuple-element.32), channel_id=1, source_target_pairs={{0,1},{1,2},{2,3},{3,0},{4,5},{5,6},{6,7},{7,4},{8,9},{9,10},{10,1... | collective-permute-start | bytes 393224 | tf_op jit(solution)/shard_map/ppermute | solution.py:225
  115.4 6.4 %collective-permute-start.18 = (bf16[128,1024]{1,0:T(8,128)(2,1)S(1)}, bf16[128,1024]{1,0:T(8,128)(2,1)S(1)}, u32[]{:S(2)}, u32[]{:S(2)}) collective-permute-start(bf16[128,1024]{1,0:T(8,128)(2,1)S(1)} %get-tuple-element.34), channel_id=1, source_target_pairs={{0,8},{8,0},{16,24},{24,16},{1,9},{9,1},{17,25},{25,17},{2,10},{10... | collective-permute-start | bytes 786440 | tf_op jit(solution)/shard_map/ppermute | solution.py:344
  119.8 5.9 %collective-permute-start.17 = (bf16[32,1024]{1,0:T(8,128)(2,1)S(1)}, bf16[32,1024]{1,0:T(8,128)(2,1)S(1)}, u32[]{:S(2)}, u32[]{:S(2)}) collective-permute-start(bf16[32,1024]{1,0:T(8,128)(2,1)S(1)} %slice.71), channel_id=1, source_target_pairs={{0,8},{8,0},{16,24},{24,16},{1,9},{9,1},{17,25},{25,17},{2,10},{10... | collective-permute-start | bytes 196616 | tf_op jit(solution)/shard_map/ppermute | solution.py:353
  121.9 5.6 %collective-permute-start.19 = (bf16[32,1024]{1,0:T(8,128)(2,1)S(1)}, bf16[32,1024]{1,0:T(8,128)(2,1)S(1)}, u32[]{:S(2)}, u32[]{:S(2)}) collective-permute-start(bf16[32,1024]{1,0:T(8,128)(2,1)S(1)} %get-tuple-element.39), channel_id=1, source_target_pairs={{0,3},{1,0},{2,1},{3,2},{4,7},{5,4},{6,5},{7,6},{8,11},{9,8},{10,9... | collective-permute-start | bytes 196616 | tf_op jit(solution)/shard_map/ppermute | solution.py:225
  123.4 4.3 %collective-permute-start.21 = (bf16[32,1024]{1,0:T(8,128)(2,1)S(1)}, bf16[32,1024]{1,0:T(8,128)(2,1)S(1)}, u32[]{:S(2)}, u32[]{:S(2)}) collective-permute-start(bf16[32,1024]{1,0:T(8,128)(2,1)S(1)} %get-tuple-element.40), channel_id=1, source_target_pairs={{0,1},{1,2},{2,3},{3,0},{4,5},{5,6},{6,7},{7,4},{8,9},{9,10},{10,1... | collective-permute-start | bytes 196616 | tf_op jit(solution)/shard_map/ppermute | solution.py:225
  125.2 5.8 %collective-permute-start.20 = (bf16[32,1024]{1,0:T(8,128)(2,1)S(1)}, bf16[32,1024]{1,0:T(8,128)(2,1)S(1)}, u32[]{:S(2)}, u32[]{:S(2)}) collective-permute-start(bf16[32,1024]{1,0:T(8,128)(2,1)S(1)} %get-tuple-element.41), channel_id=1, source_target_pairs={{0,2},{1,3},{2,0},{3,1},{4,6},{5,7},{6,4},{7,5},{8,10},{9,11},{10,... | collective-permute-start | bytes 196616 | tf_op jit(solution)/shard_map/ppermute | solution.py:225
Sparse Core Ops, SparseCore 0:
  22.8 72.7 all-gather.1

commit v5 on v4

--- a/solution.py
+++ b/solution.py
@@ -164,19 +164,29 @@
         write(give_ref, False)
 
 
-def in_order_body(at_ref, whole_ref, weights_ref, sems):
-    _, y_size, cores, _, _ = weights_ref.shape
-    y = at_ref[0]
+def in_order_body(at_ref, *refs):
+    pieces, (weights_ref, sems) = refs[:18], refs[18:]
+    z_size, y_size, cores, _, _ = weights_ref.shape
+    y, z, core = at_ref[0], at_ref[1], at_ref[2]
+    ahead = z_size // 2
     copies = []
     for c in range(cores):
-        for k in range(y_size):
-            copies.append(
-                pltpu.make_async_copy(
-                    whole_ref.at[:, c, k],
-                    weights_ref.at[:, lax.rem(y + y_size - k, y_size), c],
-                    sems.at[c * y_size + k],
+        lines = pieces[9 * c : 9 * c + 9]
+        row_core = core if c == 0 else 1 - core
+        for back in range(z_size):
+            at_z = lax.rem(z + z_size - back, z_size)
+            for k in range(y_size):
+                if back == ahead:
+                    source = lines[ahead].at[k] if k < 2 else lines[ahead + 1].at[k - 2]
+                else:
+                    source = lines[back if back < ahead else back + 1].at[k]
+                copies.append(
+                    pltpu.make_async_copy(
+                        source,
+                        weights_ref.at[at_z, lax.rem(y + y_size - k, y_size), row_core],
+                        sems.at[(c * z_size + back) * y_size + k],
+                    )
                 )
-            )
     for copy in copies:
         copy.start()
     for copy in copies:
@@ -280,7 +290,8 @@
     got = lax.all_to_all(send, SP, 0, 0, tiled=True)
     line = [keep] + [shift(give if d % 2 else keep, "sp_1", d) for d in range(1, y_size)]
     line = jnp.concatenate(line, axis=0)
-    whole = lax.all_gather(line, ("sp_0", "sp_2"), axis=0, tiled=True).reshape(z_size, cores, y_size, slab, wide)
+    line = line.reshape(y_size, slab, wide)
+    ups, downs = [shift(line, "sp_0", 1)], [shift(line, "sp_0", z_size - 1)]
     give = pl.pallas_call(
         scan_body,
         out_shape=jax.ShapeDtypeStruct((blocks, chunk, HEAD), BF16),
@@ -289,7 +300,12 @@
         compiler_params=pltpu.CompilerParams(vmem_limit_bytes=12 * 1024 * 1024),
         name="block_scan",
     )((sp_at >= blocks // 2).astype(jnp.int32)[None], got)
-    enter = lax.all_to_all(give, SP, 0, 0, tiled=True).reshape(2 * heads, HEAD, HEAD)
+    enter = lax.all_to_all(give, SP, 0, 0, tiled=True)
+    ups.append(shift(ups[0], "sp_0", 1))
+    downs.append(shift(downs[0], "sp_0", z_size - 1))
+    crossed = [shift(piece, "sp_2", 1) for piece in (line, ups[0], downs[0])]
+    crossed, enter = lax.optimization_barrier((crossed, enter))
+    enter = enter.reshape(2 * heads, HEAD, HEAD)
 
     part = rows // n_tp
     parts = pl.pallas_call(
@@ -301,6 +317,10 @@
         name="norm_project",
     )(tp_at[None], near, reach, enter, output_gate_logits, head_norm_gain[None], output_weight)
 
+    ups[1], downs[1], parts = lax.optimization_barrier((ups[1], downs[1], parts))
+    ups.append(shift(ups[1], "sp_0", 1))
+    downs.append(shift(downs[1], "sp_0", z_size - 1))
+    crossed += [shift(piece, "sp_2", 1) for piece in (ups[1], downs[1])]
     arrived = [parts[0]] + [shift(parts[d], "tp", d) for d in range(1, n_tp)]
     own_resid = lax.dynamic_slice_in_dim(residual, tp_at * part, part, 0)
     hidden_f = own_resid.astype(F32)
@@ -314,21 +334,30 @@
         * mixer_norm_gain.astype(F32)
     ).astype(BF16)
     swap = [(k, k ^ 1) for k in range(y_size)]
+    ups[2], downs[2], crossed, normed = lax.optimization_barrier((ups[2], downs[2], crossed, normed))
+    far = shift(ups[2][: y_size // 2], "sp_0", 1)
+    far_back = shift(downs[2][y_size // 2 :], "sp_0", z_size - 1)
+    crossed = crossed + [shift(piece, "sp_2", 1) for piece in (ups[2], downs[2])]
     split = model // 2
     left, right = normed[:, :split], normed[:, split:]
     both = jnp.concatenate([right, lax.ppermute(right, "sp_1", swap)], axis=0)
     own = jnp.concatenate([left] + [shift(left, "tp", d) for d in range(1, n_tp)], axis=0)
     lines = [both] + [shift(both, "tp", d) for d in range(1, n_tp)]
     tokens = [own, lax.ppermute(own, "sp_1", swap)] + lines
+    crossed = crossed + [shift(piece, "sp_2", 1) for piece in (far, far_back)]
+    near_line, u1, d1, u2, d2, u3, d3, f, g = crossed
+    pieces = [line] + ups + [far, far_back] + downs[::-1]
+    pieces += [near_line, u1, u2, u3, f, g, d3, d2, d1]
+    at = jnp.stack([y_at, lax.axis_index("sp_0"), lax.axis_index("sp_2")])
     weights = pl.pallas_call(
         in_order_body,
         out_shape=jax.ShapeDtypeStruct((z_size, y_size, cores, slab, wide), BF16),
-        in_specs=[SMEM, ANY],
+        in_specs=[SMEM] + [ANY] * len(pieces),
         out_specs=VMEM,
-        scratch_shapes=[pltpu.SemaphoreType.DMA((y_size * cores,))],
-        compiler_params=pltpu.CompilerParams(vmem_limit_bytes=40 * 1024 * 1024),
+        scratch_shapes=[pltpu.SemaphoreType.DMA((z_size * y_size * cores,))],
+        compiler_params=pltpu.CompilerParams(vmem_limit_bytes=28 * 1024 * 1024),
         name="weights_in_order",
-    )(y_at[None], whole)
+    )(at, *pieces)
     weights = weights.reshape(model, wide)
     lowered = pl.pallas_call(
         lambda *refs: mixer_body(*refs, hidden=hidden),

time: 139 us -> 160 us (1.15)
  the two profiles are of different devices: /device:TPU:6 before, /device:TPU:24 now
where the time goes in v5:
time: 160 us
  waiting for transfers between devices  73.3 us (46%)
  starting transfers between devices  58.4 us (36%)
  Pallas kernels  23.9 us (15%)
  other arithmetic  3.21 us (2%)
    ppermute x35, waiting for transfers between devices, shift(): lax.ppermute(array, axis, [(k, (k + by) % size) for k in range(size)])  57.4 us
    ppermute x35, starting transfers between devices, shift(): lax.ppermute(array, axis, [(k, (k + by) % size) for k in range(size)])  33.9 us
    pallas_call x1, Pallas kernels, local(): pl.pallas_call(in_order_body, out_shape=jax.ShapeDtypeStruct((z_size, y_s...  13.3 us
    all_to_all x1, starting transfers between devices, local(): got = lax.all_to_all(send, SP, 0, 0, tiled=True)  12.3 us
    all_to_all x1, waiting for transfers between devices, local(): enter = lax.all_to_all(give, SP, 0, 0, tiled=True)  11 us
    all_to_all x1, starting transfers between devices, local(): enter = lax.all_to_all(give, SP, 0, 0, tiled=True)  7.83 us
    ppermute x1, waiting for transfers between devices, local(): both = jnp.concatenate([right, lax.ppermute(right, 'sp_1', swap)], axis=0)  4.92 us
    pallas_call x1, Pallas kernels, local(): pl.pallas_call(local_body, out_shape=(jax.ShapeDtypeStruct((blocks, chunk...  3.63 us
  transfers between devices with their start and end apart: 41, of which 15 were waited for; matrix products, arithmetic and copies ran while one was open for 2% of the time, Pallas kernels for 11%

profile of v5, /device:TPU:24, one launch (start us, length us, event | category | flops | bytes accessed | tf_op | source)
XLA Modules:
  0.0 159.8 jit_solution(5435805883018921163)
XLA Ops:
  0.0 3.6 %local_sweep.1 = (bf16[64,24,128]{2,1,0:T(8,128)(2,1)}, f32[128,512]{1,0:T(8,128)}, bf16[2,128,512]{2,1,0:T(8,128)(2,1)}, bf16[32,2176]{1,0:T(8,128)(2,1)}, bf16[32,2176]{1,0:T(8,128)(2,1)}) custom-call(s32[1]{0:T(128)} %bitcast.parity_ref, bf16[128,512]{1,0:T(8,128)(2,1)} %q_ref.1, bf16[2,128,512]{2,1,0:T(8,128)(2,1)} %f_ref.1, bf16[128,512]{1,0:T(8,128)(2,1)} %v_ref.1, ...), custom_call_target="tpu_custom_call" | custom-call | tf_op jit(solution)/shard_map/local_sweep/pallas_call | solution.py:267
  3.6 1.9 %collective-permute-start = (bf16[32,2176]{1,0:T(8,128)(2,1)}, bf16[32,2176]{1,0:T(8,128)(2,1)S(1)}, u32[]{:S(2)}, u32[]{:S(2)}) collective-permute-start(bf16[32,2176]{1,0:T(8,128)(2,1)} %get-tuple-element.39), channel_id=1, source_target_pairs={{0,8},{8,16},{16,24},{24,0},{1,9},{9,17},{17,25},{25,1},{2,10},{10... | collective-permute-start | bytes 417800 | tf_op jit(solution)/shard_map/ppermute | solution.py:235
  5.5 0.9 collective-permute-start.1
  6.4 0.1 collective-permute-start.2
  6.5 12.3 %all-to-all-start = ((bf16[64,24,128]{2,1,0:T(8,128)(2,1)}), bf16[64,24,128]{2,1,0:T(8,128)(2,1)S(1)}, u32[]{:S(2)}, u32[]{:S(2)}) async-start(bf16[64,24,128]{2,1,0:T(8,128)(2,1)} %get-tuple-element.42), calls=%async_computation | async-start | bytes 786432 | tf_op jit(solution)/shard_map/all_to_all | solution.py:290
  18.8 0.0 collective-permute-done.1
  18.8 0.0 collective-permute-done.2
  18.9 0.9 pad_maximum_fusion
  19.8 1.5 collective-permute-start.3
  21.4 1.8 %collective-permute-start.5 = (bf16[4,32,2176]{2,1,0:T(8,128)(2,1)S(1)}, bf16[4,32,2176]{2,1,0:T(8,128)(2,1)S(1)}, u32[]{:S(2)}, u32[]{:S(2)}) collective-permute-start(bf16[4,32,2176]{2,1,0:T(8,128)(2,1)S(1)} %bitcast.15), channel_id=1, source_target_pairs={{0,224},{32,0},{64,32},{96,64},{128,96},{160,128},{192,160},{224,1... | collective-permute-start | bytes 1671176 | tf_op jit(solution)/shard_map/ppermute | solution.py:235
  23.1 19.9 %collective-permute-done.3.refs_1_ = bf16[4,32,2176]{2,1,0:T(8,128)(2,1)S(1)} collective-permute-done((bf16[4,32,2176]{2,1,0:T(8,128)(2,1)S(1)}, bf16[4,32,2176]{2,1,0:T(8,128)(2,1)S(1)}, u32[]{:S(2)}, u32[]{:S(2)}) %collective-permute-start.3) | collective-permute-done | bytes 557088 | tf_op jit(solution)/shard_map/ppermute | solution.py:235
  43.0 0.0 collective-permute-done.5.refs_8_
  43.0 0.5 collective-permute-start.9
  43.5 3.2 %collective-permute-start.6 = (bf16[4,32,2176]{2,1,0:T(8,128)(2,1)S(1)}, bf16[4,32,2176]{2,1,0:T(8,128)(2,1)}, u32[]{:S(2)}, u32[]{:S(2)}) collective-permute-start(bf16[4,32,2176]{2,1,0:T(8,128)(2,1)S(1)} %collective-permute-done.5.refs_8_), channel_id=1, source_target_pairs={{0,224},{32,0},{64,32},{96,64},{128,96},{160,128},{192,160},{224,1... | collective-permute-start | bytes 1671176 | tf_op jit(solution)/shard_map/ppermute | solution.py:235
  46.7 0.8 block_scan.1
  47.6 7.8 %all-to-all-start.1 = ((bf16[64,16,128]{2,1,0:T(8,128)(2,1)}), bf16[64,16,128]{2,1,0:T(8,128)(2,1)S(1)}, u32[]{:S(2)}, u32[]{:S(2)}) async-start(bf16[64,16,128]{2,1,0:T(8,128)(2,1)} %block_scan.1), calls=%async_computation.1 | async-start | bytes 524288 | tf_op jit(solution)/shard_map/all_to_all | solution.py:303
  55.4 11.0 %all-to-all-done.1 = bf16[64,16,128]{2,1,0:T(8,128)(2,1)S(1)} async-done(((bf16[64,16,128]{2,1,0:T(8,128)(2,1)}), bf16[64,16,128]{2,1,0:T(8,128)(2,1)S(1)}, u32[]{:S(2)}, u32[]{:S(2)}) %all-to-all-start.1) | async-done | bytes 262176 | tf_op jit(solution)/shard_map/all_to_all | solution.py:303
  66.4 0.7 copy-done
  67.1 3.5 %norm_project.1 = (bf16[32,2048]{1,0:T(8,128)(2,1)}, bf16[32,2048]{1,0:T(8,128)(2,1)}, bf16[32,2048]{1,0:T(8,128)(2,1)}, bf16[32,2048]{1,0:T(8,128)(2,1)}) custom-call(s32[1]{0:T(128)} %bitcast.5.own_ref, f32[128,512]{1,0:T(8,128)} %get-tuple-element.40.near_ref, bf16[2,128,512]{2,1,0:T(8,128)(2,1)} %get-tuple-element.41.reach_ref, ...), custom_call_target="tpu_custom_call" | custom-call | tf_op jit(solution)/shard_map/norm_project/pallas_call | solution.py:311
  70.6 1.6 collective-permute-start.10
  72.2 2.7 %collective-permute-start.11 = (bf16[32,2048]{1,0:T(8,128)(2,1)}, bf16[32,2048]{1,0:T(8,128)(2,1)S(1)}, u32[]{:S(2)}, u32[]{:S(2)}) collective-permute-start(bf16[32,2048]{1,0:T(8,128)(2,1)} %get-tuple-element.50), channel_id=1, source_target_pairs={{0,2},{1,3},{2,0},{3,1},{4,6},{5,7},{6,4},{7,5},{8,10},{9,11},{10,... | collective-permute-start | bytes 393224 | tf_op jit(solution)/shard_map/ppermute | solution.py:235
  74.9 1.4 collective-permute-start.12
  76.4 2.7 %collective-permute-start.13 = (bf16[4,32,2176]{2,1,0:T(8,128)(2,1)}, bf16[4,32,2176]{2,1,0:T(8,128)(2,1)S(1)}, u32[]{:S(2)}, u32[]{:S(2)}) collective-permute-start(bf16[4,32,2176]{2,1,0:T(8,128)(2,1)} %collective-permute-done.4.refs_2_), channel_id=1, source_target_pairs={{0,32},{32,64},{64,96},{96,128},{128,160},{160,192},{192,224},{224... | collective-permute-start | bytes 1671176 | tf_op jit(solution)/shard_map/ppermute | solution.py:235
  79.1 0.5 collective-permute-start.14
  79.6 1.1 collective-permute-done.11
  80.7 0.1 collective-permute-done.12
  80.7 1.2 fusion
  81.9 0.1 fusion.2
  82.0 8.8 %collective-permute-done.13.refs_3_ = bf16[4,32,2176]{2,1,0:T(8,128)(2,1)S(1)} collective-permute-done((bf16[4,32,2176]{2,1,0:T(8,128)(2,1)}, bf16[4,32,2176]{2,1,0:T(8,128)(2,1)S(1)}, u32[]{:S(2)}, u32[]{:S(2)}) %collective-permute-start.13) | collective-permute-done | bytes 557088 | tf_op jit(solution)/shard_map/ppermute | solution.py:235
  90.8 3.5 %collective-permute-done.14.refs_6_ = bf16[4,32,2176]{2,1,0:T(8,128)(2,1)S(1)} collective-permute-done((bf16[4,32,2176]{2,1,0:T(8,128)(2,1)}, bf16[4,32,2176]{2,1,0:T(8,128)(2,1)S(1)}, u32[]{:S(2)}, u32[]{:S(2)}) %collective-permute-start.14) | collective-permute-done | bytes 557088 | tf_op jit(solution)/shard_map/ppermute | solution.py:235
  94.4 0.1 collective-permute-start.27
  94.5 0.3 collective-permute-start.25
  94.8 3.1 %collective-permute-start.26 = (bf16[2,32,2176]{2,1,0:T(8,128)(2,1)S(1)}, bf16[2,32,2176]{2,1,0:T(8,128)(2,1)S(1)}, u32[]{:S(2)}, u32[]{:S(2)}) collective-permute-start(bf16[2,32,2176]{2,1,0:T(8,128)(2,1)S(1)} %slice.44), channel_id=1, source_target_pairs={{0,224},{32,0},{64,32},{96,64},{128,96},{160,128},{192,160},{224,1... | collective-permute-start | bytes 835592 | tf_op jit(solution)/shard_map/ppermute | solution.py:235
  97.9 0.7 collective-permute-start.17
  98.6 4.9 %collective-permute-done.17 = bf16[32,1024]{1,0:T(8,128)(2,1)S(1)} collective-permute-done((bf16[32,1024]{1,0:T(8,128)(2,1)S(1)}, bf16[32,1024]{1,0:T(8,128)(2,1)S(1)}, u32[]{:S(2)}, u32[]{:S(2)}) %collective-permute-start.17) | collective-permute-done | bytes 65568 | tf_op jit(solution)/shard_map/ppermute | solution.py:235
  103.5 5.8 %collective-permute-done.18 = bf16[32,1024]{1,0:T(8,128)(2,1)S(1)} collective-permute-done((bf16[32,1024]{1,0:T(8,128)(2,1)S(1)}, bf16[32,1024]{1,0:T(8,128)(2,1)S(1)}, u32[]{:S(2)}, u32[]{:S(2)}) %collective-permute-start.18) | collective-permute-done | bytes 65568 | tf_op jit(solution)/shard_map/ppermute | solution.py:235
  109.3 0.5 collective-permute-start.29
  109.8 3.7 %collective-permute-done.19 = bf16[32,1024]{1,0:T(8,128)(2,1)S(1)} collective-permute-done((bf16[32,1024]{1,0:T(8,128)(2,1)S(1)}, bf16[32,1024]{1,0:T(8,128)(2,1)S(1)}, u32[]{:S(2)}, u32[]{:S(2)}) %collective-permute-start.19) | collective-permute-done | bytes 65568 | tf_op jit(solution)/shard_map/ppermute | solution.py:235
  113.5 0.0 collective-permute-start.21
  113.5 4.9 %collective-permute-done.21 = bf16[32,1024]{1,0:T(8,128)(2,1)S(1)} collective-permute-done((bf16[32,1024]{1,0:T(8,128)(2,1)S(1)}, bf16[32,1024]{1,0:T(8,128)(2,1)S(1)}, u32[]{:S(2)}, u32[]{:S(2)}) %collective-permute-start.21) | collective-permute-done | bytes 65568 | tf_op jit(solution)/shard_map/ppermute | solution.py:343
  118.5 0.0 collective-permute-start.20
  118.5 0.1 collective-permute-start.22
  118.6 2.7 %collective-permute-start.23 = (bf16[64,1024]{1,0:T(8,128)(2,1)S(1)}, bf16[64,1024]{1,0:T(8,128)(2,1)S(1)}, u32[]{:S(2)}, u32[]{:S(2)}) collective-permute-start(bf16[64,1024]{1,0:T(8,128)(2,1)S(1)} %pad_maximum_fusion.2.refs_3_), channel_id=1, source_target_pairs={{0,2},{1,3},{2,0},{3,1},{4,6},{5,7},{6,4},{7,5},{8,10},{9,11},{10,... | collective-permute-start | bytes 393224 | tf_op jit(solution)/shard_map/ppermute | solution.py:235
  121.3 0.9 collective-permute-start.24
  122.1 0.1 pad_add_fusion.at_ref
  122.2 13.3 %weights_in_order.1 = bf16[8,4,2,32,2176]{4,3,2,1,0:T(8,128)(2,1)S(1)} custom-call(s32[3]{0:T(128)S(1)} %pad_add_fusion.at_ref, bf16[4,32,2176]{2,1,0:T(8,128)(2,1)S(1)} %bitcast.17, bf16[4,32,2176]{2,1,0:T(8,128)(2,1)S(1)} %collective-permute-done.3.refs_1_, bf16[4,32,2176]{2,1,0:T(8,128)(2,1)} %collective-permute-done.4.refs_2_, ...), custom_call_target="tpu_custom_call" | custom-call | tf_op jit(solution)/shard_map/weights_in_order/pallas_call | solution.py:352
  135.5 2.6 %channel_mixer.1 = (f32[64,1024]{1,0:T(8,128)S(1)}, bf16[64,1024]{1,0:T(8,128)(2,1)S(1)}, bf16[64,1024]{1,0:T(8,128)(2,1)S(1)}, bf16[64,1024]{1,0:T(8,128)(2,1)S...) custom-call(s32[1]{0:T(128)} %bitcast.9.refs_0_, bf16[128,1024]{1,0:T(8,128)(2,1)S(1)} %pad_maximum_fusion.1.refs_1_, ...), custom_call_target="tpu_custom_call" | custom-call | tf_op jit(solution)/shard_map/channel_mixer/pallas_call | solution.py:362
  138.2 0.7 collective-permute-start.31
  138.9 2.6 %collective-permute-start.32 = (bf16[64,1024]{1,0:T(8,128)(2,1)S(1)}, bf16[64,1024]{1,0:T(8,128)(2,1)S(1)}, u32[]{:S(2)}, u32[]{:S(2)}) collective-permute-start(bf16[64,1024]{1,0:T(8,128)(2,1)S(1)} %get-tuple-element.67), channel_id=1, source_target_pairs={{0,2},{1,3},{2,0},{3,1},{4,6},{5,7},{6,4},{7,5},{8,10},{9,11},{10,... | collective-permute-start | bytes 393224 | tf_op jit(solution)/shard_map/ppermute | solution.py:235
  141.5 0.8 collective-permute-start.33
  142.3 2.0 %collective-permute-start.35 = (bf16[128,1024]{1,0:T(8,128)(2,1)S(1)}, bf16[128,1024]{1,0:T(8,128)(2,1)S(1)}, u32[]{:S(2)}, u32[]{:S(2)}) collective-permute-start(bf16[128,1024]{1,0:T(8,128)(2,1)S(1)} %get-tuple-element.70), channel_id=1, source_target_pairs={{0,8},{8,0},{16,24},{24,16},{1,9},{9,1},{17,25},{25,17},{2,10},{10... | collective-permute-start | bytes 786440 | tf_op jit(solution)/shard_map/ppermute | solution.py:373
  144.3 1.1 collective-permute-done.32
  145.4 3.1 %collective-permute-done.33 = bf16[64,1024]{1,0:T(8,128)(2,1)S(1)} collective-permute-done((bf16[64,1024]{1,0:T(8,128)(2,1)S(1)}, bf16[64,1024]{1,0:T(8,128)(2,1)S(1)}, u32[]{:S(2)}, u32[]{:S(2)}) %collective-permute-start.33) | collective-permute-done | bytes 131104 | tf_op jit(solution)/shard_map/ppermute | solution.py:235
  148.5 0.1 convert_add_fusion.1
  148.6 2.2 %collective-permute-start.34 = (bf16[32,1024]{1,0:T(8,128)(2,1)S(1)}, bf16[32,1024]{1,0:T(8,128)(2,1)S(1)}, u32[]{:S(2)}, u32[]{:S(2)}) collective-permute-start(bf16[32,1024]{1,0:T(8,128)(2,1)S(1)} %slice.77), channel_id=1, source_target_pairs={{0,8},{8,0},{16,24},{24,16},{1,9},{9,1},{17,25},{25,17},{2,10},{10... | collective-permute-start | bytes 196616 | tf_op jit(solution)/shard_map/ppermute | solution.py:382
  150.8 0.1 fusion.9
  150.9 0.3 collective-permute-start.36
  151.3 2.3 %collective-permute-start.37 = (bf16[32,1024]{1,0:T(8,128)(2,1)S(1)}, bf16[32,1024]{1,0:T(8,128)(2,1)S(1)}, u32[]{:S(2)}, u32[]{:S(2)}) collective-permute-start(bf16[32,1024]{1,0:T(8,128)(2,1)S(1)} %get-tuple-element.77), channel_id=1, source_target_pairs={{0,2},{1,3},{2,0},{3,1},{4,6},{5,7},{6,4},{7,5},{8,10},{9,11},{10,... | collective-permute-start | bytes 196616 | tf_op jit(solution)/shard_map/ppermute | solution.py:235
  153.6 0.0 collective-permute-start.38
  153.6 1.7 %collective-permute-done.36 = bf16[32,1024]{1,0:T(8,128)(2,1)S(1)} collective-permute-done((bf16[32,1024]{1,0:T(8,128)(2,1)S(1)}, bf16[32,1024]{1,0:T(8,128)(2,1)S(1)}, u32[]{:S(2)}, u32[]{:S(2)}) %collective-permute-start.36) | collective-permute-done | bytes 65568 | tf_op jit(solution)/shard_map/ppermute | solution.py:235
  155.3 1.7 %collective-permute-done.37 = bf16[32,1024]{1,0:T(8,128)(2,1)S(1)} collective-permute-done((bf16[32,1024]{1,0:T(8,128)(2,1)S(1)}, bf16[32,1024]{1,0:T(8,128)(2,1)S(1)}, u32[]{:S(2)}, u32[]{:S(2)}) %collective-permute-start.37) | collective-permute-done | bytes 65568 | tf_op jit(solution)/shard_map/ppermute | solution.py:235
  157.0 2.0 %collective-permute-done.38 = bf16[32,1024]{1,0:T(8,128)(2,1)S(1)} collective-permute-done((bf16[32,1024]{1,0:T(8,128)(2,1)S(1)}, bf16[32,1024]{1,0:T(8,128)(2,1)S(1)}, u32[]{:S(2)}, u32[]{:S(2)}) %collective-permute-start.38) | collective-permute-done | bytes 65568 | tf_op jit(solution)/shard_map/ppermute | solution.py:235
  159.1 0.1 fusion.8
  159.1 0.7 pad_maximum_fusion.3
  (44 shorter events, 0.2 us)
Async XLA Ops:
  3.6 15.2 %collective-permute-start = (bf16[32,2176]{1,0:T(8,128)(2,1)}, bf16[32,2176]{1,0:T(8,128)(2,1)S(1)}, u32[]{:S(2)}, u32[]{:S(2)}) collective-permute-start(bf16[32,2176]{1,0:T(8,128)(2,1)} %get-tuple-element.39), channel_id=1, source_target_pairs={{0,8},{8,16},{16,24},{24,0},{1,9},{9,17},{17,25},{25,1},{2,10},{10... | collective-permute-start | bytes 417800 | tf_op jit(solution)/shard_map/ppermute | solution.py:235
  5.5 13.3 %collective-permute-start.1 = (bf16[32,2176]{1,0:T(8,128)(2,1)}, bf16[32,2176]{1,0:T(8,128)(2,1)S(1)}, u32[]{:S(2)}, u32[]{:S(2)}) collective-permute-start(bf16[32,2176]{1,0:T(8,128)(2,1)} %get-tuple-element.38), channel_id=1, source_target_pairs={{0,16},{8,24},{16,0},{24,8},{1,17},{9,25},{17,1},{25,9},{2,18},{10... | collective-permute-start | bytes 417800 | tf_op jit(solution)/shard_map/ppermute | solution.py:235
  6.4 12.4 %collective-permute-start.2 = (bf16[32,2176]{1,0:T(8,128)(2,1)}, bf16[32,2176]{1,0:T(8,128)(2,1)S(1)}, u32[]{:S(2)}, u32[]{:S(2)}) collective-permute-start(bf16[32,2176]{1,0:T(8,128)(2,1)} %get-tuple-element.39), channel_id=1, source_target_pairs={{0,24},{8,0},{16,8},{24,16},{1,25},{9,1},{17,9},{25,17},{2,26},{10... | collective-permute-start | bytes 417800 | tf_op jit(solution)/shard_map/ppermute | solution.py:235
  6.5 40.2 %all-to-all-start = ((bf16[64,24,128]{2,1,0:T(8,128)(2,1)}), bf16[64,24,128]{2,1,0:T(8,128)(2,1)S(1)}, u32[]{:S(2)}, u32[]{:S(2)}) async-start(bf16[64,24,128]{2,1,0:T(8,128)(2,1)} %get-tuple-element.42), calls=%async_computation | async-start | bytes 786432 | tf_op jit(solution)/shard_map/all_to_all | solution.py:290
  19.8 23.2 %collective-permute-start.3 = (bf16[4,32,2176]{2,1,0:T(8,128)(2,1)S(1)}, bf16[4,32,2176]{2,1,0:T(8,128)(2,1)S(1)}, u32[]{:S(2)}, u32[]{:S(2)}) collective-permute-start(bf16[4,32,2176]{2,1,0:T(8,128)(2,1)S(1)} %bitcast.14), channel_id=1, source_target_pairs={{0,32},{32,64},{64,96},{96,128},{128,160},{160,192},{192,224},{224... | collective-permute-start | bytes 1671176 | tf_op jit(solution)/shard_map/ppermute | solution.py:235
  21.4 21.6 %collective-permute-start.5 = (bf16[4,32,2176]{2,1,0:T(8,128)(2,1)S(1)}, bf16[4,32,2176]{2,1,0:T(8,128)(2,1)S(1)}, u32[]{:S(2)}, u32[]{:S(2)}) collective-permute-start(bf16[4,32,2176]{2,1,0:T(8,128)(2,1)S(1)} %bitcast.15), channel_id=1, source_target_pairs={{0,224},{32,0},{64,32},{96,64},{128,96},{160,128},{192,160},{224,1... | collective-permute-start | bytes 1671176 | tf_op jit(solution)/shard_map/ppermute | solution.py:235
  23.1 32.3 %collective-permute-start.7 = (bf16[4,32,2176]{2,1,0:T(8,128)(2,1)S(1)}, bf16[4,32,2176]{2,1,0:T(8,128)(2,1)S(1)}, u32[]{:S(2)}, u32[]{:S(2)}) collective-permute-start(bf16[4,32,2176]{2,1,0:T(8,128)(2,1)S(1)} %bitcast.16), channel_id=1, source_target_pairs={{0,4},{4,0},{1,5},{5,1},{2,6},{6,2},{3,7},{7,3},{8,12},{12,8},{9,1... | collective-permute-start | bytes 1671176 | tf_op jit(solution)/shard_map/ppermute | solution.py:235
  43.0 12.4 %collective-permute-start.8 = (bf16[4,32,2176]{2,1,0:T(8,128)(2,1)S(1)}, bf16[4,32,2176]{2,1,0:T(8,128)(2,1)S(1)}, u32[]{:S(2)}, u32[]{:S(2)}) collective-permute-start(bf16[4,32,2176]{2,1,0:T(8,128)(2,1)S(1)} %collective-permute-done.3.refs_1_), channel_id=1, source_target_pairs={{0,4},{4,0},{1,5},{5,1},{2,6},{6,2},{3,7},{7,3},{8,12},{12,8},{9,1... | collective-permute-start | bytes 1671176 | tf_op jit(solution)/shard_map/ppermute | solution.py:235
  43.0 12.4 %collective-permute-start.9 = (bf16[4,32,2176]{2,1,0:T(8,128)(2,1)S(1)}, bf16[4,32,2176]{2,1,0:T(8,128)(2,1)}, u32[]{:S(2)}, u32[]{:S(2)}) collective-permute-start(bf16[4,32,2176]{2,1,0:T(8,128)(2,1)S(1)} %collective-permute-done.5.refs_8_), channel_id=1, source_target_pairs={{0,4},{4,0},{1,5},{5,1},{2,6},{6,2},{3,7},{7,3},{8,12},{12,8},{9,1... | collective-permute-start | bytes 1671176 | tf_op jit(solution)/shard_map/ppermute | solution.py:235
  43.5 27.1 %collective-permute-start.4 = (bf16[4,32,2176]{2,1,0:T(8,128)(2,1)S(1)}, bf16[4,32,2176]{2,1,0:T(8,128)(2,1)}, u32[]{:S(2)}, u32[]{:S(2)}) collective-permute-start(bf16[4,32,2176]{2,1,0:T(8,128)(2,1)S(1)} %collective-permute-done.3.refs_1_), channel_id=1, source_target_pairs={{0,32},{32,64},{64,96},{96,128},{128,160},{160,192},{192,224},{224... | collective-permute-start | bytes 1671176 | tf_op jit(solution)/shard_map/ppermute | solution.py:235
  43.5 27.1 %collective-permute-start.6 = (bf16[4,32,2176]{2,1,0:T(8,128)(2,1)S(1)}, bf16[4,32,2176]{2,1,0:T(8,128)(2,1)}, u32[]{:S(2)}, u32[]{:S(2)}) collective-permute-start(bf16[4,32,2176]{2,1,0:T(8,128)(2,1)S(1)} %collective-permute-done.5.refs_8_), channel_id=1, source_target_pairs={{0,224},{32,0},{64,32},{96,64},{128,96},{160,128},{192,160},{224,1... | collective-permute-start | bytes 1671176 | tf_op jit(solution)/shard_map/ppermute | solution.py:235
  47.6 18.8 %all-to-all-start.1 = ((bf16[64,16,128]{2,1,0:T(8,128)(2,1)}), bf16[64,16,128]{2,1,0:T(8,128)(2,1)S(1)}, u32[]{:S(2)}, u32[]{:S(2)}) async-start(bf16[64,16,128]{2,1,0:T(8,128)(2,1)} %block_scan.1), calls=%async_computation.1 | async-start | bytes 524288 | tf_op jit(solution)/shard_map/all_to_all | solution.py:303
  66.4 0.7 copy-start
  67.1 9.3 %copy-start.1 = (bf16[2048]{0:T(1024)(128)(2,1)S(1)}, bf16[2048]{0:T(1024)(128)(2,1)}, u32[]{:S(2)}) copy-start(bf16[2048]{0:T(1024)(128)(2,1)} %param.22) | copy-start | bytes 12292
  70.6 8.5 %collective-permute-start.10 = (bf16[32,2048]{1,0:T(8,128)(2,1)}, bf16[32,2048]{1,0:T(8,128)(2,1)S(1)}, u32[]{:S(2)}, u32[]{:S(2)}) collective-permute-start(bf16[32,2048]{1,0:T(8,128)(2,1)} %get-tuple-element.49), channel_id=1, source_target_pairs={{0,1},{1,2},{2,3},{3,0},{4,5},{5,6},{6,7},{7,4},{8,9},{9,10},{10,1... | collective-permute-start | bytes 393224 | tf_op jit(solution)/shard_map/ppermute | solution.py:235
  72.2 8.5 %collective-permute-start.11 = (bf16[32,2048]{1,0:T(8,128)(2,1)}, bf16[32,2048]{1,0:T(8,128)(2,1)S(1)}, u32[]{:S(2)}, u32[]{:S(2)}) collective-permute-start(bf16[32,2048]{1,0:T(8,128)(2,1)} %get-tuple-element.50), channel_id=1, source_target_pairs={{0,2},{1,3},{2,0},{3,1},{4,6},{5,7},{6,4},{7,5},{8,10},{9,11},{10,... | collective-permute-start | bytes 393224 | tf_op jit(solution)/shard_map/ppermute | solution.py:235
  74.9 5.8 %collective-permute-start.12 = (bf16[32,2048]{1,0:T(8,128)(2,1)}, bf16[32,2048]{1,0:T(8,128)(2,1)S(1)}, u32[]{:S(2)}, u32[]{:S(2)}) collective-permute-start(bf16[32,2048]{1,0:T(8,128)(2,1)} %get-tuple-element.51), channel_id=1, source_target_pairs={{0,3},{1,0},{2,1},{3,2},{4,7},{5,4},{6,5},{7,6},{8,11},{9,8},{10,9... | collective-permute-start | bytes 393224 | tf_op jit(solution)/shard_map/ppermute | solution.py:235
  76.4 14.5 %collective-permute-start.13 = (bf16[4,32,2176]{2,1,0:T(8,128)(2,1)}, bf16[4,32,2176]{2,1,0:T(8,128)(2,1)S(1)}, u32[]{:S(2)}, u32[]{:S(2)}) collective-permute-start(bf16[4,32,2176]{2,1,0:T(8,128)(2,1)} %collective-permute-done.4.refs_2_), channel_id=1, source_target_pairs={{0,32},{32,64},{64,96},{96,128},{128,160},{160,192},{192,224},{224... | collective-permute-start | bytes 1671176 | tf_op jit(solution)/shard_map/ppermute | solution.py:235
  79.1 15.3 %collective-permute-start.15 = (bf16[4,32,2176]{2,1,0:T(8,128)(2,1)}, bf16[4,32,2176]{2,1,0:T(8,128)(2,1)S(1)}, u32[]{:S(2)}, u32[]{:S(2)}) collective-permute-start(bf16[4,32,2176]{2,1,0:T(8,128)(2,1)} %collective-permute-done.4.refs_2_), channel_id=1, source_target_pairs={{0,4},{4,0},{1,5},{5,1},{2,6},{6,2},{3,7},{7,3},{8,12},{12,8},{9,1... | collective-permute-start | bytes 1671176 | tf_op jit(solution)/shard_map/ppermute | solution.py:235
  79.1 15.2 %collective-permute-start.14 = (bf16[4,32,2176]{2,1,0:T(8,128)(2,1)}, bf16[4,32,2176]{2,1,0:T(8,128)(2,1)S(1)}, u32[]{:S(2)}, u32[]{:S(2)}) collective-permute-start(bf16[4,32,2176]{2,1,0:T(8,128)(2,1)} %collective-permute-done.6.refs_7_), channel_id=1, source_target_pairs={{0,224},{32,0},{64,32},{96,64},{128,96},{160,128},{192,160},{224,1... | collective-permute-start | bytes 1671176 | tf_op jit(solution)/shard_map/ppermute | solution.py:235
  80.7 13.7 %collective-permute-start.16 = (bf16[4,32,2176]{2,1,0:T(8,128)(2,1)}, bf16[4,32,2176]{2,1,0:T(8,128)(2,1)S(1)}, u32[]{:S(2)}, u32[]{:S(2)}) collective-permute-start(bf16[4,32,2176]{2,1,0:T(8,128)(2,1)} %collective-permute-done.6.refs_7_), channel_id=1, source_target_pairs={{0,4},{4,0},{1,5},{5,1},{2,6},{6,2},{3,7},{7,3},{8,12},{12,8},{9,1... | collective-permute-start | bytes 1671176 | tf_op jit(solution)/shard_map/ppermute | solution.py:235
  94.4 26.9 %collective-permute-start.27 = (bf16[4,32,2176]{2,1,0:T(8,128)(2,1)S(1)}, bf16[4,32,2176]{2,1,0:T(8,128)(2,1)S(1)}, u32[]{:S(2)}, u32[]{:S(2)}) collective-permute-start(bf16[4,32,2176]{2,1,0:T(8,128)(2,1)S(1)} %collective-permute-done.13.refs_3_), channel_id=1, source_target_pairs={{0,4},{4,0},{1,5},{5,1},{2,6},{6,2},{3,7},{7,3},{8,12},{12,8},{9,1... | collective-permute-start | bytes 1671176 | tf_op jit(solution)/shard_map/ppermute | solution.py:235
  94.5 14.8 %collective-permute-start.25 = (bf16[2,32,2176]{2,1,0:T(8,128)(2,1)S(1)}, bf16[2,32,2176]{2,1,0:T(8,128)(2,1)S(1)}, u32[]{:S(2)}, u32[]{:S(2)}) collective-permute-start(bf16[2,32,2176]{2,1,0:T(8,128)(2,1)S(1)} %slice.43), channel_id=1, source_target_pairs={{0,32},{32,64},{64,96},{96,128},{128,160},{160,192},{192,224},{224... | collective-permute-start | bytes 835592 | tf_op jit(solution)/shard_map/ppermute | solution.py:235
  94.8 14.5 %collective-permute-start.26 = (bf16[2,32,2176]{2,1,0:T(8,128)(2,1)S(1)}, bf16[2,32,2176]{2,1,0:T(8,128)(2,1)S(1)}, u32[]{:S(2)}, u32[]{:S(2)}) collective-permute-start(bf16[2,32,2176]{2,1,0:T(8,128)(2,1)S(1)} %slice.44), channel_id=1, source_target_pairs={{0,224},{32,0},{64,32},{96,64},{128,96},{160,128},{192,160},{224,1... | collective-permute-start | bytes 835592 | tf_op jit(solution)/shard_map/ppermute | solution.py:235
  97.9 5.6 %collective-permute-start.17 = (bf16[32,1024]{1,0:T(8,128)(2,1)S(1)}, bf16[32,1024]{1,0:T(8,128)(2,1)S(1)}, u32[]{:S(2)}, u32[]{:S(2)}) collective-permute-start(bf16[32,1024]{1,0:T(8,128)(2,1)S(1)} %get-tuple-element.81), channel_id=1, source_target_pairs={{0,1},{1,2},{2,3},{3,0},{4,5},{5,6},{6,7},{7,4},{8,9},{9,10},{10,1... | collective-permute-start | bytes 196616 | tf_op jit(solution)/shard_map/ppermute | solution.py:235
  98.6 23.6 %collective-permute-start.30 = (bf16[4,32,2176]{2,1,0:T(8,128)(2,1)S(1)}, bf16[4,32,2176]{2,1,0:T(8,128)(2,1)S(1)}, u32[]{:S(2)}, u32[]{:S(2)}) collective-permute-start(bf16[4,32,2176]{2,1,0:T(8,128)(2,1)S(1)} %collective-permute-done.14.refs_6_), channel_id=1, source_target_pairs={{0,4},{4,0},{1,5},{5,1},{2,6},{6,2},{3,7},{7,3},{8,12},{12,8},{9,1... | collective-permute-start | bytes 1671176 | tf_op jit(solution)/shard_map/ppermute | solution.py:235
  103.5 5.8 %collective-permute-start.18 = (bf16[32,1024]{1,0:T(8,128)(2,1)S(1)}, bf16[32,1024]{1,0:T(8,128)(2,1)S(1)}, u32[]{:S(2)}, u32[]{:S(2)}) collective-permute-start(bf16[32,1024]{1,0:T(8,128)(2,1)S(1)} %get-tuple-element.81), channel_id=1, source_target_pairs={{0,2},{1,3},{2,0},{3,1},{4,6},{5,7},{6,4},{7,5},{8,10},{9,11},{10,... | collective-permute-start | bytes 196616 | tf_op jit(solution)/shard_map/ppermute | solution.py:235
  109.2 4.3 %collective-permute-start.19 = (bf16[32,1024]{1,0:T(8,128)(2,1)S(1)}, bf16[32,1024]{1,0:T(8,128)(2,1)S(1)}, u32[]{:S(2)}, u32[]{:S(2)}) collective-permute-start(bf16[32,1024]{1,0:T(8,128)(2,1)S(1)} %get-tuple-element.81), channel_id=1, source_target_pairs={{0,3},{1,0},{2,1},{3,2},{4,7},{5,4},{6,5},{7,6},{8,11},{9,8},{10,9... | collective-permute-start | bytes 196616 | tf_op jit(solution)/shard_map/ppermute | solution.py:235
  109.2 9.3 %collective-permute-start.28 = (bf16[2,32,2176]{2,1,0:T(8,128)(2,1)S(1)}, bf16[2,32,2176]{2,1,0:T(8,128)(2,1)S(1)}, u32[]{:S(2)}, u32[]{:S(2)}) collective-permute-start(bf16[2,32,2176]{2,1,0:T(8,128)(2,1)S(1)} %collective-permute-done.25.refs_4_), channel_id=1, source_target_pairs={{0,4},{4,0},{1,5},{5,1},{2,6},{6,2},{3,7},{7,3},{8,12},{12,8},{9,1... | collective-permute-start | bytes 835592 | tf_op jit(solution)/shard_map/ppermute | solution.py:235
  109.3 9.3 %collective-permute-start.29 = (bf16[2,32,2176]{2,1,0:T(8,128)(2,1)S(1)}, bf16[2,32,2176]{2,1,0:T(8,128)(2,1)S(1)}, u32[]{:S(2)}, u32[]{:S(2)}) collective-permute-start(bf16[2,32,2176]{2,1,0:T(8,128)(2,1)S(1)} %collective-permute-done.26.refs_5_), channel_id=1, source_target_pairs={{0,4},{4,0},{1,5},{5,1},{2,6},{6,2},{3,7},{7,3},{8,12},{12,8},{9,1... | collective-permute-start | bytes 835592 | tf_op jit(solution)/shard_map/ppermute | solution.py:235
  113.5 5.0 %collective-permute-start.21 = (bf16[32,1024]{1,0:T(8,128)(2,1)S(1)}, bf16[32,1024]{1,0:T(8,128)(2,1)S(1)}, u32[]{:S(2)}, u32[]{:S(2)}) collective-permute-start(bf16[32,1024]{1,0:T(8,128)(2,1)S(1)} %get-tuple-element.80), channel_id=1, source_target_pairs={{0,8},{8,0},{16,24},{24,16},{1,9},{9,1},{17,25},{25,17},{2,10},{10... | collective-permute-start | bytes 196616 | tf_op jit(solution)/shard_map/ppermute | solution.py:343
  118.5 17.1 %collective-permute-start.20 = (bf16[128,1024]{1,0:T(8,128)(2,1)S(1)}, bf16[128,1024]{1,0:T(8,128)(2,1)S(1)}, u32[]{:S(2)}, u32[]{:S(2)}) collective-permute-start(bf16[128,1024]{1,0:T(8,128)(2,1)S(1)} %pad_maximum_fusion.1.refs_1_), channel_id=1, source_target_pairs={{0,8},{8,0},{16,24},{24,16},{1,9},{9,1},{17,25},{25,17},{2,10},{10... | collective-permute-start | bytes 786440 | tf_op jit(solution)/shard_map/ppermute | solution.py:346
  118.5 17.0 %collective-permute-start.22 = (bf16[64,1024]{1,0:T(8,128)(2,1)S(1)}, bf16[64,1024]{1,0:T(8,128)(2,1)S(1)}, u32[]{:S(2)}, u32[]{:S(2)}) collective-permute-start(bf16[64,1024]{1,0:T(8,128)(2,1)S(1)} %pad_maximum_fusion.2.refs_3_), channel_id=1, source_target_pairs={{0,1},{1,2},{2,3},{3,0},{4,5},{5,6},{6,7},{7,4},{8,9},{9,10},{10,1... | collective-permute-start | bytes 393224 | tf_op jit(solution)/shard_map/ppermute | solution.py:235
  118.6 16.9 %collective-permute-start.23 = (bf16[64,1024]{1,0:T(8,128)(2,1)S(1)}, bf16[64,1024]{1,0:T(8,128)(2,1)S(1)}, u32[]{:S(2)}, u32[]{:S(2)}) collective-permute-start(bf16[64,1024]{1,0:T(8,128)(2,1)S(1)} %pad_maximum_fusion.2.refs_3_), channel_id=1, source_target_pairs={{0,2},{1,3},{2,0},{3,1},{4,6},{5,7},{6,4},{7,5},{8,10},{9,11},{10,... | collective-permute-start | bytes 393224 | tf_op jit(solution)/shard_map/ppermute | solution.py:235
  121.3 14.3 %collective-permute-start.24 = (bf16[64,1024]{1,0:T(8,128)(2,1)S(1)}, bf16[64,1024]{1,0:T(8,128)(2,1)S(1)}, u32[]{:S(2)}, u32[]{:S(2)}) collective-permute-start(bf16[64,1024]{1,0:T(8,128)(2,1)S(1)} %pad_maximum_fusion.2.refs_3_), channel_id=1, source_target_pairs={{0,3},{1,0},{2,1},{3,2},{4,7},{5,4},{6,5},{7,6},{8,11},{9,8},{10,9... | collective-permute-start | bytes 393224 | tf_op jit(solution)/shard_map/ppermute | solution.py:235
  138.2 6.1 %collective-permute-start.31 = (bf16[64,1024]{1,0:T(8,128)(2,1)S(1)}, bf16[64,1024]{1,0:T(8,128)(2,1)S(1)}, u32[]{:S(2)}, u32[]{:S(2)}) collective-permute-start(bf16[64,1024]{1,0:T(8,128)(2,1)S(1)} %get-tuple-element.66), channel_id=1, source_target_pairs={{0,3},{1,0},{2,1},{3,2},{4,7},{5,4},{6,5},{7,6},{8,11},{9,8},{10,9... | collective-permute-start | bytes 393224 | tf_op jit(solution)/shard_map/ppermute | solution.py:235
  138.9 6.5 %collective-permute-start.32 = (bf16[64,1024]{1,0:T(8,128)(2,1)S(1)}, bf16[64,1024]{1,0:T(8,128)(2,1)S(1)}, u32[]{:S(2)}, u32[]{:S(2)}) collective-permute-start(bf16[64,1024]{1,0:T(8,128)(2,1)S(1)} %get-tuple-element.67), channel_id=1, source_target_pairs={{0,2},{1,3},{2,0},{3,1},{4,6},{5,7},{6,4},{7,5},{8,10},{9,11},{10,... | collective-permute-start | bytes 393224 | tf_op jit(solution)/shard_map/ppermute | solution.py:235
  141.5 7.0 %collective-permute-start.33 = (bf16[64,1024]{1,0:T(8,128)(2,1)S(1)}, bf16[64,1024]{1,0:T(8,128)(2,1)S(1)}, u32[]{:S(2)}, u32[]{:S(2)}) collective-permute-start(bf16[64,1024]{1,0:T(8,128)(2,1)S(1)} %get-tuple-element.68), channel_id=1, source_target_pairs={{0,1},{1,2},{2,3},{3,0},{4,5},{5,6},{6,7},{7,4},{8,9},{9,10},{10,1... | collective-permute-start | bytes 393224 | tf_op jit(solution)/shard_map/ppermute | solution.py:235
  142.3 8.6 %collective-permute-start.35 = (bf16[128,1024]{1,0:T(8,128)(2,1)S(1)}, bf16[128,1024]{1,0:T(8,128)(2,1)S(1)}, u32[]{:S(2)}, u32[]{:S(2)}) collective-permute-start(bf16[128,1024]{1,0:T(8,128)(2,1)S(1)} %get-tuple-element.70), channel_id=1, source_target_pairs={{0,8},{8,0},{16,24},{24,16},{1,9},{9,1},{17,25},{25,17},{2,10},{10... | collective-permute-start | bytes 786440 | tf_op jit(solution)/shard_map/ppermute | solution.py:373
  148.6 5.0 %collective-permute-start.34 = (bf16[32,1024]{1,0:T(8,128)(2,1)S(1)}, bf16[32,1024]{1,0:T(8,128)(2,1)S(1)}, u32[]{:S(2)}, u32[]{:S(2)}) collective-permute-start(bf16[32,1024]{1,0:T(8,128)(2,1)S(1)} %slice.77), channel_id=1, source_target_pairs={{0,8},{8,0},{16,24},{24,16},{1,9},{9,1},{17,25},{25,17},{2,10},{10... | collective-permute-start | bytes 196616 | tf_op jit(solution)/shard_map/ppermute | solution.py:382
  150.9 4.3 %collective-permute-start.36 = (bf16[32,1024]{1,0:T(8,128)(2,1)S(1)}, bf16[32,1024]{1,0:T(8,128)(2,1)S(1)}, u32[]{:S(2)}, u32[]{:S(2)}) collective-permute-start(bf16[32,1024]{1,0:T(8,128)(2,1)S(1)} %get-tuple-element.75), channel_id=1, source_target_pairs={{0,3},{1,0},{2,1},{3,2},{4,7},{5,4},{6,5},{7,6},{8,11},{9,8},{10,9... | collective-permute-start | bytes 196616 | tf_op jit(solution)/shard_map/ppermute | solution.py:235
  151.3 5.8 %collective-permute-start.37 = (bf16[32,1024]{1,0:T(8,128)(2,1)S(1)}, bf16[32,1024]{1,0:T(8,128)(2,1)S(1)}, u32[]{:S(2)}, u32[]{:S(2)}) collective-permute-start(bf16[32,1024]{1,0:T(8,128)(2,1)S(1)} %get-tuple-element.77), channel_id=1, source_target_pairs={{0,2},{1,3},{2,0},{3,1},{4,6},{5,7},{6,4},{7,5},{8,10},{9,11},{10,... | collective-permute-start | bytes 196616 | tf_op jit(solution)/shard_map/ppermute | solution.py:235
  153.6 5.5 %collective-permute-start.38 = (bf16[32,1024]{1,0:T(8,128)(2,1)S(1)}, bf16[32,1024]{1,0:T(8,128)(2,1)S(1)}, u32[]{:S(2)}, u32[]{:S(2)}) collective-permute-start(bf16[32,1024]{1,0:T(8,128)(2,1)S(1)} %get-tuple-element.76), channel_id=1, source_target_pairs={{0,1},{1,2},{2,3},{3,0},{4,5},{5,6},{6,7},{7,4},{8,9},{9,10},{10,1... | collective-permute-start | bytes 196616 | tf_op jit(solution)/shard_map/ppermute | solution.py:235

commit v6 on v5

--- a/solution.py
+++ b/solution.py
@@ -165,32 +165,22 @@
 
 
 def in_order_body(at_ref, *refs):
-    pieces, (weights_ref, sems) = refs[:18], refs[18:]
+    pieces, weights_ref = refs[:18], refs[18]
     z_size, y_size, cores, _, _ = weights_ref.shape
     y, z, core = at_ref[0], at_ref[1], at_ref[2]
     ahead = z_size // 2
-    copies = []
     for c in range(cores):
         lines = pieces[9 * c : 9 * c + 9]
         row_core = core if c == 0 else 1 - core
         for back in range(z_size):
             at_z = lax.rem(z + z_size - back, z_size)
             for k in range(y_size):
+                at_y = lax.rem(y + y_size - k, y_size)
                 if back == ahead:
-                    source = lines[ahead].at[k] if k < 2 else lines[ahead + 1].at[k - 2]
+                    piece = lines[ahead][k] if k < 2 else lines[ahead + 1][k - 2]
                 else:
-                    source = lines[back if back < ahead else back + 1].at[k]
-                copies.append(
-                    pltpu.make_async_copy(
-                        source,
-                        weights_ref.at[at_z, lax.rem(y + y_size - k, y_size), row_core],
-                        sems.at[(c * z_size + back) * y_size + k],
-                    )
-                )
-    for copy in copies:
-        copy.start()
-    for copy in copies:
-        copy.wait()
+                    piece = lines[back if back < ahead else back + 1][k]
+                weights_ref[at_z, at_y, row_core] = piece
 
 
 def mixer_body(at_ref, *refs, hidden):
@@ -317,7 +307,6 @@
         name="norm_project",
     )(tp_at[None], near, reach, enter, output_gate_logits, head_norm_gain[None], output_weight)
 
-    ups[1], downs[1], parts = lax.optimization_barrier((ups[1], downs[1], parts))
     ups.append(shift(ups[1], "sp_0", 1))
     downs.append(shift(downs[1], "sp_0", z_size - 1))
     crossed += [shift(piece, "sp_2", 1) for piece in (ups[1], downs[1])]
@@ -334,7 +323,6 @@
         * mixer_norm_gain.astype(F32)
     ).astype(BF16)
     swap = [(k, k ^ 1) for k in range(y_size)]
-    ups[2], downs[2], crossed, normed = lax.optimization_barrier((ups[2], downs[2], crossed, normed))
     far = shift(ups[2][: y_size // 2], "sp_0", 1)
     far_back = shift(downs[2][y_size // 2 :], "sp_0", z_size - 1)
     crossed = crossed + [shift(piece, "sp_2", 1) for piece in (ups[2], downs[2])]
@@ -352,9 +340,8 @@
     weights = pl.pallas_call(
         in_order_body,
         out_shape=jax.ShapeDtypeStruct((z_size, y_size, cores, slab, wide), BF16),
-        in_specs=[SMEM] + [ANY] * len(pieces),
+        in_specs=[SMEM] + [VMEM] * len(pieces),
         out_specs=VMEM,
-        scratch_shapes=[pltpu.SemaphoreType.DMA((z_size * y_size * cores,))],
         compiler_params=pltpu.CompilerParams(vmem_limit_bytes=28 * 1024 * 1024),
         name="weights_in_order",
     )(at, *pieces)

time: 160 us -> 140 us (0.88)
  the two profiles are of different devices: /device:TPU:24 before, /device:TPU:1 now
where the time goes in v6:
time: 140 us; the launch traced here: 137 us
  starting transfers between devices  70.9 us (51%)
  waiting for transfers between devices  49.6 us (35%)
  Pallas kernels  12.7 us (9%)
  other arithmetic  3.2 us (2%)
    ppermute x35, starting transfers between devices, shift(): lax.ppermute(array, axis, [(k, (k + by) % size) for k in range(size)])  47.7 us
    ppermute x35, waiting for transfers between devices, shift(): lax.ppermute(array, axis, [(k, (k + by) % size) for k in range(size)])  39.4 us
    all_to_all x1, starting transfers between devices, local(): got = lax.all_to_all(send, SP, 0, 0, tiled=True)  10.7 us
    all_to_all x1, waiting for transfers between devices, local(): enter = lax.all_to_all(give, SP, 0, 0, tiled=True)  10.1 us
    all_to_all x1, starting transfers between devices, local(): enter = lax.all_to_all(give, SP, 0, 0, tiled=True)  7.85 us
    pallas_call x1, Pallas kernels, local(): pl.pallas_call(local_body, out_shape=(jax.ShapeDtypeStruct((blocks, chunk...  3.61 us
    pallas_call x1, Pallas kernels, local(): pl.pallas_call(project_body, out_shape=(jax.ShapeDtypeStruct((part, model...  3.53 us
  transfers between devices with their start and end apart: 41, of which 14 were waited for; matrix products, arithmetic and copies ran while one was open for 2% of the time, Pallas kernels for 5%

profile of v6, /device:TPU:1, one launch (start us, length us, event | category | flops | bytes accessed | tf_op | source)
XLA Modules:
  0.0 137.4 jit_solution(13047996078859081845)
XLA Ops:
  0.0 3.6 %local_sweep.1 = (bf16[64,24,128]{2,1,0:T(8,128)(2,1)}, f32[128,512]{1,0:T(8,128)}, bf16[2,128,512]{2,1,0:T(8,128)(2,1)}, bf16[32,2176]{1,0:T(8,128)(2,1)}, bf16[32,2176]{1,0:T(8,128)(2,1)}) custom-call(s32[1]{0:T(128)} %bitcast.1.parity_ref, bf16[128,512]{1,0:T(8,128)(2,1)} %q_ref.1, bf16[2,128,512]{2,1,0:T(8,128)(2,1)} %f_ref.1, bf16[128,512]{1,0:T(8,128)(2,1)} %v_ref.1, ...), custom_call_target="tpu_custom_call" | custom-call | tf_op jit(solution)/shard_map/local_sweep/pallas_call | solution.py:257
  3.6 2.1 %collective-permute-start = (bf16[32,2176]{1,0:T(8,128)(2,1)}, bf16[32,2176]{1,0:T(8,128)(2,1)S(1)}, u32[]{:S(2)}, u32[]{:S(2)}) collective-permute-start(bf16[32,2176]{1,0:T(8,128)(2,1)} %get-tuple-element.27), channel_id=1, source_target_pairs={{0,8},{8,16},{16,24},{24,0},{1,9},{9,17},{17,25},{25,1},{2,10},{10... | collective-permute-start | bytes 417800 | tf_op jit(solution)/shard_map/ppermute | solution.py:225
  5.7 2.6 %collective-permute-start.1 = (bf16[32,2176]{1,0:T(8,128)(2,1)}, bf16[32,2176]{1,0:T(8,128)(2,1)S(1)}, u32[]{:S(2)}, u32[]{:S(2)}) collective-permute-start(bf16[32,2176]{1,0:T(8,128)(2,1)} %get-tuple-element.26), channel_id=1, source_target_pairs={{0,16},{8,24},{16,0},{24,8},{1,17},{9,25},{17,1},{25,9},{2,18},{10... | collective-permute-start | bytes 417800 | tf_op jit(solution)/shard_map/ppermute | solution.py:225
  8.4 1.1 collective-permute-start.2
  9.4 10.7 %all-to-all-start = ((bf16[64,24,128]{2,1,0:T(8,128)(2,1)}), bf16[64,24,128]{2,1,0:T(8,128)(2,1)S(1)}, u32[]{:S(2)}, u32[]{:S(2)}) async-start(bf16[64,24,128]{2,1,0:T(8,128)(2,1)} %get-tuple-element.28), calls=%async_computation | async-start | bytes 786432 | tf_op jit(solution)/shard_map/all_to_all | solution.py:280
  20.1 0.9 pad_maximum_fusion
  21.1 1.4 %collective-permute-start.4 = (bf16[4,32,2176]{2,1,0:T(8,128)(2,1)S(1)}, bf16[4,32,2176]{2,1,0:T(8,128)(2,1)S(1)}, u32[]{:S(2)}, u32[]{:S(2)}) collective-permute-start(bf16[4,32,2176]{2,1,0:T(8,128)(2,1)S(1)} %bitcast.14), channel_id=1, source_target_pairs={{0,32},{32,64},{64,96},{96,128},{128,160},{160,192},{192,224},{224... | collective-permute-start | bytes 1671176 | tf_op jit(solution)/shard_map/ppermute | solution.py:225
  22.5 1.6 %collective-permute-start.6 = (bf16[4,32,2176]{2,1,0:T(8,128)(2,1)S(1)}, bf16[4,32,2176]{2,1,0:T(8,128)(2,1)S(1)}, u32[]{:S(2)}, u32[]{:S(2)}) collective-permute-start(bf16[4,32,2176]{2,1,0:T(8,128)(2,1)S(1)} %bitcast.15), channel_id=1, source_target_pairs={{0,224},{32,0},{64,32},{96,64},{128,96},{160,128},{192,160},{224,1... | collective-permute-start | bytes 1671176 | tf_op jit(solution)/shard_map/ppermute | solution.py:225
  24.1 0.8 collective-permute-start.3
  24.8 19.0 %collective-permute-done.4.refs_1_ = bf16[4,32,2176]{2,1,0:T(8,128)(2,1)S(1)} collective-permute-done((bf16[4,32,2176]{2,1,0:T(8,128)(2,1)S(1)}, bf16[4,32,2176]{2,1,0:T(8,128)(2,1)S(1)}, u32[]{:S(2)}, u32[]{:S(2)}) %collective-permute-start.4) | collective-permute-done | bytes 557088 | tf_op jit(solution)/shard_map/ppermute | solution.py:225
  43.8 1.0 collective-permute-start.5
  44.8 0.9 block_scan.1
  45.6 7.8 %all-to-all-start.1 = ((bf16[64,16,128]{2,1,0:T(8,128)(2,1)}), bf16[64,16,128]{2,1,0:T(8,128)(2,1)S(1)}, u32[]{:S(2)}, u32[]{:S(2)}) async-start(bf16[64,16,128]{2,1,0:T(8,128)(2,1)} %block_scan.1), calls=%async_computation.1 | async-start | bytes 524288 | tf_op jit(solution)/shard_map/all_to_all | solution.py:293
  53.5 1.4 %collective-permute-start.19 = (bf16[4,32,2176]{2,1,0:T(8,128)(2,1)S(1)}, bf16[4,32,2176]{2,1,0:T(8,128)(2,1)}, u32[]{:S(2)}, u32[]{:S(2)}) collective-permute-start(bf16[4,32,2176]{2,1,0:T(8,128)(2,1)S(1)} %collective-permute-done.4.refs_1_), channel_id=1, source_target_pairs={{0,32},{32,64},{64,96},{96,128},{128,160},{160,192},{192,224},{224... | collective-permute-start | bytes 1671176 | tf_op jit(solution)/shard_map/ppermute | solution.py:225
  54.9 1.6 %collective-permute-start.22 = (bf16[4,32,2176]{2,1,0:T(8,128)(2,1)S(1)}, bf16[4,32,2176]{2,1,0:T(8,128)(2,1)}, u32[]{:S(2)}, u32[]{:S(2)}) collective-permute-start(bf16[4,32,2176]{2,1,0:T(8,128)(2,1)S(1)} %collective-permute-done.6.refs_8_), channel_id=1, source_target_pairs={{0,224},{32,0},{64,32},{96,64},{128,96},{160,128},{192,160},{224,1... | collective-permute-start | bytes 1671176 | tf_op jit(solution)/shard_map/ppermute | solution.py:225
  56.5 10.1 %all-to-all-done.1 = bf16[64,16,128]{2,1,0:T(8,128)(2,1)S(1)} async-done(((bf16[64,16,128]{2,1,0:T(8,128)(2,1)}), bf16[64,16,128]{2,1,0:T(8,128)(2,1)S(1)}, u32[]{:S(2)}, u32[]{:S(2)}) %all-to-all-start.1) | async-done | bytes 262176 | tf_op jit(solution)/shard_map/all_to_all | solution.py:293
  66.6 0.7 copy-done
  67.3 3.5 %norm_project.1 = (bf16[32,2048]{1,0:T(8,128)(2,1)}, bf16[32,2048]{1,0:T(8,128)(2,1)}, bf16[32,2048]{1,0:T(8,128)(2,1)}, bf16[32,2048]{1,0:T(8,128)(2,1)}) custom-call(s32[1]{0:T(128)} %bitcast.own_ref, f32[128,512]{1,0:T(8,128)} %get-tuple-element.24.near_ref, bf16[2,128,512]{2,1,0:T(8,128)(2,1)} %get-tuple-element.25.reach_ref, ...), custom_call_target="tpu_custom_call" | custom-call | tf_op jit(solution)/shard_map/norm_project/pallas_call | solution.py:301
  70.9 2.5 %collective-permute-start.10 = (bf16[32,2048]{1,0:T(8,128)(2,1)}, bf16[32,2048]{1,0:T(8,128)(2,1)S(1)}, u32[]{:S(2)}, u32[]{:S(2)}) collective-permute-start(bf16[32,2048]{1,0:T(8,128)(2,1)} %get-tuple-element.33), channel_id=1, source_target_pairs={{0,3},{1,0},{2,1},{3,2},{4,7},{5,4},{6,5},{7,6},{8,11},{9,8},{10,9... | collective-permute-start | bytes 393224 | tf_op jit(solution)/shard_map/ppermute | solution.py:225
  73.3 1.7 %collective-permute-start.9 = (bf16[32,2048]{1,0:T(8,128)(2,1)}, bf16[32,2048]{1,0:T(8,128)(2,1)S(1)}, u32[]{:S(2)}, u32[]{:S(2)}) collective-permute-start(bf16[32,2048]{1,0:T(8,128)(2,1)} %get-tuple-element.32), channel_id=1, source_target_pairs={{0,2},{1,3},{2,0},{3,1},{4,6},{5,7},{6,4},{7,5},{8,10},{9,11},{10,... | collective-permute-start | bytes 393224 | tf_op jit(solution)/shard_map/ppermute | solution.py:225
  75.1 0.9 collective-permute-start.20
  76.0 1.2 collective-permute-start.25
  77.2 2.1 %collective-permute-start.23 = (bf16[4,32,2176]{2,1,0:T(8,128)(2,1)}, bf16[4,32,2176]{2,1,0:T(8,128)(2,1)S(1)}, u32[]{:S(2)}, u32[]{:S(2)}) collective-permute-start(bf16[4,32,2176]{2,1,0:T(8,128)(2,1)} %collective-permute-done.22.refs_7_), channel_id=1, source_target_pairs={{0,224},{32,0},{64,32},{96,64},{128,96},{160,128},{192,160},{224,1... | collective-permute-start | bytes 1671176 | tf_op jit(solution)/shard_map/ppermute | solution.py:225
  79.3 1.1 collective-permute-done.8
  80.4 0.6 collective-permute-done.9
  81.1 1.2 fusion
  82.2 0.1 fusion.2
  82.4 0.9 collective-permute-start.15
  83.2 2.6 %collective-permute-start.30 = (bf16[4,32,2176]{2,1,0:T(8,128)(2,1)}, bf16[4,32,2176]{2,1,0:T(8,128)(2,1)S(1)}, u32[]{:S(2)}, u32[]{:S(2)}) collective-permute-start(bf16[4,32,2176]{2,1,0:T(8,128)(2,1)} %collective-permute-done.22.refs_7_), channel_id=1, source_target_pairs={{0,4},{4,0},{1,5},{5,1},{2,6},{6,2},{3,7},{7,3},{8,12},{12,8},{9,1... | collective-permute-start | bytes 1671176 | tf_op jit(solution)/shard_map/ppermute | solution.py:225
  85.9 3.7 %collective-permute-done.20.refs_3_ = bf16[4,32,2176]{2,1,0:T(8,128)(2,1)S(1)} collective-permute-done((bf16[4,32,2176]{2,1,0:T(8,128)(2,1)}, bf16[4,32,2176]{2,1,0:T(8,128)(2,1)S(1)}, u32[]{:S(2)}, u32[]{:S(2)}) %collective-permute-start.20) | collective-permute-done | bytes 557088 | tf_op jit(solution)/shard_map/ppermute | solution.py:225
  89.6 2.3 %collective-permute-start.12 = (bf16[32,1024]{1,0:T(8,128)(2,1)S(1)}, bf16[32,1024]{1,0:T(8,128)(2,1)S(1)}, u32[]{:S(2)}, u32[]{:S(2)}) collective-permute-start(bf16[32,1024]{1,0:T(8,128)(2,1)S(1)} %get-tuple-element.53), channel_id=1, source_target_pairs={{0,2},{1,3},{2,0},{3,1},{4,6},{5,7},{6,4},{7,5},{8,10},{9,11},{10,... | collective-permute-start | bytes 196616 | tf_op jit(solution)/shard_map/ppermute | solution.py:225
  91.9 1.6 %collective-permute-start.13 = (bf16[32,1024]{1,0:T(8,128)(2,1)S(1)}, bf16[32,1024]{1,0:T(8,128)(2,1)S(1)}, u32[]{:S(2)}, u32[]{:S(2)}) collective-permute-start(bf16[32,1024]{1,0:T(8,128)(2,1)S(1)} %get-tuple-element.53), channel_id=1, source_target_pairs={{0,3},{1,0},{2,1},{3,2},{4,7},{5,4},{6,5},{7,6},{8,11},{9,8},{10,9... | collective-permute-start | bytes 196616 | tf_op jit(solution)/shard_map/ppermute | solution.py:225
  93.6 0.3 collective-permute-start.21
  93.8 0.5 collective-permute-done.12
  94.3 2.0 %collective-permute-start.24 = (bf16[2,32,2176]{2,1,0:T(8,128)(2,1)S(1)}, bf16[2,32,2176]{2,1,0:T(8,128)(2,1)S(1)}, u32[]{:S(2)}, u32[]{:S(2)}) collective-permute-start(bf16[2,32,2176]{2,1,0:T(8,128)(2,1)S(1)} %slice.56), channel_id=1, source_target_pairs={{0,224},{32,0},{64,32},{96,64},{128,96},{160,128},{192,160},{224,1... | collective-permute-start | bytes 835592 | tf_op jit(solution)/shard_map/ppermute | solution.py:225
  96.3 3.2 %collective-permute-start.26 = (bf16[4,32,2176]{2,1,0:T(8,128)(2,1)S(1)}, bf16[4,32,2176]{2,1,0:T(8,128)(2,1)S(1)}, u32[]{:S(2)}, u32[]{:S(2)}) collective-permute-start(bf16[4,32,2176]{2,1,0:T(8,128)(2,1)S(1)} %collective-permute-done.20.refs_3_), channel_id=1, source_target_pairs={{0,4},{4,0},{1,5},{5,1},{2,6},{6,2},{3,7},{7,3},{8,12},{12,8},{9,1... | collective-permute-start | bytes 1671176 | tf_op jit(solution)/shard_map/ppermute | solution.py:225
  99.5 0.1 collective-permute-start.29
  99.6 0.7 collective-permute-done.21.refs_4_
  100.3 3.7 %collective-permute-start.27 = (bf16[2,32,2176]{2,1,0:T(8,128)(2,1)S(1)}, bf16[2,32,2176]{2,1,0:T(8,128)(2,1)S(1)}, u32[]{:S(2)}, u32[]{:S(2)}) collective-permute-start(bf16[2,32,2176]{2,1,0:T(8,128)(2,1)S(1)} %collective-permute-done.21.refs_4_), channel_id=1, source_target_pairs={{0,4},{4,0},{1,5},{5,1},{2,6},{6,2},{3,7},{7,3},{8,12},{12,8},{9,1... | collective-permute-start | bytes 835592 | tf_op jit(solution)/shard_map/ppermute | solution.py:225
  104.0 1.1 collective-permute-start.14
  105.2 1.2 collective-permute-start.16
  106.4 1.9 %collective-permute-start.17 = (bf16[64,1024]{1,0:T(8,128)(2,1)S(1)}, bf16[64,1024]{1,0:T(8,128)(2,1)S(1)}, u32[]{:S(2)}, u32[]{:S(2)}) collective-permute-start(bf16[64,1024]{1,0:T(8,128)(2,1)S(1)} %pad_maximum_fusion.2.refs_3_), channel_id=1, source_target_pairs={{0,2},{1,3},{2,0},{3,1},{4,6},{5,7},{6,4},{7,5},{8,10},{9,11},{10,... | collective-permute-start | bytes 393224 | tf_op jit(solution)/shard_map/ppermute | solution.py:225
  108.4 1.2 collective-permute-start.18
  109.5 0.1 pad_add_fusion.at_ref
  109.6 2.1 %weights_in_order.1 = bf16[8,4,2,32,2176]{4,3,2,1,0:T(8,128)(2,1)S(1)} custom-call(s32[3]{0:T(128)S(1)} %pad_add_fusion.at_ref, bf16[4,32,2176]{2,1,0:T(8,128)(2,1)S(1)} %bitcast.17, bf16[4,32,2176]{2,1,0:T(8,128)(2,1)S(1)} %collective-permute-done.4.refs_1_, bf16[4,32,2176]{2,1,0:T(8,128)(2,1)} %collective-permute-done.19.refs_2_, ...), custom_call_target="tpu_custom_call" | custom-call | tf_op jit(solution)/shard_map/weights_in_order/pallas_call | solution.py:340
  111.7 2.7 %collective-permute-done.17.refs_5_ = bf16[64,1024]{1,0:T(8,128)(2,1)S(1)} collective-permute-done((bf16[64,1024]{1,0:T(8,128)(2,1)S(1)}, bf16[64,1024]{1,0:T(8,128)(2,1)S(1)}, u32[]{:S(2)}, u32[]{:S(2)}) %collective-permute-start.17) | collective-permute-done | bytes 131104 | tf_op jit(solution)/shard_map/ppermute | solution.py:225
  114.5 2.6 %channel_mixer.1 = (f32[64,1024]{1,0:T(8,128)S(1)}, bf16[64,1024]{1,0:T(8,128)(2,1)S(1)}, bf16[64,1024]{1,0:T(8,128)(2,1)S(1)}, bf16[64,1024]{1,0:T(8,128)(2,1)S...) custom-call(s32[1]{0:T(128)} %bitcast.9.refs_0_, bf16[128,1024]{1,0:T(8,128)(2,1)S(1)} %pad_maximum_fusion.1.refs_1_, ...), custom_call_target="tpu_custom_call" | custom-call | tf_op jit(solution)/shard_map/channel_mixer/pallas_call | solution.py:349
  117.1 2.8 %collective-permute-start.31 = (bf16[64,1024]{1,0:T(8,128)(2,1)S(1)}, bf16[64,1024]{1,0:T(8,128)(2,1)S(1)}, u32[]{:S(2)}, u32[]{:S(2)}) collective-permute-start(bf16[64,1024]{1,0:T(8,128)(2,1)S(1)} %get-tuple-element.38), channel_id=1, source_target_pairs={{0,3},{1,0},{2,1},{3,2},{4,7},{5,4},{6,5},{7,6},{8,11},{9,8},{10,9... | collective-permute-start | bytes 393224 | tf_op jit(solution)/shard_map/ppermute | solution.py:225
  119.9 1.3 collective-permute-start.32
  121.2 0.7 collective-permute-start.35
  121.9 0.6 collective-permute-done.31
  122.4 2.8 %collective-permute-done.32 = bf16[64,1024]{1,0:T(8,128)(2,1)S(1)} collective-permute-done((bf16[64,1024]{1,0:T(8,128)(2,1)S(1)}, bf16[64,1024]{1,0:T(8,128)(2,1)S(1)}, u32[]{:S(2)}, u32[]{:S(2)}) %collective-permute-start.32) | collective-permute-done | bytes 131104 | tf_op jit(solution)/shard_map/ppermute | solution.py:225
  125.2 3.7 %collective-permute-done.33 = bf16[64,1024]{1,0:T(8,128)(2,1)S(1)} collective-permute-done((bf16[64,1024]{1,0:T(8,128)(2,1)S(1)}, bf16[64,1024]{1,0:T(8,128)(2,1)S(1)}, u32[]{:S(2)}, u32[]{:S(2)}) %collective-permute-start.33) | collective-permute-done | bytes 131104 | tf_op jit(solution)/shard_map/ppermute | solution.py:225
  128.9 0.1 convert_add_fusion.1
  129.0 2.0 %collective-permute-start.34 = (bf16[32,1024]{1,0:T(8,128)(2,1)S(1)}, bf16[32,1024]{1,0:T(8,128)(2,1)S(1)}, u32[]{:S(2)}, u32[]{:S(2)}) collective-permute-start(bf16[32,1024]{1,0:T(8,128)(2,1)S(1)} %slice.81), channel_id=1, source_target_pairs={{0,8},{8,0},{16,24},{24,16},{1,9},{9,1},{17,25},{25,17},{2,10},{10... | collective-permute-start | bytes 196616 | tf_op jit(solution)/shard_map/ppermute | solution.py:369
  130.9 0.1 fusion.9
  131.0 0.1 collective-permute-start.36
  131.1 0.1 collective-permute-start.37
  131.2 1.4 collective-permute-start.38
  132.6 1.6 %collective-permute-done.36 = bf16[32,1024]{1,0:T(8,128)(2,1)S(1)} collective-permute-done((bf16[32,1024]{1,0:T(8,128)(2,1)S(1)}, bf16[32,1024]{1,0:T(8,128)(2,1)S(1)}, u32[]{:S(2)}, u32[]{:S(2)}) %collective-permute-start.36) | collective-permute-done | bytes 65568 | tf_op jit(solution)/shard_map/ppermute | solution.py:225
  134.2 1.6 %collective-permute-done.37 = bf16[32,1024]{1,0:T(8,128)(2,1)S(1)} collective-permute-done((bf16[32,1024]{1,0:T(8,128)(2,1)S(1)}, bf16[32,1024]{1,0:T(8,128)(2,1)S(1)}, u32[]{:S(2)}, u32[]{:S(2)}) %collective-permute-start.37) | collective-permute-done | bytes 65568 | tf_op jit(solution)/shard_map/ppermute | solution.py:225
  135.8 0.8 collective-permute-done.38
  136.6 0.1 fusion.8
  136.7 0.7 pad_maximum_fusion.3
  (44 shorter events, 0.2 us)
Async XLA Ops:
  3.6 16.5 %collective-permute-start = (bf16[32,2176]{1,0:T(8,128)(2,1)}, bf16[32,2176]{1,0:T(8,128)(2,1)S(1)}, u32[]{:S(2)}, u32[]{:S(2)}) collective-permute-start(bf16[32,2176]{1,0:T(8,128)(2,1)} %get-tuple-element.27), channel_id=1, source_target_pairs={{0,8},{8,16},{16,24},{24,0},{1,9},{9,17},{17,25},{25,1},{2,10},{10... | collective-permute-start | bytes 417800 | tf_op jit(solution)/shard_map/ppermute | solution.py:225
  5.7 14.4 %collective-permute-start.1 = (bf16[32,2176]{1,0:T(8,128)(2,1)}, bf16[32,2176]{1,0:T(8,128)(2,1)S(1)}, u32[]{:S(2)}, u32[]{:S(2)}) collective-permute-start(bf16[32,2176]{1,0:T(8,128)(2,1)} %get-tuple-element.26), channel_id=1, source_target_pairs={{0,16},{8,24},{16,0},{24,8},{1,17},{9,25},{17,1},{25,9},{2,18},{10... | collective-permute-start | bytes 417800 | tf_op jit(solution)/shard_map/ppermute | solution.py:225
  8.4 11.7 %collective-permute-start.2 = (bf16[32,2176]{1,0:T(8,128)(2,1)}, bf16[32,2176]{1,0:T(8,128)(2,1)S(1)}, u32[]{:S(2)}, u32[]{:S(2)}) collective-permute-start(bf16[32,2176]{1,0:T(8,128)(2,1)} %get-tuple-element.27), channel_id=1, source_target_pairs={{0,24},{8,0},{16,8},{24,16},{1,25},{9,1},{17,9},{25,17},{2,26},{10... | collective-permute-start | bytes 417800 | tf_op jit(solution)/shard_map/ppermute | solution.py:225
  9.4 35.4 %all-to-all-start = ((bf16[64,24,128]{2,1,0:T(8,128)(2,1)}), bf16[64,24,128]{2,1,0:T(8,128)(2,1)S(1)}, u32[]{:S(2)}, u32[]{:S(2)}) async-start(bf16[64,24,128]{2,1,0:T(8,128)(2,1)} %get-tuple-element.28), calls=%async_computation | async-start | bytes 786432 | tf_op jit(solution)/shard_map/all_to_all | solution.py:280
  21.1 22.7 %collective-permute-start.4 = (bf16[4,32,2176]{2,1,0:T(8,128)(2,1)S(1)}, bf16[4,32,2176]{2,1,0:T(8,128)(2,1)S(1)}, u32[]{:S(2)}, u32[]{:S(2)}) collective-permute-start(bf16[4,32,2176]{2,1,0:T(8,128)(2,1)S(1)} %bitcast.14), channel_id=1, source_target_pairs={{0,32},{32,64},{64,96},{96,128},{128,160},{160,192},{192,224},{224... | collective-permute-start | bytes 1671176 | tf_op jit(solution)/shard_map/ppermute | solution.py:225
  22.5 22.3 %collective-permute-start.6 = (bf16[4,32,2176]{2,1,0:T(8,128)(2,1)S(1)}, bf16[4,32,2176]{2,1,0:T(8,128)(2,1)S(1)}, u32[]{:S(2)}, u32[]{:S(2)}) collective-permute-start(bf16[4,32,2176]{2,1,0:T(8,128)(2,1)S(1)} %bitcast.15), channel_id=1, source_target_pairs={{0,224},{32,0},{64,32},{96,64},{128,96},{160,128},{192,160},{224,1... | collective-permute-start | bytes 1671176 | tf_op jit(solution)/shard_map/ppermute | solution.py:225
  24.1 32.4 %collective-permute-start.3 = (bf16[4,32,2176]{2,1,0:T(8,128)(2,1)S(1)}, bf16[4,32,2176]{2,1,0:T(8,128)(2,1)S(1)}, u32[]{:S(2)}, u32[]{:S(2)}) collective-permute-start(bf16[4,32,2176]{2,1,0:T(8,128)(2,1)S(1)} %bitcast.16), channel_id=1, source_target_pairs={{0,4},{4,0},{1,5},{5,1},{2,6},{6,2},{3,7},{7,3},{8,12},{12,8},{9,1... | collective-permute-start | bytes 1671176 | tf_op jit(solution)/shard_map/ppermute | solution.py:225
  43.8 12.7 %collective-permute-start.5 = (bf16[4,32,2176]{2,1,0:T(8,128)(2,1)S(1)}, bf16[4,32,2176]{2,1,0:T(8,128)(2,1)S(1)}, u32[]{:S(2)}, u32[]{:S(2)}) collective-permute-start(bf16[4,32,2176]{2,1,0:T(8,128)(2,1)S(1)} %collective-permute-done.4.refs_1_), channel_id=1, source_target_pairs={{0,4},{4,0},{1,5},{5,1},{2,6},{6,2},{3,7},{7,3},{8,12},{12,8},{9,1... | collective-permute-start | bytes 1671176 | tf_op jit(solution)/shard_map/ppermute | solution.py:225
  44.8 11.7 %collective-permute-start.7 = (bf16[4,32,2176]{2,1,0:T(8,128)(2,1)S(1)}, bf16[4,32,2176]{2,1,0:T(8,128)(2,1)}, u32[]{:S(2)}, u32[]{:S(2)}) collective-permute-start(bf16[4,32,2176]{2,1,0:T(8,128)(2,1)S(1)} %collective-permute-done.6.refs_8_), channel_id=1, source_target_pairs={{0,4},{4,0},{1,5},{5,1},{2,6},{6,2},{3,7},{7,3},{8,12},{12,8},{9,1... | collective-permute-start | bytes 1671176 | tf_op jit(solution)/shard_map/ppermute | solution.py:225
  45.6 21.0 %all-to-all-start.1 = ((bf16[64,16,128]{2,1,0:T(8,128)(2,1)}), bf16[64,16,128]{2,1,0:T(8,128)(2,1)S(1)}, u32[]{:S(2)}, u32[]{:S(2)}) async-start(bf16[64,16,128]{2,1,0:T(8,128)(2,1)} %block_scan.1), calls=%async_computation.1 | async-start | bytes 524288 | tf_op jit(solution)/shard_map/all_to_all | solution.py:293
  53.5 21.6 %collective-permute-start.19 = (bf16[4,32,2176]{2,1,0:T(8,128)(2,1)S(1)}, bf16[4,32,2176]{2,1,0:T(8,128)(2,1)}, u32[]{:S(2)}, u32[]{:S(2)}) collective-permute-start(bf16[4,32,2176]{2,1,0:T(8,128)(2,1)S(1)} %collective-permute-done.4.refs_1_), channel_id=1, source_target_pairs={{0,32},{32,64},{64,96},{96,128},{128,160},{160,192},{192,224},{224... | collective-permute-start | bytes 1671176 | tf_op jit(solution)/shard_map/ppermute | solution.py:225
  54.9 21.1 %collective-permute-start.22 = (bf16[4,32,2176]{2,1,0:T(8,128)(2,1)S(1)}, bf16[4,32,2176]{2,1,0:T(8,128)(2,1)}, u32[]{:S(2)}, u32[]{:S(2)}) collective-permute-start(bf16[4,32,2176]{2,1,0:T(8,128)(2,1)S(1)} %collective-permute-done.6.refs_8_), channel_id=1, source_target_pairs={{0,224},{32,0},{64,32},{96,64},{128,96},{160,128},{192,160},{224,1... | collective-permute-start | bytes 1671176 | tf_op jit(solution)/shard_map/ppermute | solution.py:225
  66.6 0.7 copy-start
  67.3 7.7 %copy-start.1 = (bf16[2048]{0:T(1024)(128)(2,1)S(1)}, bf16[2048]{0:T(1024)(128)(2,1)}, u32[]{:S(2)}) copy-start(bf16[2048]{0:T(1024)(128)(2,1)} %param.22) | copy-start | bytes 12292
  70.9 6.4 %collective-permute-start.10 = (bf16[32,2048]{1,0:T(8,128)(2,1)}, bf16[32,2048]{1,0:T(8,128)(2,1)S(1)}, u32[]{:S(2)}, u32[]{:S(2)}) collective-permute-start(bf16[32,2048]{1,0:T(8,128)(2,1)} %get-tuple-element.33), channel_id=1, source_target_pairs={{0,3},{1,0},{2,1},{3,2},{4,7},{5,4},{6,5},{7,6},{8,11},{9,8},{10,9... | collective-permute-start | bytes 393224 | tf_op jit(solution)/shard_map/ppermute | solution.py:225
  73.3 7.1 %collective-permute-start.8 = (bf16[32,2048]{1,0:T(8,128)(2,1)}, bf16[32,2048]{1,0:T(8,128)(2,1)S(1)}, u32[]{:S(2)}, u32[]{:S(2)}) collective-permute-start(bf16[32,2048]{1,0:T(8,128)(2,1)} %get-tuple-element.31), channel_id=1, source_target_pairs={{0,1},{1,2},{2,3},{3,0},{4,5},{5,6},{6,7},{7,4},{8,9},{9,10},{10,1... | collective-permute-start | bytes 393224 | tf_op jit(solution)/shard_map/ppermute | solution.py:225
  73.3 7.7 %collective-permute-start.9 = (bf16[32,2048]{1,0:T(8,128)(2,1)}, bf16[32,2048]{1,0:T(8,128)(2,1)S(1)}, u32[]{:S(2)}, u32[]{:S(2)}) collective-permute-start(bf16[32,2048]{1,0:T(8,128)(2,1)} %get-tuple-element.32), channel_id=1, source_target_pairs={{0,2},{1,3},{2,0},{3,1},{4,6},{5,7},{6,4},{7,5},{8,10},{9,11},{10,... | collective-permute-start | bytes 393224 | tf_op jit(solution)/shard_map/ppermute | solution.py:225
  75.1 14.5 %collective-permute-start.20 = (bf16[4,32,2176]{2,1,0:T(8,128)(2,1)}, bf16[4,32,2176]{2,1,0:T(8,128)(2,1)S(1)}, u32[]{:S(2)}, u32[]{:S(2)}) collective-permute-start(bf16[4,32,2176]{2,1,0:T(8,128)(2,1)} %collective-permute-done.19.refs_2_), channel_id=1, source_target_pairs={{0,32},{32,64},{64,96},{96,128},{128,160},{160,192},{192,224},{224... | collective-permute-start | bytes 1671176 | tf_op jit(solution)/shard_map/ppermute | solution.py:225
  76.0 23.5 %collective-permute-start.25 = (bf16[4,32,2176]{2,1,0:T(8,128)(2,1)}, bf16[4,32,2176]{2,1,0:T(8,128)(2,1)S(1)}, u32[]{:S(2)}, u32[]{:S(2)}) collective-permute-start(bf16[4,32,2176]{2,1,0:T(8,128)(2,1)} %collective-permute-done.19.refs_2_), channel_id=1, source_target_pairs={{0,4},{4,0},{1,5},{5,1},{2,6},{6,2},{3,7},{7,3},{8,12},{12,8},{9,1... | collective-permute-start | bytes 1671176 | tf_op jit(solution)/shard_map/ppermute | solution.py:225
  77.2 14.7 %collective-permute-start.23 = (bf16[4,32,2176]{2,1,0:T(8,128)(2,1)}, bf16[4,32,2176]{2,1,0:T(8,128)(2,1)S(1)}, u32[]{:S(2)}, u32[]{:S(2)}) collective-permute-start(bf16[4,32,2176]{2,1,0:T(8,128)(2,1)} %collective-permute-done.22.refs_7_), channel_id=1, source_target_pairs={{0,224},{32,0},{64,32},{96,64},{128,96},{160,128},{192,160},{224,1... | collective-permute-start | bytes 1671176 | tf_op jit(solution)/shard_map/ppermute | solution.py:225
  82.4 3.5 %collective-permute-start.15 = (bf16[32,1024]{1,0:T(8,128)(2,1)S(1)}, bf16[32,1024]{1,0:T(8,128)(2,1)S(1)}, u32[]{:S(2)}, u32[]{:S(2)}) collective-permute-start(bf16[32,1024]{1,0:T(8,128)(2,1)S(1)} %get-tuple-element.52), channel_id=1, source_target_pairs={{0,8},{8,0},{16,24},{24,16},{1,9},{9,1},{17,25},{25,17},{2,10},{10... | collective-permute-start | bytes 196616 | tf_op jit(solution)/shard_map/ppermute | solution.py:331
  83.2 20.8 %collective-permute-start.30 = (bf16[4,32,2176]{2,1,0:T(8,128)(2,1)}, bf16[4,32,2176]{2,1,0:T(8,128)(2,1)S(1)}, u32[]{:S(2)}, u32[]{:S(2)}) collective-permute-start(bf16[4,32,2176]{2,1,0:T(8,128)(2,1)} %collective-permute-done.22.refs_7_), channel_id=1, source_target_pairs={{0,4},{4,0},{1,5},{5,1},{2,6},{6,2},{3,7},{7,3},{8,12},{12,8},{9,1... | collective-permute-start | bytes 1671176 | tf_op jit(solution)/shard_map/ppermute | solution.py:225
  85.9 7.7 %collective-permute-start.11 = (bf16[32,1024]{1,0:T(8,128)(2,1)S(1)}, bf16[32,1024]{1,0:T(8,128)(2,1)S(1)}, u32[]{:S(2)}, u32[]{:S(2)}) collective-permute-start(bf16[32,1024]{1,0:T(8,128)(2,1)S(1)} %get-tuple-element.53), channel_id=1, source_target_pairs={{0,1},{1,2},{2,3},{3,0},{4,5},{5,6},{6,7},{7,4},{8,9},{9,10},{10,1... | collective-permute-start | bytes 196616 | tf_op jit(solution)/shard_map/ppermute | solution.py:225
  89.6 4.7 %collective-permute-start.12 = (bf16[32,1024]{1,0:T(8,128)(2,1)S(1)}, bf16[32,1024]{1,0:T(8,128)(2,1)S(1)}, u32[]{:S(2)}, u32[]{:S(2)}) collective-permute-start(bf16[32,1024]{1,0:T(8,128)(2,1)S(1)} %get-tuple-element.53), channel_id=1, source_target_pairs={{0,2},{1,3},{2,0},{3,1},{4,6},{5,7},{6,4},{7,5},{8,10},{9,11},{10,... | collective-permute-start | bytes 196616 | tf_op jit(solution)/shard_map/ppermute | solution.py:225
  91.9 4.4 %collective-permute-start.13 = (bf16[32,1024]{1,0:T(8,128)(2,1)S(1)}, bf16[32,1024]{1,0:T(8,128)(2,1)S(1)}, u32[]{:S(2)}, u32[]{:S(2)}) collective-permute-start(bf16[32,1024]{1,0:T(8,128)(2,1)S(1)} %get-tuple-element.53), channel_id=1, source_target_pairs={{0,3},{1,0},{2,1},{3,2},{4,7},{5,4},{6,5},{7,6},{8,11},{9,8},{10,9... | collective-permute-start | bytes 196616 | tf_op jit(solution)/shard_map/ppermute | solution.py:225
  93.6 6.7 %collective-permute-start.21 = (bf16[2,32,2176]{2,1,0:T(8,128)(2,1)S(1)}, bf16[2,32,2176]{2,1,0:T(8,128)(2,1)S(1)}, u32[]{:S(2)}, u32[]{:S(2)}) collective-permute-start(bf16[2,32,2176]{2,1,0:T(8,128)(2,1)S(1)} %slice.55), channel_id=1, source_target_pairs={{0,32},{32,64},{64,96},{96,128},{128,160},{160,192},{192,224},{224... | collective-permute-start | bytes 835592 | tf_op jit(solution)/shard_map/ppermute | solution.py:225
  94.3 9.7 %collective-permute-start.24 = (bf16[2,32,2176]{2,1,0:T(8,128)(2,1)S(1)}, bf16[2,32,2176]{2,1,0:T(8,128)(2,1)S(1)}, u32[]{:S(2)}, u32[]{:S(2)}) collective-permute-start(bf16[2,32,2176]{2,1,0:T(8,128)(2,1)S(1)} %slice.56), channel_id=1, source_target_pairs={{0,224},{32,0},{64,32},{96,64},{128,96},{160,128},{192,160},{224,1... | collective-permute-start | bytes 835592 | tf_op jit(solution)/shard_map/ppermute | solution.py:225
  96.3 12.0 %collective-permute-start.26 = (bf16[4,32,2176]{2,1,0:T(8,128)(2,1)S(1)}, bf16[4,32,2176]{2,1,0:T(8,128)(2,1)S(1)}, u32[]{:S(2)}, u32[]{:S(2)}) collective-permute-start(bf16[4,32,2176]{2,1,0:T(8,128)(2,1)S(1)} %collective-permute-done.20.refs_3_), channel_id=1, source_target_pairs={{0,4},{4,0},{1,5},{5,1},{2,6},{6,2},{3,7},{7,3},{8,12},{12,8},{9,1... | collective-permute-start | bytes 1671176 | tf_op jit(solution)/shard_map/ppermute | solution.py:225
  99.5 10.1 %collective-permute-start.29 = (bf16[4,32,2176]{2,1,0:T(8,128)(2,1)S(1)}, bf16[4,32,2176]{2,1,0:T(8,128)(2,1)S(1)}, u32[]{:S(2)}, u32[]{:S(2)}) collective-permute-start(bf16[4,32,2176]{2,1,0:T(8,128)(2,1)S(1)} %collective-permute-done.23.refs_6_), channel_id=1, source_target_pairs={{0,4},{4,0},{1,5},{5,1},{2,6},{6,2},{3,7},{7,3},{8,12},{12,8},{9,1... | collective-permute-start | bytes 1671176 | tf_op jit(solution)/shard_map/ppermute | solution.py:225
  100.3 4.9 %collective-permute-start.27 = (bf16[2,32,2176]{2,1,0:T(8,128)(2,1)S(1)}, bf16[2,32,2176]{2,1,0:T(8,128)(2,1)S(1)}, u32[]{:S(2)}, u32[]{:S(2)}) collective-permute-start(bf16[2,32,2176]{2,1,0:T(8,128)(2,1)S(1)} %collective-permute-done.21.refs_4_), channel_id=1, source_target_pairs={{0,4},{4,0},{1,5},{5,1},{2,6},{6,2},{3,7},{7,3},{8,12},{12,8},{9,1... | collective-permute-start | bytes 835592 | tf_op jit(solution)/shard_map/ppermute | solution.py:225
  104.0 2.4 %collective-permute-start.28 = (bf16[2,32,2176]{2,1,0:T(8,128)(2,1)S(1)}, bf16[2,32,2176]{2,1,0:T(8,128)(2,1)S(1)}, u32[]{:S(2)}, u32[]{:S(2)}) collective-permute-start(bf16[2,32,2176]{2,1,0:T(8,128)(2,1)S(1)} %collective-permute-done.24.refs_5_), channel_id=1, source_target_pairs={{0,4},{4,0},{1,5},{5,1},{2,6},{6,2},{3,7},{7,3},{8,12},{12,8},{9,1... | collective-permute-start | bytes 835592 | tf_op jit(solution)/shard_map/ppermute | solution.py:225
  104.0 10.4 %collective-permute-start.14 = (bf16[128,1024]{1,0:T(8,128)(2,1)S(1)}, bf16[128,1024]{1,0:T(8,128)(2,1)S(1)}, u32[]{:S(2)}, u32[]{:S(2)}) collective-permute-start(bf16[128,1024]{1,0:T(8,128)(2,1)S(1)} %pad_maximum_fusion.1.refs_1_), channel_id=1, source_target_pairs={{0,8},{8,0},{16,24},{24,16},{1,9},{9,1},{17,25},{25,17},{2,10},{10... | collective-permute-start | bytes 786440 | tf_op jit(solution)/shard_map/ppermute | solution.py:334
  105.2 6.5 %collective-permute-start.16 = (bf16[64,1024]{1,0:T(8,128)(2,1)S(1)}, bf16[64,1024]{1,0:T(8,128)(2,1)S(1)}, u32[]{:S(2)}, u32[]{:S(2)}) collective-permute-start(bf16[64,1024]{1,0:T(8,128)(2,1)S(1)} %pad_maximum_fusion.2.refs_3_), channel_id=1, source_target_pairs={{0,1},{1,2},{2,3},{3,0},{4,5},{5,6},{6,7},{7,4},{8,9},{9,10},{10,1... | collective-permute-start | bytes 393224 | tf_op jit(solution)/shard_map/ppermute | solution.py:225
  106.4 8.1 %collective-permute-start.17 = (bf16[64,1024]{1,0:T(8,128)(2,1)S(1)}, bf16[64,1024]{1,0:T(8,128)(2,1)S(1)}, u32[]{:S(2)}, u32[]{:S(2)}) collective-permute-start(bf16[64,1024]{1,0:T(8,128)(2,1)S(1)} %pad_maximum_fusion.2.refs_3_), channel_id=1, source_target_pairs={{0,2},{1,3},{2,0},{3,1},{4,6},{5,7},{6,4},{7,5},{8,10},{9,11},{10,... | collective-permute-start | bytes 393224 | tf_op jit(solution)/shard_map/ppermute | solution.py:225
  108.4 6.1 %collective-permute-start.18 = (bf16[64,1024]{1,0:T(8,128)(2,1)S(1)}, bf16[64,1024]{1,0:T(8,128)(2,1)S(1)}, u32[]{:S(2)}, u32[]{:S(2)}) collective-permute-start(bf16[64,1024]{1,0:T(8,128)(2,1)S(1)} %pad_maximum_fusion.2.refs_3_), channel_id=1, source_target_pairs={{0,3},{1,0},{2,1},{3,2},{4,7},{5,4},{6,5},{7,6},{8,11},{9,8},{10,9... | collective-permute-start | bytes 393224 | tf_op jit(solution)/shard_map/ppermute | solution.py:225
  117.1 5.3 %collective-permute-start.31 = (bf16[64,1024]{1,0:T(8,128)(2,1)S(1)}, bf16[64,1024]{1,0:T(8,128)(2,1)S(1)}, u32[]{:S(2)}, u32[]{:S(2)}) collective-permute-start(bf16[64,1024]{1,0:T(8,128)(2,1)S(1)} %get-tuple-element.38), channel_id=1, source_target_pairs={{0,3},{1,0},{2,1},{3,2},{4,7},{5,4},{6,5},{7,6},{8,11},{9,8},{10,9... | collective-permute-start | bytes 393224 | tf_op jit(solution)/shard_map/ppermute | solution.py:225
  119.9 5.4 %collective-permute-start.32 = (bf16[64,1024]{1,0:T(8,128)(2,1)S(1)}, bf16[64,1024]{1,0:T(8,128)(2,1)S(1)}, u32[]{:S(2)}, u32[]{:S(2)}) collective-permute-start(bf16[64,1024]{1,0:T(8,128)(2,1)S(1)} %get-tuple-element.39), channel_id=1, source_target_pairs={{0,2},{1,3},{2,0},{3,1},{4,6},{5,7},{6,4},{7,5},{8,10},{9,11},{10,... | collective-permute-start | bytes 393224 | tf_op jit(solution)/shard_map/ppermute | solution.py:225
  121.2 7.7 %collective-permute-start.33 = (bf16[64,1024]{1,0:T(8,128)(2,1)S(1)}, bf16[64,1024]{1,0:T(8,128)(2,1)S(1)}, u32[]{:S(2)}, u32[]{:S(2)}) collective-permute-start(bf16[64,1024]{1,0:T(8,128)(2,1)S(1)} %get-tuple-element.40), channel_id=1, source_target_pairs={{0,1},{1,2},{2,3},{3,0},{4,5},{5,6},{6,7},{7,4},{8,9},{9,10},{10,1... | collective-permute-start | bytes 393224 | tf_op jit(solution)/shard_map/ppermute | solution.py:225
  121.2 9.7 %collective-permute-start.35 = (bf16[128,1024]{1,0:T(8,128)(2,1)S(1)}, bf16[128,1024]{1,0:T(8,128)(2,1)S(1)}, u32[]{:S(2)}, u32[]{:S(2)}) collective-permute-start(bf16[128,1024]{1,0:T(8,128)(2,1)S(1)} %get-tuple-element.42), channel_id=1, source_target_pairs={{0,8},{8,0},{16,24},{24,16},{1,9},{9,1},{17,25},{25,17},{2,10},{10... | collective-permute-start | bytes 786440 | tf_op jit(solution)/shard_map/ppermute | solution.py:360
  129.0 3.6 %collective-permute-start.34 = (bf16[32,1024]{1,0:T(8,128)(2,1)S(1)}, bf16[32,1024]{1,0:T(8,128)(2,1)S(1)}, u32[]{:S(2)}, u32[]{:S(2)}) collective-permute-start(bf16[32,1024]{1,0:T(8,128)(2,1)S(1)} %slice.81), channel_id=1, source_target_pairs={{0,8},{8,0},{16,24},{24,16},{1,9},{9,1},{17,25},{25,17},{2,10},{10... | collective-permute-start | bytes 196616 | tf_op jit(solution)/shard_map/ppermute | solution.py:369
  131.0 3.2 %collective-permute-start.36 = (bf16[32,1024]{1,0:T(8,128)(2,1)S(1)}, bf16[32,1024]{1,0:T(8,128)(2,1)S(1)}, u32[]{:S(2)}, u32[]{:S(2)}) collective-permute-start(bf16[32,1024]{1,0:T(8,128)(2,1)S(1)} %get-tuple-element.47), channel_id=1, source_target_pairs={{0,3},{1,0},{2,1},{3,2},{4,7},{5,4},{6,5},{7,6},{8,11},{9,8},{10,9... | collective-permute-start | bytes 196616 | tf_op jit(solution)/shard_map/ppermute | solution.py:225
  131.1 4.7 %collective-permute-start.37 = (bf16[32,1024]{1,0:T(8,128)(2,1)S(1)}, bf16[32,1024]{1,0:T(8,128)(2,1)S(1)}, u32[]{:S(2)}, u32[]{:S(2)}) collective-permute-start(bf16[32,1024]{1,0:T(8,128)(2,1)S(1)} %get-tuple-element.49), channel_id=1, source_target_pairs={{0,2},{1,3},{2,0},{3,1},{4,6},{5,7},{6,4},{7,5},{8,10},{9,11},{10,... | collective-permute-start | bytes 196616 | tf_op jit(solution)/shard_map/ppermute | solution.py:225
  131.2 5.4 %collective-permute-start.38 = (bf16[32,1024]{1,0:T(8,128)(2,1)S(1)}, bf16[32,1024]{1,0:T(8,128)(2,1)S(1)}, u32[]{:S(2)}, u32[]{:S(2)}) collective-permute-start(bf16[32,1024]{1,0:T(8,128)(2,1)S(1)} %get-tuple-element.48), channel_id=1, source_target_pairs={{0,1},{1,2},{2,3},{3,0},{4,5},{5,6},{6,7},{7,4},{8,9},{9,10},{10,1... | collective-permute-start | bytes 196616 | tf_op jit(solution)/shard_map/ppermute | solution.py:225
